TPU v7x, 128 devices: a whole 4x4x4 slice. The times are simulated.
128 devices in a mesh: ep: 32 (over z, y, core), tp: 4 (over x).
Axes of the slice: x: 4, y: 4, z: 4, core: 2. Of those that a mesh axis runs over, the one named last changes fastest.
Arguments:
- mixer_input: bfloat16 [16384, 2048], P(('ep', 'tp')), may hold values from -6 to 6
- expert_input: bfloat16 [16384, 2048], P(('ep', 'tp')), may hold values from -6 to 6
- mixer_gain: float32 [2048], replicated, may hold values from 0.1 to 1.9
- query_down: bfloat16 [2048, 1536], replicated, may hold values from -0.125 to 0.125
- latent_down: bfloat16 [2048, 512], replicated, may hold values from -0.125 to 0.125
- rotary_down: bfloat16 [2048, 32], replicated, may hold values from -0.125 to 0.125
- query_gain: float32 [1536], replicated, may hold values from 0.8 to 40, as said below
- latent_gain: float32 [512], replicated, may hold values from 0.1 to 1.9
- query_plain: bfloat16 [1536, 1024], P(None, 'tp'), may hold values from -0.15625 to 0.15625
- query_rotary: bfloat16 [1536, 512], P(None, 'tp'), may hold values from -0.15625 to 0.15625
- key_plain: bfloat16 [512, 1024], P(None, 'tp'), may hold values from -0.25 to 0.25
- value_up: bfloat16 [512, 1024], P(None, 'tp'), may hold values from -0.25 to 0.25
- output_proj: bfloat16 [1024, 2048], P('tp'), may hold values from -0.1875 to 0.1875
- mixed_gain: float32 [2048], replicated, may hold values from 0.1 to 1.9
- expert_norm: float32 [2048], replicated, may hold values from 0.1 to 1.9
- route_ids: int32 [16384, 2], P(('ep', 'tp')), may hold values from 0 to 31, all different within a row; in each aligned block of 128 rows (0 to 127, 128 to 255, ...) at most 10 rows name the same one
- route_weight: float32 [16384, 2], P(('ep', 'tp')), may hold values from 0.2 to 1
- gate_proj: bfloat16 [32, 2048, 2048], P('ep', None, 'tp'), may hold values from -0.3984375 to 0.3984375
- up_proj: bfloat16 [32, 2048, 2048], P('ep', None, 'tp'), may hold values from -0.3984375 to 0.3984375
- down_proj: bfloat16 [32, 2048, 2048], P('ep', 'tp'), may hold values from -0.125 to 0.125
- expert_gain: float32 [2048], replicated, may hold values from 0.1 to 1.9
Outputs:
- mixer_out: bfloat16 [16384, 2048], P(('ep', 'tp'))
- expert_out: bfloat16 [16384, 2048], P(('ep', 'tp'))
Inputs may be any that keep to these rules, and one draw needn't show every extreme that they name: `route_ids`: each row names 2 different experts. Within the rows of one device (128 aligned rows) no expert is named more than 10 times, a bound that some block reaches. `query_gain`: Positive.
All inputs are finite; a program needn't handle non-finite values.
Results may differ from a plain program's by a relative error of at most 0.018.
The roundings to bfloat16 on the way count: a program that leaves them out, or rounds other values in their place, can miss the bound.
Values may be sent and summed in bfloat16 or wider, within the bound.
A program may use at most 128 MiB of HBM per device.

v0:
```python
import math

import jax
import jax.numpy as jnp
from jax import lax
from jax.sharding import PartitionSpec as P

NOPE = 64
ROPE = 32
VDIM = 64


EPS = 1e-06
CLAMP = 7.0
ALPHA = 1.702
THETA = 10000.0
FLOOR = -1e30


def in_one_piece(arrays, axis, dim, along):
    widths = [a.shape[along] for a in arrays]
    both = jnp.concatenate(arrays, axis=along)
    out = lax.all_gather(both, axis, axis=dim, tiled=True)
    return tuple(jnp.split(out, [sum(widths[:k]) for k in range(1, len(widths))], axis=along))


def split_up(shard, dim, peers):
    before, after = (shard.shape[:dim], shard.shape[dim + 1 :])
    return jnp.moveaxis(shard.reshape(*before, peers, -1, *after), dim, 0)


def summed_on_arrival(shard, axis, dim):
    blocks = split_up(shard, dim, lax.axis_size(axis))
    arrived = lax.all_to_all(blocks, axis, split_axis=0, concat_axis=0, tiled=True)
    return arrived.astype(jnp.float32).sum(axis=0)


def norm_rows(values, gain):
    values = values.astype(jnp.float32)
    scale = lax.rsqrt(jnp.mean(values * values, axis=-1, keepdims=True) + EPS)
    return values * scale * gain


def turn_tables(positions, width):
    half = width // 2
    freqs = THETA ** (-2.0 * jnp.arange(half, dtype=jnp.float32) / width)
    angles = positions.astype(jnp.float32)[:, None] * freqs[None, :]
    return (jnp.cos(angles), jnp.sin(angles))


def rotate(values, cosine, sine):
    half = values.shape[-1] // 2
    first = values[..., :half]
    second = values[..., half:]
    return jnp.concatenate(
        [first * cosine - second * sine, second * cosine + first * sine], axis=-1
    )


def on_device(
    mixer_input,
    expert_input,
    mixer_gain,
    query_down,
    latent_down,
    rotary_down,
    query_gain,
    latent_gain,
    query_plain,
    query_rotary,
    key_plain,
    value_up,
    output_proj,
    mixed_gain,
    expert_norm,
    route_ids,
    route_weight,
    gate_proj,
    up_proj,
    down_proj,
    expert_gain,
):
    tok_rows = mixer_input.shape[0]
    groups = lax.axis_size("tp")
    group_base = lax.axis_index("ep") * groups * tok_rows
    offset = group_base + lax.axis_index("tp") * tok_rows
    heads_here = query_plain.shape[1] // NOPE
    hidden = norm_rows(mixer_input, mixer_gain).astype(jnp.bfloat16)
    query_lat = norm_rows(
        jnp.dot(hidden, query_down, preferred_element_type=jnp.float32), query_gain
    ).astype(jnp.bfloat16)
    key_lat = norm_rows(
        jnp.dot(hidden, latent_down, preferred_element_type=jnp.float32), latent_gain
    ).astype(jnp.bfloat16)
    cosine, sine = turn_tables(offset + jnp.arange(tok_rows, dtype=jnp.int32), ROPE)
    key_turn = rotate(
        jnp.dot(hidden, rotary_down, preferred_element_type=jnp.float32), cosine, sine
    ).astype(jnp.bfloat16)
    query_rows_all = groups * tok_rows
    scale = (NOPE + ROPE) ** (-0.5)

    def attend_block(carry, keys, values, turned, query_nope, query_pe):
        peak, total, accum = carry
        count = keys.shape[0]
        keys = keys.reshape(count, heads_here, NOPE)
        values = values.reshape(count, heads_here, VDIM)
        scores = jnp.einsum("qhd,khd->qhk", query_nope, keys, preferred_element_type=jnp.float32)
        scores = (
            scores + jnp.einsum("qhr,kr->qhk", query_pe, turned, preferred_element_type=jnp.float32)
        ) * scale
        new_peak = jnp.maximum(peak, jnp.max(scores, axis=-1))
        expos = jnp.exp(scores - new_peak[..., None])
        shrink = jnp.exp(peak - new_peak)
        total = total * shrink + jnp.sum(expos, axis=-1)
        accum = accum * shrink[..., None] + jnp.einsum(
            "qhk,khd->qhd", expos.astype(jnp.bfloat16), values, preferred_element_type=jnp.float32
        )
        return (new_peak, total, accum)

    start_state = (
        jnp.full((query_rows_all, heads_here), FLOOR, jnp.float32),
        jnp.zeros((query_rows_all, heads_here), jnp.float32),
        jnp.zeros((query_rows_all, heads_here, VDIM), jnp.float32),
    )
    collected = in_one_piece((query_lat, key_lat, key_turn), "tp", 0, 1)
    piece = collected[0]
    count = piece.shape[0]
    plain = jnp.dot(piece, query_plain, preferred_element_type=jnp.float32).astype(jnp.bfloat16)
    piece_cos, piece_sin = turn_tables(group_base + jnp.arange(count, dtype=jnp.int32), ROPE)
    rotated = jnp.dot(piece, query_rotary, preferred_element_type=jnp.float32).reshape(
        count, heads_here, ROPE
    )
    rotated = rotate(rotated, piece_cos[:, None, :], piece_sin[:, None, :]).astype(jnp.bfloat16)
    query_all = jnp.concatenate([plain, rotated.reshape(count, heads_here * ROPE)], axis=1)
    latents = collected[1]
    keys = jnp.dot(latents, key_plain, preferred_element_type=jnp.float32).astype(jnp.bfloat16)
    values = jnp.dot(latents, value_up, preferred_element_type=jnp.float32).astype(jnp.bfloat16)
    carry = start_state
    piece = in_one_piece((keys, values, collected[2]), "ep", 0, 1)
    query_nope = query_all[:, : heads_here * NOPE].reshape(query_rows_all, heads_here, NOPE)
    query_pe = query_all[:, heads_here * NOPE :].reshape(query_rows_all, heads_here, ROPE)
    count = piece[0].shape[0]
    size = math.gcd(count, 1024)
    blocked = tuple((item.reshape(count // size, size, item.shape[1]) for item in piece))

    def step(inner, members):
        keys, values, turned = members
        return (attend_block(inner, keys, values, turned, query_nope, query_pe), None)

    carry, _ = lax.scan(step, carry, blocked)
    attended = (
        (carry[2] / carry[1][..., None])
        .astype(jnp.bfloat16)
        .reshape(query_rows_all, heads_here * VDIM)
    )
    rows = attended
    mixed = summed_on_arrival(
        jnp.dot(rows, output_proj, preferred_element_type=jnp.float32).astype(jnp.bfloat16), "tp", 0
    )
    mixer_out = norm_rows(mixed, mixed_gain).astype(jnp.bfloat16)
    expert_hidden = norm_rows(expert_input, expert_norm).astype(jnp.bfloat16)
    experts = lax.axis_size("ep")
    topk = route_ids.shape[1]
    capacity = 5 * tok_rows * topk // (4 * experts)
    slots = experts * capacity
    flat_ids = route_ids.reshape(-1)
    onehot = (flat_ids[:, None] == jnp.arange(experts, dtype=jnp.int32)[None, :]).astype(jnp.int32)
    order = jnp.sum((jnp.cumsum(onehot, axis=0) - onehot) * onehot, axis=1)
    target = flat_ids * capacity + order
    dispatch = jnp.any(
        target.reshape(tok_rows, topk)[None, :, :]
        == jnp.arange(slots, dtype=jnp.int32)[:, None, None],
        axis=2,
    ).astype(jnp.bfloat16)
    outgoing = (
        jnp.dot(dispatch, expert_hidden, preferred_element_type=jnp.float32)
        .astype(jnp.bfloat16)
        .reshape(experts, capacity, expert_hidden.shape[1])
    )
    gate_w = gate_proj[0]
    up_w = up_proj[0]
    down_w = down_proj[0]
    received = lax.all_to_all(outgoing, "ep", split_axis=0, concat_axis=0, tiled=True)
    sources, count, width = received.shape
    rows = received.reshape(sources * count, width)
    piece = lax.all_gather(rows, "tp", axis=0, tiled=True)
    gate = jnp.minimum(jnp.dot(piece, gate_w, preferred_element_type=jnp.float32), CLAMP)
    up = jnp.clip(jnp.dot(piece, up_w, preferred_element_type=jnp.float32), -CLAMP, CLAMP)
    acts = ((up + 1.0) * gate * jax.nn.sigmoid(ALPHA * gate)).astype(jnp.bfloat16)
    sums = summed_on_arrival(
        jnp.dot(acts, down_w, preferred_element_type=jnp.float32).astype(jnp.bfloat16), "tp", 0
    )
    returned = sums.astype(jnp.bfloat16).reshape(sources, count, width)
    back_rows = lax.all_to_all(returned, "ep", split_axis=0, concat_axis=0, tiled=True).reshape(
        slots, expert_hidden.shape[1]
    )
    picked = back_rows[target].astype(jnp.float32).reshape(tok_rows, topk, expert_hidden.shape[1])
    combined = jnp.sum(picked * route_weight[:, :, None], axis=1)
    expert_out = norm_rows(combined, expert_gain).astype(jnp.bfloat16)
    return (mixer_out, expert_out)


def solution(mesh):
    in_specs = (
        P(("ep", "tp"), None),
        P(("ep", "tp"), None),
        P(),
        P(),
        P(),
        P(),
        P(),
        P(),
        P(None, "tp"),
        P(None, "tp"),
        P(None, "tp"),
        P(None, "tp"),
        P("tp", None),
        P(),
        P(),
        P(("ep", "tp"), None),
        P(("ep", "tp"), None),
        P("ep", None, "tp"),
        P("ep", None, "tp"),
        P("ep", "tp", None),
        P(),
    )
    out_specs = (P(("ep", "tp"), None), P(("ep", "tp"), None))
    return jax.shard_map(
        on_device, mesh=mesh, in_specs=in_specs, out_specs=out_specs, check_vma=False
    )
```

profile of v0, /device:TPU:1, one launch (start us, length us, event | category | flops | bytes accessed | tf_op | source)
XLA Modules:
  0.0 379.3 jit_solution(1128897995090948125)
XLA Ops:
  7.3 1.4 fusion.30
  8.7 1.4 fusion.61
  10.5 2.4 multiply_reduce_fusion.4
  12.9 3.9 %multiply_reduce_fusion.3 = (f32[128]{0:T(128)S(1)}, f32[128,1536]{1,0:T(8,128)S(1)}) fusion(bf16[2048,1536]{1,0:T(8,128)(2,1)} %param.26, bf16[128,2048]{1,0:T(8,128)(2,1)S(1)} %copy-done.2, f32[2048]{0:T(1024)S(1)} %copy-done.4, f32[128]{0:T(128)S(1)} %add_rsqrt_fusion.5), kind=kOutput, calls=%fused_computation.59 | convolution fusion | flops 806748032 | bytes 7611392 | tf_op jit(solution)/shard_map/dot_general | solution.py:90
  20.0 1.6 convolution_convert_fusion.2
  21.6 1.5 reshape.232
  23.1 38.0 %all_to_all.20 = bf16[32,10,2048]{2,1,0:T(8,128)(2,1)} all-to-all(bf16[32,10,2048]{2,1,0:T(8,128)(2,1)} %reshape.232), channel_id=1, replica_groups=mesh['ep'=32,'tp'=4] {'ep'}, dimensions={0} | all-to-all | bytes 2621440 | tf_op jit(solution)/shard_map/all_to_all | solution.py:183
  61.1 3.6 reshape.233
  65.9 1.4 convolution_convert_fusion.3
  67.3 1.4 convolution_convert_fusion.4
  69.6 49.6 %all-gather.8.cloned.1.call-done = bf16[1280,2048]{1,0:T(8,128)(2,1)} async-done(((bf16[320,2048]{1,0:T(8,128)(2,1)}), bf16[1280,2048]{1,0:T(8,128)(2,1)}) %all-gather.8.cloned.1.call-update) | async-done | bytes 5242896 | tf_op jit(solution)/shard_map/all_gather | solution.py:186
  119.1 7.6 %convolution_minimum_fusion = f32[1280,512]{1,0:T(8,128)} fusion(bf16[1280,2048]{1,0:T(8,128)(2,1)} %all-gather.8.cloned.1.call-done, bf16[1,2048,512]{2,1,0:T(8,128)(2,1)} %param.40), kind=kOutput, calls=%fused_computation.25 | convolution fusion | flops 2685009920 | bytes 9961472 | tf_op jit(solution)/shard_map/dot_general | solution.py:187
  126.8 10.5 %convolution_convert_fusion = bf16[1280,2048]{1,0:T(8,128)(2,1)} fusion(bf16[1,512,2048]{2,1,0:T(8,128)(2,1)S(1)} %copy-done, f32[1280,512]{1,0:T(8,128)} %convolution_minimum_fusion, bf16[1280,2048]{1,0:T(8,128)(2,1)} %all-gather.8.cloned.1.call-done, bf16[1,2048,512]{2,1,0:T(8,128)(2,1)} %param.41), kind=kOutput, calls=%fused_computation.22 | convolution fusion | flops 5377228800 | bytes 17301504 | tf_op jit(solution)/shard_map/dot_general | solution.py:191
  137.2 5.4 %all-to-all-start.2 = ((bf16[4,320,2048]{2,1,0:T(8,128)(2,1)}), bf16[4,320,2048]{2,1,0:T(8,128)(2,1)}, u32[]{:S(2)}, u32[]{:S(2)}) async-start(bf16[4,320,2048]{2,1,0:T(8,128)(2,1)} %bitcast.103), calls=%async_computation.2 | async-start | bytes 10485760 | tf_op jit(solution)/shard_map/all_to_all | solution.py:34
  142.9 2.1 fusion.23
  145.0 2.0 fusion.27
  147.1 54.7 %all-to-all-done.2 = bf16[4,320,2048]{2,1,0:T(8,128)(2,1)} async-done(((bf16[4,320,2048]{2,1,0:T(8,128)(2,1)}), bf16[4,320,2048]{2,1,0:T(8,128)(2,1)}, u32[]{:S(2)}, u32[]{:S(2)}) %all-to-all-start.2) | async-done | bytes 5242912 | tf_op jit(solution)/shard_map/all_to_all | solution.py:34
  201.8 3.6 reduce_sum.114
  205.4 1.6 reshape.235
  207.0 8.8 %all-to-all-start.3 = ((bf16[32,10,2048]{2,1,0:T(8,128)(2,1)}), bf16[32,10,2048]{2,1,0:T(8,128)(2,1)}, u32[]{:S(2)}, u32[]{:S(2)}) async-start(bf16[32,10,2048]{2,1,0:T(8,128)(2,1)} %reshape.235), calls=%async_computation.3 | async-start | bytes 4194304 | tf_op jit(solution)/shard_map/all_to_all | solution.py:194
  217.2 6.7 %fusion.68 = (bf16[16384,256]{0,1:T(8,128)(2,1)S(1)}, bf16[16384,256]{0,1:T(8,128)(2,1)S(1)}) fusion(bf16[16384,544]{0,1:T(8,128)(2,1)} %all-gather.6.cloned.1.call-done), kind=kLoop, calls=%fused_computation.115 | loop fusion | bytes 33554432 | tf_op jit(solution)/shard_map/split | solution.py:24
  223.9 6.2 %copy_bitcast_fusion = (bf16[16,1024,256]{1,2,0:T(8,128)(2,1)}, bf16[16,1024,256]{1,2,0:T(8,128)(2,1)}) fusion(bf16[32,16,8,1024]{3,2,1,0:T(8,128)(2,1)S(1)} %bitcast.99, bf16[32,16,8,1024]{3,2,1,0:T(8,128)(2,1)S(1)} %bitcast.100), kind=kLoop, calls=%fused_computation.20 | loop fusion | bytes 33554432
  230.2 105.3 %while.15 = (s32[]{:T(128)}, f32[512,4]{0,1:T(4,128)S(1)}, f32[512,4]{0,1:T(4,128)S(1)}, f32[512,4,64]{0,2,1:T(8,128)S(1)}, bf16[16,1024,256]{1,2,0:T(8,128)(2,1...) while((s32[]{:T(128)}, f32[512,4]{0,1:T(4,128)S(1)}, ...), condition=%wide.region_6.7_spmd.clone, body=%wide.region_3.6_spmd.clone.sunk | while | flops 686172160 | bytes 46727300 | solution.py:150
  235.2 1.5 fusion.105
  239.3 1.3 fusion.102
  241.8 1.5 fusion.105
  248.4 1.5 fusion.105
  255.0 1.5 fusion.105
  261.5 1.5 fusion.105
  268.1 1.5 fusion.105
  274.7 1.5 fusion.105
  281.3 1.5 fusion.105
  287.9 1.5 fusion.105
  294.5 1.5 fusion.105
  301.1 1.5 fusion.105
  307.6 1.5 fusion.105
  314.2 1.5 fusion.105
  320.8 1.5 fusion.105
  327.4 1.5 fusion.105
  334.0 1.5 fusion.105
  335.6 3.3 convolution_convert_fusion.1
  338.9 4.8 %all-to-all-start = ((bf16[4,128,2048]{2,1,0:T(8,128)(2,1)}), bf16[4,128,2048]{2,1,0:T(8,128)(2,1)}, u32[]{:S(2)}, u32[]{:S(2)}) async-start(bf16[4,128,2048]{2,1,0:T(8,128)(2,1)} %bitcast.3), calls=%async_computation | async-start | bytes 4194304 | tf_op jit(solution)/shard_map/all_to_all | solution.py:34
  344.0 2.5 reshape.236
  346.5 1.4 gather_fusion
  347.9 1.3 reshape.237
  349.2 3.2 multiply_reduce_fusion
  353.6 16.0 %all-to-all-done = bf16[4,128,2048]{2,1,0:T(8,128)(2,1)} async-done(((bf16[4,128,2048]{2,1,0:T(8,128)(2,1)}), bf16[4,128,2048]{2,1,0:T(8,128)(2,1)}, u32[]{:S(2)}, u32[]{:S(2)}) %all-to-all-start) | async-done | bytes 2097184 | tf_op jit(solution)/shard_map/all_to_all | solution.py:34
  369.5 2.1 convert_reduce_fusion
  (202 shorter events, 88.6 us)
Async XLA Ops:
  7.2 119.6 %copy-start = (bf16[1,512,2048]{2,1,0:T(8,128)(2,1)S(1)}, bf16[1,512,2048]{2,1,0:T(8,128)(2,1)}, u32[]{:S(2)}) copy-start(bf16[1,512,2048]{2,1,0:T(8,128)(2,1)} %param.42) | copy-start | bytes 6291460
  7.2 5.7 %copy-start.2 = (bf16[128,2048]{1,0:T(8,128)(2,1)S(1)}, bf16[128,2048]{1,0:T(8,128)(2,1)}, u32[]{:S(2)}) copy-start(bf16[128,2048]{1,0:T(8,128)(2,1)} %param.23) | copy-start | bytes 1572868
  7.2 5.7 %copy-start.4 = (f32[2048]{0:T(1024)S(1)}, f32[2048]{0:T(1024)}, u32[]{:S(2)}) copy-start(f32[2048]{0:T(1024)} %param.25) | copy-start | bytes 24580
  7.2 57.7 %all-gather.4.cloned.1.call-start = ((), (), s32[]{:S(2)}) async-start(), calls=%async_computation.4 | async-start | bytes 2785280 | tf_op jit(solution)/shard_map/all_gather | solution.py:23
  12.9 4.0 %copy-start.9 = (f32[512]{0:T(512)S(1)}, f32[512]{0:T(512)}, u32[]{:S(2)}) copy-start(f32[512]{0:T(512)} %param.30) | copy-start | bytes 6148
  12.9 4.1 %copy-start.5 = (f32[1536]{0:T(1024)S(1)}, f32[1536]{0:T(1024)}, u32[]{:S(2)}) copy-start(f32[1536]{0:T(1024)} %param.29) | copy-start | bytes 18436
  16.8 1.3 copy-start.10
  16.8 3.0 copy-start.3
  16.8 3.2 copy-start.6
  18.1 101.0 %all-gather.8.cloned.1.call-start = ((), (), s32[]{:S(2)}) async-start(), calls=%async_computation.6 | async-start | bytes 6553600 | tf_op jit(solution)/shard_map/all_gather | solution.py:186
  61.1 4.8 %copy-start.14 = (bf16[512,256]{1,0:T(8,128)(2,1)S(1)}, bf16[512,256]{1,0:T(8,128)(2,1)}, u32[]{:S(2)}) copy-start(bf16[512,256]{1,0:T(8,128)(2,1)} %param.34) | copy-start | bytes 786436
  61.1 6.2 %copy-start.15 = (bf16[512,256]{1,0:T(8,128)(2,1)S(1)}, bf16[512,256]{1,0:T(8,128)(2,1)}, u32[]{:S(2)}) copy-start(bf16[512,256]{1,0:T(8,128)(2,1)} %param.33) | copy-start | bytes 786436
  64.8 151.0 %all-gather.6.cloned.1.call-start = ((), (), s32[]{:S(2)}) async-start(), calls=%async_computation.5 | async-start | bytes 18382848 | tf_op jit(solution)/shard_map/all_gather | solution.py:23
  137.2 5.7 %copy-start.13 = (bf16[1536,128]{1,0:T(8,128)(2,1)S(1)}, bf16[1536,128]{1,0:T(8,128)(2,1)}, u32[]{:S(2)}) copy-start(bf16[1536,128]{1,0:T(8,128)(2,1)} %param.32) | copy-start | bytes 1179652
  137.2 64.6 %all-to-all-start.2 = ((bf16[4,320,2048]{2,1,0:T(8,128)(2,1)}), bf16[4,320,2048]{2,1,0:T(8,128)(2,1)}, u32[]{:S(2)}, u32[]{:S(2)}) async-start(bf16[4,320,2048]{2,1,0:T(8,128)(2,1)} %bitcast.103), calls=%async_computation.2 | async-start | bytes 10485760 | tf_op jit(solution)/shard_map/all_to_all | solution.py:34
  142.6 2.4 copy-start.12
  207.0 131.9 %all-to-all-start.3 = ((bf16[32,10,2048]{2,1,0:T(8,128)(2,1)}), bf16[32,10,2048]{2,1,0:T(8,128)(2,1)}, u32[]{:S(2)}, u32[]{:S(2)}) async-start(bf16[32,10,2048]{2,1,0:T(8,128)(2,1)} %reshape.235), calls=%async_computation.3 | async-start | bytes 4194304 | tf_op jit(solution)/shard_map/all_to_all | solution.py:194
  215.8 1.2 slice-start
  338.9 5.0 %copy-start.11 = (f32[128,2]{0,1:T(2,128)S(1)}, f32[128,2]{0,1:T(2,128)}, u32[]{:S(2)}) copy-start(f32[128,2]{0,1:T(2,128)} %param.39) | copy-start | bytes 3076
  338.9 30.6 %all-to-all-start = ((bf16[4,128,2048]{2,1,0:T(8,128)(2,1)}), bf16[4,128,2048]{2,1,0:T(8,128)(2,1)}, u32[]{:S(2)}, u32[]{:S(2)}) async-start(bf16[4,128,2048]{2,1,0:T(8,128)(2,1)} %bitcast.3), calls=%async_computation | async-start | bytes 4194304 | tf_op jit(solution)/shard_map/all_to_all | solution.py:34
  349.2 3.3 copy-start.7
  352.6 19.2 %copy-start.8 = (f32[2048]{0:T(1024)S(1)}, f32[2048]{0:T(1024)}, u32[]{:S(2)}) copy-start(f32[2048]{0:T(1024)} %param.36) | copy-start | bytes 24580
  352.6 20.2 %copy-start.1 = (bf16[1,512,2048]{2,1,0:T(8,128)(2,1)S(1)}, bf16[1,512,2048]{2,1,0:T(8,128)(2,1)}, u32[]{:S(2)}) copy-start(bf16[1,512,2048]{2,1,0:T(8,128)(2,1)} %param.42) | copy-start | bytes 6291460
Sparse Core Ops, SparseCore 0:
  18.2 34.8 all-gather.3
  64.9 54.1 all-gather.7
  121.3 83.8 all-gather.5
where the time goes:
time: 381 us; the launch traced here: 379 us
  waiting for transfers between devices  120 us (31%)
  matrix products  103 us (27%)
  local copies, waits for them, and re-layouts  50 us (13%)
  blocking collectives  38 us (10%)
  other arithmetic  33.4 us (9%)
  starting transfers between devices  19.1 us (5%)
  between operations  14.3 us (4%)
    all_to_all x2, waiting for transfers between devices, summed_on_arrival(): lax.all_to_all(blocks, axis, split_axis=0, concat_axis=0, tiled=True)  70.7 us
    all_gather x1, waiting for transfers between devices, on_device(): piece = lax.all_gather(rows, 'tp', axis=0, tiled=True)  49.6 us
    all_to_all x1, blocking collectives, on_device(): lax.all_to_all(outgoing, 'ep', split_axis=0, concat_axis=0, tiled=True)  38 us
    dot_general x16, matrix products, attend_block(): jnp.einsum('qhk,khd->qhd', expos.astype(jnp.bfloat16), values, preferred_...  24.2 us
    dot_general x16, matrix products, attend_block(): jnp.einsum('qhr,kr->qhk', query_pe, turned, preferred_element_type=jnp.fl...  20.8 us
    dot_general x16, matrix products, attend_block(): jnp.einsum('qhd,khd->qhk', query_nope, keys, preferred_element_type=jnp.f...  20.6 us
    dynamic_slice x16, local copies, waits for them, and re-layouts, on_device(): carry, _ = lax.scan(step, carry, blocked)  20.4 us
    reduce_sum x16, other arithmetic, attend_block(): total = total * shrink + jnp.sum(expos, axis=-1)  18 us
  transfers between devices with their start and end apart: 6, of which 3 were waited for; matrix products, arithmetic and copies ran while one was open for 45% of the time, Pallas kernels for 0%

commit v1 on v0

--- a/solution.py
+++ b/solution.py
@@ -1,8 +1,10 @@
-import math
+import functools
 
 import jax
 import jax.numpy as jnp
 from jax import lax
+from jax.experimental import pallas as pl
+from jax.experimental.pallas import tpu as pltpu
 from jax.sharding import PartitionSpec as P
 
 NOPE = 64
@@ -15,6 +17,127 @@
 ALPHA = 1.702
 THETA = 10000.0
 FLOOR = -1e30
+LOG2E = 1.4426950408889634
+C = (NOPE + ROPE) ** (-0.5) * LOG2E
+SUB = 128
+
+def attend_kernel(heads, qn_ref, qt_ref, kv_ref, o_ref, rhs, s_buf, p_buf, peak, acc):
+    step = pl.program_id(0)
+    pair, size = kv_ref.shape[0], kv_ref.shape[2]
+    subs = size // SUB
+    wide = heads * NOPE
+    rows = pair * SUB
+    queries = qn_ref.shape[1]
+
+    @pl.when(step == 0)
+    def _():
+        rhs[...] = jnp.zeros_like(rhs)
+        for h in range(heads):
+            for j in range(subs):
+                at = h % 2 * NOPE
+                rhs[h, j, at : at + NOPE, :] = qn_ref[h * NOPE : (h + 1) * NOPE, :]
+                low = 128 + j * ROPE
+                rhs[h, j, low : low + ROPE, :] = qt_ref[h * ROPE : (h + 1) * ROPE, :]
+        peak[...] = jnp.full_like(peak, -1e30)
+        acc[...] = jnp.zeros_like(acc)
+
+    turned = jnp.concatenate(
+        [
+            kv_ref[b, 2 * wide :, g * 128 : (g + 1) * 128]
+            for b in range(pair)
+            for g in range(size // 128)
+        ],
+        axis=0,
+    )
+
+    def scores(h):
+        half = wide // SUB
+        best = None
+        for j in range(subs):
+            left = jnp.concatenate(
+                [
+                    kv_ref[
+                        b,
+                        j % half * SUB : (j % half + 1) * SUB,
+                        j // half * wide + h // 2 * 128 : j // half * wide + h // 2 * 128 + 128,
+                    ]
+                    for b in range(pair)
+                ],
+                axis=0,
+            )
+            left = jnp.concatenate([left, turned], axis=1)
+            part = jnp.dot(left, rhs[h, j], preferred_element_type=jnp.float32)
+            s_buf[h % 2, j * rows : (j + 1) * rows, :] = part
+            top = jnp.max(part.reshape(rows // 8, 8, queries), axis=0)
+            best = top if best is None else jnp.maximum(best, top)
+        return jnp.max(best, axis=0, keepdims=True)
+
+    def finish(h, best):
+        old = peak[h : h + 1, :]
+        new = jnp.maximum(old, best)
+        peak[h : h + 1, :] = new
+        shrink = jnp.exp2((old - new) * C)
+        base = new * C
+        for j in range(subs):
+            at = slice(j * rows, (j + 1) * rows)
+            p_buf[h % 2, at, :] = jnp.exp2(s_buf[h % 2, at, :] * C - base).astype(jnp.bfloat16)
+        left = jnp.concatenate(
+            [
+                kv_ref[b, wide + h * VDIM : wide + (h + 1) * VDIM, j * SUB : (j + 1) * SUB]
+                for j in range(subs)
+                for b in range(pair)
+            ],
+            axis=1,
+        )
+        left = jnp.concatenate([left, jnp.ones((16, left.shape[1]), jnp.bfloat16)], axis=0)
+        more = jnp.dot(left, p_buf[h % 2], preferred_element_type=jnp.float32)
+        acc[h] = acc[h] * shrink + more
+
+    best = scores(0)
+    for h in range(heads):
+        later = scores(h + 1) if h + 1 < heads else None
+        finish(h, best)
+        best = later
+
+    @pl.when(step == pl.num_programs(0) - 1)
+    def _():
+        for h in range(heads):
+            o_ref[h * VDIM : (h + 1) * VDIM, :] = (
+                acc[h, :VDIM, :] / acc[h, VDIM : VDIM + 1, :]
+            ).astype(jnp.bfloat16)
+
+
+def attend(qn, qt, packed, pair=2):
+    heads = qn.shape[0] // NOPE
+    queries = qn.shape[1]
+    blocks, height, size = packed.shape
+    subs = size // SUB
+    return pl.pallas_call(
+        functools.partial(attend_kernel, heads),
+        out_shape=jax.ShapeDtypeStruct((heads * VDIM, queries), jnp.bfloat16),
+        grid=(blocks // pair,),
+        in_specs=[
+            pl.BlockSpec(qn.shape, lambda i: (0, 0)),
+            pl.BlockSpec(qt.shape, lambda i: (0, 0)),
+            pl.BlockSpec((pair, height, size), lambda i: (i, 0, 0)),
+        ],
+        out_specs=pl.BlockSpec((heads * VDIM, queries), lambda i: (0, 0)),
+        scratch_shapes=[
+            pltpu.VMEM((heads, subs, 256, queries), jnp.bfloat16),
+            pltpu.VMEM((2, pair * size, queries), jnp.float32),
+            pltpu.VMEM((2, pair * size, queries), jnp.bfloat16),
+            pltpu.VMEM((8, queries), jnp.float32),
+            pltpu.VMEM((heads, VDIM + 16, queries), jnp.float32),
+        ],
+        compiler_params=pltpu.CompilerParams(
+            dimension_semantics=("arbitrary",), vmem_limit_bytes=56 * 1024 * 1024
+        ),
+        cost_estimate=pl.CostEstimate(
+            flops=2 * heads * queries * blocks * size * (256 + VDIM),
+            bytes_accessed=blocks * height * size * 2,
+            transcendentals=heads * queries * blocks * size,
+        ),
+    )(qn, qt, packed)
 
 
 def in_one_piece(arrays, axis, dim, along):
@@ -96,66 +219,45 @@
     key_turn = rotate(
         jnp.dot(hidden, rotary_down, preferred_element_type=jnp.float32), cosine, sine
     ).astype(jnp.bfloat16)
-    query_rows_all = groups * tok_rows
-    scale = (NOPE + ROPE) ** (-0.5)
-
-    def attend_block(carry, keys, values, turned, query_nope, query_pe):
-        peak, total, accum = carry
-        count = keys.shape[0]
-        keys = keys.reshape(count, heads_here, NOPE)
-        values = values.reshape(count, heads_here, VDIM)
-        scores = jnp.einsum("qhd,khd->qhk", query_nope, keys, preferred_element_type=jnp.float32)
-        scores = (
-            scores + jnp.einsum("qhr,kr->qhk", query_pe, turned, preferred_element_type=jnp.float32)
-        ) * scale
-        new_peak = jnp.maximum(peak, jnp.max(scores, axis=-1))
-        expos = jnp.exp(scores - new_peak[..., None])
-        shrink = jnp.exp(peak - new_peak)
-        total = total * shrink + jnp.sum(expos, axis=-1)
-        accum = accum * shrink[..., None] + jnp.einsum(
-            "qhk,khd->qhd", expos.astype(jnp.bfloat16), values, preferred_element_type=jnp.float32
+    collected = in_one_piece((query_lat, key_lat), "tp", 0, 1)
+    turned = lax.all_gather(key_turn, "tp", axis=1, tiled=True)
+    qlat, latents = collected
+    count = qlat.shape[0]
+    across = (((0,), (1,)), ((), ()))
+    qn = lax.dot_general(query_plain, qlat, across, preferred_element_type=jnp.float32).astype(
+        jnp.bfloat16
+    )
+    rotated = lax.dot_general(query_rotary, qlat, across, preferred_element_type=jnp.float32)
+    rotated = rotated.reshape(heads_here, 2, ROPE // 2, count)
+    all_cos, all_sin = turn_tables(group_base + jnp.arange(count, dtype=jnp.int32), ROPE)
+    all_cos, all_sin = all_cos.T[None], all_sin.T[None]
+    first, second = rotated[:, 0], rotated[:, 1]
+    qt = (
+        jnp.concatenate(
+            [first * all_cos - second * all_sin, second * all_cos + first * all_sin], axis=1
         )
-        return (new_peak, total, accum)
-
-    start_state = (
-        jnp.full((query_rows_all, heads_here), FLOOR, jnp.float32),
-        jnp.zeros((query_rows_all, heads_here), jnp.float32),
-        jnp.zeros((query_rows_all, heads_here, VDIM), jnp.float32),
-    )
-    collected = in_one_piece((query_lat, key_lat, key_turn), "tp", 0, 1)
-    piece = collected[0]
-    count = piece.shape[0]
-    plain = jnp.dot(piece, query_plain, preferred_element_type=jnp.float32).astype(jnp.bfloat16)
-    piece_cos, piece_sin = turn_tables(group_base + jnp.arange(count, dtype=jnp.int32), ROPE)
-    rotated = jnp.dot(piece, query_rotary, preferred_element_type=jnp.float32).reshape(
-        count, heads_here, ROPE
-    )
-    rotated = rotate(rotated, piece_cos[:, None, :], piece_sin[:, None, :]).astype(jnp.bfloat16)
-    query_all = jnp.concatenate([plain, rotated.reshape(count, heads_here * ROPE)], axis=1)
-    latents = collected[1]
+        .astype(jnp.bfloat16)
+        .reshape(heads_here * ROPE, count)
+    )
     keys = jnp.dot(latents, key_plain, preferred_element_type=jnp.float32).astype(jnp.bfloat16)
-    values = jnp.dot(latents, value_up, preferred_element_type=jnp.float32).astype(jnp.bfloat16)
-    carry = start_state
-    piece = in_one_piece((keys, values, collected[2]), "ep", 0, 1)
-    query_nope = query_all[:, : heads_here * NOPE].reshape(query_rows_all, heads_here, NOPE)
-    query_pe = query_all[:, heads_here * NOPE :].reshape(query_rows_all, heads_here, ROPE)
-    count = piece[0].shape[0]
-    size = math.gcd(count, 1024)
-    blocked = tuple((item.reshape(count // size, size, item.shape[1]) for item in piece))
-
-    def step(inner, members):
-        keys, values, turned = members
-        return (attend_block(inner, keys, values, turned, query_nope, query_pe), None)
-
-    carry, _ = lax.scan(step, carry, blocked)
-    attended = (
-        (carry[2] / carry[1][..., None])
-        .astype(jnp.bfloat16)
-        .reshape(query_rows_all, heads_here * VDIM)
-    )
-    rows = attended
+    values = lax.dot_general(value_up, latents, across, preferred_element_type=jnp.float32).astype(
+        jnp.bfloat16
+    )
+    half = heads_here * NOPE
+    keys = jnp.concatenate([keys[g * half : (g + 1) * half] for g in range(count // half)], axis=1)
+    strips = tok_rows * turned.shape[1] // count
+    turned = jnp.concatenate(
+        [turned[g * strips : (g + 1) * strips] for g in range(tok_rows // strips)], axis=1
+    )
+    packed = jnp.concatenate([keys, values, turned], axis=0)
+    packed = lax.all_gather(packed, "ep", axis=0, tiled=False)
+    attended = attend(qn, qt, packed)
     mixed = summed_on_arrival(
-        jnp.dot(rows, output_proj, preferred_element_type=jnp.float32).astype(jnp.bfloat16), "tp", 0
+        lax.dot_general(
+            attended, output_proj, (((0,), (0,)), ((), ())), preferred_element_type=jnp.float32
+        ).astype(jnp.bfloat16),
+        "tp",
+        0,
     )
     mixer_out = norm_rows(mixed, mixed_gain).astype(jnp.bfloat16)
     expert_hidden = norm_rows(expert_input, expert_norm).astype(jnp.bfloat16)

time: 381 us -> 309 us (0.81)
  matrix products: 103 us -> 35.7 us
  Pallas kernels: 0 us -> 50.8 us
  local copies, waits for them, and re-layouts: 50 us -> 13.2 us
  other arithmetic: 33.4 us -> 17.4 us
  blocking collectives: 38 us -> 47.4 us
  waiting for transfers between devices: 120 us -> 111 us
    dot_general x52 -> x4, matrix products: 74.4 us -> 7.93 us  [the longest x1 3.03 us: on_device(): lax.dot_general(attended, output_proj, (((0,), (0,)), ((), ())), preferre...]
    pallas_call x0 -> x1, Pallas kernels: none -> 50.8 us  [attend(): pl.pallas_call(functools.partial(attend_kernel, heads), out_shape=jax.Sha...]
    dynamic_slice x16 -> x0, local copies, waits for them, and re-layouts: 20.4 us -> none  [on_device(): carry, _ = lax.scan(step, carry, blocked)]
    reduce_sum x16 -> x0, other arithmetic: 18 us -> none  [attend_block(): total = total * shrink + jnp.sum(expos, axis=-1)]
    all_gather x0 -> x1, blocking collectives: none -> 9.38 us  [on_device(): turned = lax.all_gather(key_turn, 'tp', axis=1, tiled=True)]
    all_gather x1, waiting for transfers between devices: 49.6 us -> 40.3 us  [on_device(): piece = lax.all_gather(rows, 'tp', axis=0, tiled=True)]
    split x5 -> x0, local copies, waits for them, and re-layouts: 8.96 us -> none  [in_one_piece(): jnp.split(out, [sum(widths[:k]) for k in range(1, len(widths))], axis=along)]
    unnamed x35 -> x42, local copies, waits for them, and re-layouts: 6.57 us -> 0.33 us
  transfers between devices with their start and end apart: 6 -> 6, of which waited for: 3 -> 3; matrix products, arithmetic and copies ran while one was open for 45% -> 18% of each run, Pallas kernels for 0% -> 16%
where the time goes in v1:
time: 309 us; the launch traced here: 308 us
  waiting for transfers between devices  111 us (36%)
  Pallas kernels  50.8 us (16%)
  blocking collectives  47.4 us (15%)
  matrix products  35.7 us (12%)
  starting transfers between devices  19 us (6%)
  other arithmetic  17.4 us (6%)
  between operations  14.2 us (5%)
  local copies, waits for them, and re-layouts  13.2 us (4%)
    all_to_all x2, waiting for transfers between devices, summed_on_arrival(): lax.all_to_all(blocks, axis, split_axis=0, concat_axis=0, tiled=True)  70.3 us
    pallas_call x1, Pallas kernels, attend(): pl.pallas_call(functools.partial(attend_kernel, heads), out_shape=jax.Sha...  50.8 us
    all_gather x1, waiting for transfers between devices, on_device(): piece = lax.all_gather(rows, 'tp', axis=0, tiled=True)  40.3 us
    all_to_all x1, blocking collectives, on_device(): lax.all_to_all(outgoing, 'ep', split_axis=0, concat_axis=0, tiled=True)  38 us
    dot_general x1, matrix products, on_device(): jnp.dot(acts, down_w, preferred_element_type=jnp.float32)  10.5 us
    all_to_all x2, starting transfers between devices, summed_on_arrival(): lax.all_to_all(blocks, axis, split_axis=0, concat_axis=0, tiled=True)  10.2 us
    all_gather x1, blocking collectives, on_device(): turned = lax.all_gather(key_turn, 'tp', axis=1, tiled=True)  9.38 us
    all_to_all x1, starting transfers between devices, on_device(): lax.all_to_all(returned, 'ep', split_axis=0, concat_axis=0, tiled=True)  8.7 us
  transfers between devices with their start and end apart: 6, of which 3 were waited for; matrix products, arithmetic and copies ran while one was open for 18% of the time, Pallas kernels for 16%

profile of v1, /device:TPU:1, one launch (start us, length us, event | category | flops | bytes accessed | tf_op | source)
XLA Modules:
  0.0 308.5 jit_solution(12752314583323973436)
XLA Ops:
  7.3 1.4 fusion.18
  8.6 2.4 multiply_reduce_fusion.4
  11.0 3.9 %multiply_reduce_fusion.3 = (f32[128]{0:T(128)S(1)}, f32[128,1536]{1,0:T(8,128)S(1)}) fusion(bf16[2048,1536]{1,0:T(8,128)(2,1)} %param.24, bf16[128,2048]{1,0:T(8,128)(2,1)S(1)} %copy-done.2, f32[2048]{0:T(1024)S(1)} %copy-done.8, f32[128]{0:T(128)S(1)} %add_rsqrt_fusion.5), kind=kOutput, calls=%fused_computation.39 | convolution fusion | flops 806748032 | bytes 7611392 | tf_op jit(solution)/shard_map/dot_general | solution.py:213
  15.1 0.1 multiply_convert_fusion.2
  15.3 0.8 pad_maximum_fusion
  16.2 0.1 copy.58
  16.3 0.1 eq.38
  16.4 0.1 eq.42
  16.6 0.6 reduce-window.6
  17.2 0.2 slice_reduce_fusion
  17.5 0.1 reduce_sum.103
  17.8 0.2 fusion.21
  18.0 1.6 convolution_convert_fusion.2
  19.7 1.5 reshape.210
  21.2 38.0 %all_to_all.20 = bf16[32,10,2048]{2,1,0:T(8,128)(2,1)} all-to-all(bf16[32,10,2048]{2,1,0:T(8,128)(2,1)} %reshape.210), channel_id=1, replica_groups=mesh['ep'=32,'tp'=4] {'ep'}, dimensions={0} | all-to-all | bytes 2621440 | tf_op jit(solution)/shard_map/all_to_all | solution.py:285
  59.2 3.6 %reshape.211 = bf16[320,2048]{1,0:T(8,128)(2,1)} reshape(bf16[32,10,2048]{2,1,0:T(8,128)(2,1)} %all_to_all.20) | data formatting | bytes 2621440 | tf_op jit(solution)/shard_map/reshape | solution.py:287
  63.0 0.3 fusion.49
  63.3 0.1 fusion.41
  63.5 9.4 %all_gather.16 = bf16[128,128]{0,1:T(8,128)(2,1)S(1)} all-gather(bf16[128,32]{0,1:T(8,128)(2,1)S(1)} %pad_maximum_fusion.2), channel_id=1, replica_groups=mesh['ep'=32,'tp'=4] {'tp'}, dimensions={1}, use_global_device_ids=true | all-gather | bytes 40960 | tf_op jit(solution)/shard_map/all_gather | solution.py:223
  73.0 1.4 convolution_convert_fusion.4
  74.5 1.3 fusion.14
  75.9 1.0 copy.57
  76.9 40.3 %all-gather.7.cloned.1.call-done = bf16[1280,2048]{1,0:T(8,128)(2,1)} async-done(((bf16[320,2048]{1,0:T(8,128)(2,1)}), bf16[1280,2048]{1,0:T(8,128)(2,1)}) %all-gather.7.cloned.1.call-update) | async-done | bytes 5242896 | tf_op jit(solution)/shard_map/all_gather | solution.py:288
  117.2 7.6 %convolution_minimum_fusion = f32[1280,512]{1,0:T(8,128)} fusion(bf16[1280,2048]{1,0:T(8,128)(2,1)} %all-gather.7.cloned.1.call-done, bf16[1,2048,512]{2,1,0:T(8,128)(2,1)} %param.38), kind=kOutput, calls=%fused_computation.4 | convolution fusion | flops 2685009920 | bytes 9961472 | tf_op jit(solution)/shard_map/dot_general | solution.py:289
  124.9 10.5 %convolution_convert_fusion = bf16[1280,2048]{1,0:T(8,128)(2,1)} fusion(bf16[1,512,2048]{2,1,0:T(8,128)(2,1)S(1)} %copy-done, f32[1280,512]{1,0:T(8,128)} %convolution_minimum_fusion, bf16[1280,2048]{1,0:T(8,128)(2,1)} %all-gather.7.cloned.1.call-done, bf16[1,2048,512]{2,1,0:T(8,128)(2,1)} %param.39), kind=kOutput, calls=%fused_computation.1 | convolution fusion | flops 5377228800 | bytes 17301504 | tf_op jit(solution)/shard_map/dot_general | solution.py:293
  135.3 5.4 %all-to-all-start.2 = ((bf16[4,320,2048]{2,1,0:T(8,128)(2,1)}), bf16[4,320,2048]{2,1,0:T(8,128)(2,1)}, u32[]{:S(2)}, u32[]{:S(2)}) async-start(bf16[4,320,2048]{2,1,0:T(8,128)(2,1)} %bitcast.71), calls=%async_computation.2 | async-start | bytes 10485760 | tf_op jit(solution)/shard_map/all_to_all | solution.py:157
  140.8 0.2 multiply_cosine_fusion
  141.0 2.2 fusion.7
  143.3 0.7 pad_maximum_fusion.1
  143.9 1.3 fusion.15.qn_ref
  145.3 54.6 %all-to-all-done.2 = bf16[4,320,2048]{2,1,0:T(8,128)(2,1)} async-done(((bf16[4,320,2048]{2,1,0:T(8,128)(2,1)}), bf16[4,320,2048]{2,1,0:T(8,128)(2,1)}, u32[]{:S(2)}, u32[]{:S(2)}) %all-to-all-start.2) | async-done | bytes 5242912 | tf_op jit(solution)/shard_map/all_to_all | solution.py:157
  199.9 3.6 %reduce_sum.105 = bf16[320,2048]{1,0:T(8,128)(2,1)S(1)} reduce(bf16[4,320,2048]{2,1,0:T(8,128)(2,1)} %all-to-all-done.2, bf16[]{:T(256)} %constant.59.clone.1), dimensions={0}, to_apply=%region_10.11 | reduce | flops 1966080 | bytes 6553602 | tf_op jit(solution)/shard_map/reduce_sum | solution.py:158
  203.5 1.6 reshape.213
  205.1 8.7 %all-to-all-start.3 = ((bf16[32,10,2048]{2,1,0:T(8,128)(2,1)}), bf16[32,10,2048]{2,1,0:T(8,128)(2,1)S(1)}, u32[]{:S(2)}, u32[]{:S(2)}) async-start(bf16[32,10,2048]{2,1,0:T(8,128)(2,1)} %reshape.213), calls=%async_computation.3 | async-start | bytes 4194304 | tf_op jit(solution)/shard_map/all_to_all | solution.py:296
  213.9 50.8 %shard_map.212 = bf16[256,512]{1,0:T(8,128)(2,1)} custom-call(bf16[256,512]{1,0:T(8,128)(2,1)} %fusion.15.qn_ref, bf16[128,512]{1,0:T(8,128)(2,1)} %bitcast.73, bf16[32,544,512]{2,1,0:T(8,128)(2,1)} %bitcast.76), custom_call_target="tpu_custom_call" | custom-call | flops 21474836480 | bytes 17825792 | tf_op jit(solution)/shard_map/pallas_call | solution.py:115
  264.7 3.0 convolution_convert_fusion.1
  267.7 4.8 %all-to-all-start = ((bf16[4,128,2048]{2,1,0:T(8,128)(2,1)}), bf16[4,128,2048]{2,1,0:T(8,128)(2,1)}, u32[]{:S(2)}, u32[]{:S(2)}) async-start(bf16[4,128,2048]{2,1,0:T(8,128)(2,1)} %bitcast.9), calls=%async_computation | async-start | bytes 4194304 | tf_op jit(solution)/shard_map/all_to_all | solution.py:157
  272.5 0.1 mul.290
  272.8 0.5 reshape.214
  273.3 1.4 gather_fusion
  274.7 2.3 reshape.215
  277.0 4.7 %multiply_reduce_fusion = f32[128,2048]{1,0:T(8,128)S(1)} fusion(f32[128,2,2048]{2,1,0:T(2,128)} %reshape.215, f32[128,2]{1,0:T(8,128)S(1)} %copy.63), kind=kLoop, calls=%fused_computation.14 | loop fusion | flops 786432 | bytes 3146752 | tf_op jit(solution)/shard_map/reduce_sum | solution.py:300
  281.8 0.2 multiply_reduce_fusion.1
  281.9 1.0 multiply_convert_fusion
  282.9 15.7 %all-to-all-done = bf16[4,128,2048]{2,1,0:T(8,128)(2,1)} async-done(((bf16[4,128,2048]{2,1,0:T(8,128)(2,1)}), bf16[4,128,2048]{2,1,0:T(8,128)(2,1)}, u32[]{:S(2)}, u32[]{:S(2)}) %all-to-all-start) | async-done | bytes 2097184 | tf_op jit(solution)/shard_map/all_to_all | solution.py:157
  298.6 2.2 convert_reduce_fusion
  300.8 0.2 multiply_reduce_fusion.2
  301.0 1.0 multiply_convert_fusion.1
  (74 shorter events, 1.1 us)
Async XLA Ops:
  7.2 117.7 %copy-start = (bf16[1,512,2048]{2,1,0:T(8,128)(2,1)S(1)}, bf16[1,512,2048]{2,1,0:T(8,128)(2,1)}, u32[]{:S(2)}) copy-start(bf16[1,512,2048]{2,1,0:T(8,128)(2,1)} %param.40) | copy-start | bytes 6291460
  7.2 3.8 %copy-start.2 = (bf16[128,2048]{1,0:T(8,128)(2,1)S(1)}, bf16[128,2048]{1,0:T(8,128)(2,1)}, u32[]{:S(2)}) copy-start(bf16[128,2048]{1,0:T(8,128)(2,1)} %param.21) | copy-start | bytes 1572868
  7.2 3.8 %copy-start.8 = (f32[2048]{0:T(1024)S(1)}, f32[2048]{0:T(1024)}, u32[]{:S(2)}) copy-start(f32[2048]{0:T(1024)} %param.23) | copy-start | bytes 24580
  7.2 65.8 %all-gather.5.cloned.1.call-start = ((), (), s32[]{:S(2)}) async-start(), calls=%async_computation.4 | async-start | bytes 2621440 | tf_op jit(solution)/shard_map/all_gather | solution.py:146
  11.0 4.0 %copy-start.11 = (f32[512]{0:T(512)S(1)}, f32[512]{0:T(512)}, u32[]{:S(2)}) copy-start(f32[512]{0:T(512)} %param.28) | copy-start | bytes 6148
  11.0 4.1 %copy-start.6 = (f32[1536]{0:T(1024)S(1)}, f32[1536]{0:T(1024)}, u32[]{:S(2)}) copy-start(f32[1536]{0:T(1024)} %param.27) | copy-start | bytes 18436
  15.0 1.2 copy-start.12
  15.0 2.9 copy-start.4
  15.1 2.9 copy-start.7
  16.1 101.1 %all-gather.7.cloned.1.call-start = ((), (), s32[]{:S(2)}) async-start(), calls=%async_computation.5 | async-start | bytes 6553600 | tf_op jit(solution)/shard_map/all_gather | solution.py:288
  59.2 3.8 %copy-start.3 = (bf16[128,2048]{1,0:T(8,128)(2,1)S(1)}, bf16[128,2048]{1,0:T(8,128)(2,1)}, u32[]{:S(2)}) copy-start(bf16[128,2048]{1,0:T(8,128)(2,1)} %param.21) | copy-start | bytes 1572868
  59.2 3.8 %copy-start.19 = (bf16[2048,32]{0,1:T(8,128)(2,1)S(1)}, bf16[2048,32]{0,1:T(8,128)(2,1)}, u32[]{:S(2)}) copy-start(bf16[2048,32]{0,1:T(8,128)(2,1)} %param.26) | copy-start | bytes 393220
  62.8 10.1 %copy-start.17 = (bf16[512,256]{1,0:T(8,128)(2,1)S(1)}, bf16[512,256]{1,0:T(8,128)(2,1)}, u32[]{:S(2)}) copy-start(bf16[512,256]{1,0:T(8,128)(2,1)} %param.31) | copy-start | bytes 786436
  62.8 11.6 %copy-start.18 = (bf16[512,256]{1,0:T(8,128)(2,1)S(1)}, bf16[512,256]{1,0:T(8,128)(2,1)}, u32[]{:S(2)}) copy-start(bf16[512,256]{1,0:T(8,128)(2,1)} %param.32) | copy-start | bytes 786436
  62.9 151.0 %all-gather.9.cloned.1.call-start = ((), (), s32[]{:S(2)}) async-start(), calls=%async_computation.6 | async-start | bytes 18382848 | tf_op jit(solution)/shard_map/all_gather | solution.py:253
  135.3 5.7 %copy-start.16 = (bf16[1536,128]{1,0:T(8,128)(2,1)S(1)}, bf16[1536,128]{1,0:T(8,128)(2,1)}, u32[]{:S(2)}) copy-start(bf16[1536,128]{1,0:T(8,128)(2,1)} %param.30) | copy-start | bytes 1179652
  135.3 64.6 %all-to-all-start.2 = ((bf16[4,320,2048]{2,1,0:T(8,128)(2,1)}), bf16[4,320,2048]{2,1,0:T(8,128)(2,1)}, u32[]{:S(2)}, u32[]{:S(2)}) async-start(bf16[4,320,2048]{2,1,0:T(8,128)(2,1)} %bitcast.71), calls=%async_computation.2 | async-start | bytes 10485760 | tf_op jit(solution)/shard_map/all_to_all | solution.py:157
  140.7 3.2 %copy-start.14 = (bf16[512,2048]{1,0:T(8,128)(2,1)S(1)}, bf16[512,2048]{1,0:T(8,128)(2,1)}, u32[]{:S(2)}) copy-start(bf16[512,2048]{1,0:T(8,128)(2,1)} %all-gather.5.cloned.1.call-done) | copy-start | bytes 6291460
  140.8 3.2 %copy-start.15 = (bf16[1536,256]{1,0:T(8,128)(2,1)S(1)}, bf16[1536,256]{1,0:T(8,128)(2,1)}, u32[]{:S(2)}) copy-start(bf16[1536,256]{1,0:T(8,128)(2,1)} %param.29) | copy-start | bytes 2359300
  205.1 62.6 %all-to-all-start.3 = ((bf16[32,10,2048]{2,1,0:T(8,128)(2,1)}), bf16[32,10,2048]{2,1,0:T(8,128)(2,1)S(1)}, u32[]{:S(2)}, u32[]{:S(2)}) async-start(bf16[32,10,2048]{2,1,0:T(8,128)(2,1)} %reshape.213), calls=%async_computation.3 | async-start | bytes 4194304 | tf_op jit(solution)/shard_map/all_to_all | solution.py:296
  213.8 50.8 %copy-start.5 = (bf16[256,2048]{1,0:T(8,128)(2,1)S(1)}, bf16[256,2048]{1,0:T(8,128)(2,1)}, u32[]{:S(2)}) copy-start(bf16[256,2048]{1,0:T(8,128)(2,1)} %param.33) | copy-start | bytes 3145732
  267.7 4.9 %copy-start.13 = (f32[128,2]{0,1:T(2,128)S(1)}, f32[128,2]{0,1:T(2,128)}, u32[]{:S(2)}) copy-start(f32[128,2]{0,1:T(2,128)} %param.37) | copy-start | bytes 3076
  267.7 30.8 %all-to-all-start = ((bf16[4,128,2048]{2,1,0:T(8,128)(2,1)}), bf16[4,128,2048]{2,1,0:T(8,128)(2,1)}, u32[]{:S(2)}, u32[]{:S(2)}) async-start(bf16[4,128,2048]{2,1,0:T(8,128)(2,1)} %bitcast.9), calls=%async_computation | async-start | bytes 4194304 | tf_op jit(solution)/shard_map/all_to_all | solution.py:157
  277.0 4.9 %copy-start.9 = (f32[2048]{0:T(1024)S(1)}, f32[2048]{0:T(1024)}, u32[]{:S(2)}) copy-start(f32[2048]{0:T(1024)} %param.41) | copy-start | bytes 24580
  282.9 18.1 %copy-start.10 = (f32[2048]{0:T(1024)S(1)}, f32[2048]{0:T(1024)}, u32[]{:S(2)}) copy-start(f32[2048]{0:T(1024)} %param.34) | copy-start | bytes 24580
  298.6 3.4 %copy-start.1 = (bf16[1,512,2048]{2,1,0:T(8,128)(2,1)S(1)}, bf16[1,512,2048]{2,1,0:T(8,128)(2,1)}, u32[]{:S(2)}) copy-start(bf16[1,512,2048]{2,1,0:T(8,128)(2,1)} %param.40) | copy-start | bytes 6291460
Sparse Core Ops, SparseCore 0:
  16.2 33.7 all-gather.4
  63.0 54.2 all-gather.6
  119.5 76.1 all-gather.8

commit v2 on v1

--- a/solution.py
+++ b/solution.py
@@ -21,8 +21,361 @@
 C = (NOPE + ROPE) ** (-0.5) * LOG2E
 SUB = 128
 
-def attend_kernel(heads, qn_ref, qt_ref, kv_ref, o_ref, rhs, s_buf, p_buf, peak, acc):
+MESH = pl.DeviceIdType.MESH
+ANY = pl.BlockSpec(memory_space=pl.ANY)
+VMEM = pl.BlockSpec(memory_space=pltpu.VMEM)
+DMA = pltpu.SemaphoreType.DMA
+
+
+def ring_places():
+    ep, tp, n = lax.axis_index("ep"), lax.axis_index("tp"), lax.axis_size("tp")
+    right = lax.rem(tp + 1, n)
+    left = lax.rem(tp + n - 1, n)
+    across = lax.rem(tp + 2, n)
+    return ep, tp, right, left, across
+
+
+def partner(ep, r):
+    for bit in range(r.bit_length()):
+        if r >> bit & 1:
+            ep = ep + (1 - 2 * lax.rem(ep // (1 << bit), 2)) * (1 << bit)
+    return ep
+
+
+def greet(places):
+    barrier = pltpu.get_barrier_semaphore()
+    for place in places:
+        pl.semaphore_signal(barrier, inc=1, device_id=place, device_id_type=MESH)
+    pl.semaphore_wait(barrier, len(places))
+
+
+def remote(src, dst, sends, recvs, k, place):
+    return pltpu.make_async_remote_copy(
+        src_ref=src,
+        dst_ref=dst,
+        send_sem=sends.at[k],
+        recv_sem=recvs.at[k],
+        device_id=place,
+        device_id_type=MESH,
+    )
+
+
+def exchange_kernel(latent_count, *refs):
+    lats, rows = refs[:latent_count], refs[latent_count]
+    outs, rows_out = refs[latent_count + 1 : 2 * latent_count + 1], refs[2 * latent_count + 1]
+    kept, kept_rows = refs[2 * latent_count + 2 : 3 * latent_count + 2], refs[3 * latent_count + 2]
+    own_sem, sends, recvs, row_sends, row_recvs = refs[3 * latent_count + 3 :]
+    ep, tp, right, left, across = ring_places()
+    peers = rows.shape[0]
+    swaps = [(partner(ep, r), tp) for r in range(1, peers)]
+    to_right, to_left = (ep, right), (ep, left)
+    greet(swaps + [to_right, to_left])
+    own = [
+        pltpu.make_async_copy(src, dst, own_sem.at[k])
+        for k, (src, dst) in enumerate(
+            [(a, b) for a, b in zip(lats, kept)] + [(rows.at[0], kept_rows)]
+        )
+    ]
+    first, second, waits = [], [], []
+    for k, (lat, out) in enumerate(zip(lats, outs)):
+        half = lat.shape[0] // 2
+        for part, place in ((0, to_right), (1, to_left), (1, to_right), (0, to_left)):
+            way = 0 if place is to_right else 1
+            at = pl.ds(part * half, half)
+            first.append(
+                remote(
+                    lat.at[at], out.at[tp, at], sends, recvs, 6 * k + 2 * way + part, place
+                )
+            )
+        for way, place, origin in ((0, to_right, left), (1, to_left, right)):
+            at = pl.ds(way * half, half)
+            second.append(
+                remote(
+                    out.at[origin, at], out.at[origin, at], sends, recvs, 6 * k + 4 + way, place
+                )
+            )
+    moves = [
+        remote(rows.at[r], rows_out.at[r], row_sends, row_recvs, r - 1, swaps[r - 1])
+        for r in range(1, peers)
+    ]
+    for copy in first:
+        copy.start()
+    for copy in moves:
+        copy.start()
+    for copy in own:
+        copy.start()
+    for copy in own:
+        copy.wait()
+    back = [
+        pltpu.make_async_copy(src, dst, own_sem.at[k])
+        for k, (src, dst) in enumerate(
+            [(a, b.at[tp]) for a, b in zip(kept, outs)] + [(kept_rows, rows_out.at[0])]
+        )
+    ]
+    for copy in back:
+        copy.start()
+    for k in range(latent_count):
+        first[4 * k].wait_recv()
+        second[2 * k].start()
+        first[4 * k + 1].wait_recv()
+        second[2 * k + 1].start()
+    for k in range(latent_count):
+        first[4 * k + 2].wait_recv()
+        first[4 * k + 3].wait_recv()
+    for copy in second:
+        copy.wait_recv()
+    for copy in moves:
+        copy.wait_recv()
+    for copy in first + second + moves:
+        copy.wait_send()
+    for copy in back:
+        copy.wait()
+
+
+def exchange(lats, rows):
+    groups = lax.axis_size("tp")
+    count = len(lats)
+    peers = rows.shape[0]
+    return pl.pallas_call(
+        functools.partial(exchange_kernel, count),
+        out_shape=[jax.ShapeDtypeStruct((groups, *a.shape), a.dtype) for a in lats]
+        + [jax.ShapeDtypeStruct(rows.shape, rows.dtype)],
+        in_specs=[ANY] * (count + 1),
+        out_specs=[ANY] * (count + 1),
+        scratch_shapes=[pltpu.VMEM(a.shape, a.dtype) for a in lats]
+        + [
+            pltpu.VMEM(rows.shape[1:], rows.dtype),
+            DMA((count + 1,)),
+            DMA((6 * count,)),
+            DMA((6 * count,)),
+            DMA((peers - 1,)),
+            DMA((peers - 1,)),
+        ],
+        compiler_params=pltpu.CompilerParams(
+            collective_id=1, has_side_effects=True, vmem_limit_bytes=8 * 1024 * 1024
+        ),
+        cost_estimate=pl.CostEstimate(flops=10**10, bytes_accessed=10**6, transcendentals=0),
+    )(*lats, rows)
+
+
+def gather_kernel(x, out, kept, own_sem, sends, recvs):
+    ep, tp, right, left, across = ring_places()
+    to_right, to_left = (ep, right), (ep, left)
+    greet([to_right, to_left])
+    size = x.shape[0] // 4
+
+    def chunk(c):
+        return pl.ds(c * size, size)
+
+    def fresh(c, way):
+        return remote(
+            x.at[chunk(c)], out.at[tp, chunk(c)], sends, recvs, 4 * way + c, (to_right, to_left)[way]
+        )
+
+    def onward(c):
+        way = c // 2
+        origin = (left, right)[way]
+        part = out.at[origin, chunk(c)]
+        return remote(part, part, sends, recvs, 8 + c, (to_right, to_left)[way])
+
+    news = {(c, way): fresh(c, way) for c in range(4) for way in range(2)}
+    passed = [onward(c) for c in range(4)]
+    for key in ((0, 0), (2, 1), (1, 0), (3, 1)):
+        news[key].start()
+    take = pltpu.make_async_copy(x, kept, own_sem.at[0])
+    take.start()
+    take.wait()
+    put = pltpu.make_async_copy(kept, out.at[tp], own_sem.at[0])
+    put.start()
+    for c in range(2):
+        news[c, 0].wait_recv()
+        passed[c].start()
+        news[2 + c, 0].start()
+        news[2 + c, 1].wait_recv()
+        passed[2 + c].start()
+        news[c, 1].start()
+    for c in range(2):
+        news[2 + c, 0].wait_recv()
+        news[c, 1].wait_recv()
+    for copy in passed:
+        copy.wait_recv()
+    for copy in passed + list(news.values()):
+        copy.wait_send()
+    put.wait()
+
+
+def gather_rows(x):
+    groups = lax.axis_size("tp")
+    return pl.pallas_call(
+        gather_kernel,
+        out_shape=jax.ShapeDtypeStruct((groups, *x.shape), x.dtype),
+        in_specs=[ANY],
+        out_specs=ANY,
+        scratch_shapes=[pltpu.VMEM(x.shape, x.dtype), DMA((1,)), DMA((12,)), DMA((12,))],
+        compiler_params=pltpu.CompilerParams(
+            collective_id=2, has_side_effects=True, vmem_limit_bytes=8 * 1024 * 1024
+        ),
+        cost_estimate=pl.CostEstimate(flops=10**10, bytes_accessed=10**6, transcendentals=0),
+    )(x)
+
+
+class Fold:
+    def __init__(self, part, far, near, mixed, sends, recvs):
+        self.part, self.far, self.near, self.mixed = part, far, near, mixed
+        ep, tp, right, left, across = ring_places()
+        self.tp, self.sides = tp, (right, left)
+        self.places = ((ep, right), (ep, left))
+        self.size = size = part.shape[1] // 4
+        self.at = [pl.ds(c * size, size) for c in range(4)]
+        self.hops = []
+        self.plain = []
+        self.joined = []
+        for c in range(4):
+            way = c // 2
+            other = 1 - way
+            self.hops.append(
+                remote(part.at[across, self.at[c]], far.at[c], sends, recvs, c, self.places[way])
+            )
+            self.plain.append(
+                remote(
+                    part.at[self.sides[other], self.at[c]],
+                    near.at[c],
+                    sends,
+                    recvs,
+                    4 + c,
+                    self.places[other],
+                )
+            )
+            self.joined.append(
+                remote(mixed.at[c], far.at[4 + c], sends, recvs, 8 + c, self.places[way])
+            )
+
+    def open(self):
+        greet(list(self.places))
+        for c in (0, 2, 1, 3):
+            self.hops[c].start()
+        for c in (2, 0, 3, 1):
+            self.plain[c].start()
+
+    def join(self, c):
+        own = self.part[self.sides[c // 2], self.at[c], :]
+        self.mixed[c] = (own.astype(jnp.float32) + self.far[c].astype(jnp.float32)).astype(
+            jnp.bfloat16
+        )
+
+    def total(self, c):
+        self.joined[c].wait_recv()
+        own = self.part[self.tp, self.at[c], :].astype(jnp.float32)
+        return own + self.near[c].astype(jnp.float32) + self.far[4 + c].astype(jnp.float32)
+
+    def close(self):
+        for copy in self.hops + self.plain + self.joined:
+            copy.wait_send()
+
+
+def fold_scratch(rows, width):
+    return [
+        pltpu.VMEM((8, rows // 4, width), jnp.bfloat16),
+        pltpu.VMEM((4, rows // 4, width), jnp.bfloat16),
+        pltpu.VMEM((4, rows // 4, width), jnp.bfloat16),
+        DMA((12,)),
+        DMA((12,)),
+    ]
+
+
+def finish_kernel(part, gain, rows, out, rows_out, kept, own_sem, far, near, mixed, sends, recvs, row_sends, row_recvs):
+    ep, tp, right, left, across = ring_places()
+    peers = rows.shape[0]
+    swaps = [(partner(ep, r), tp) for r in range(1, peers)]
+    barrier = pltpu.get_barrier_semaphore()
+    for place in swaps:
+        pl.semaphore_signal(barrier, inc=1, device_id=place, device_id_type=MESH)
+    fold = Fold(part, far, near, mixed, sends, recvs)
+    for place in fold.places:
+        pl.semaphore_signal(barrier, inc=1, device_id=place, device_id_type=MESH)
+    pl.semaphore_wait(barrier, len(swaps) + 2)
+    for c in (0, 2, 1, 3):
+        fold.hops[c].start()
+    for c in (2, 0, 3, 1):
+        fold.plain[c].start()
+    moves = [
+        remote(rows.at[r], rows_out.at[r], row_sends, row_recvs, r - 1, swaps[r - 1])
+        for r in range(1, peers)
+    ]
+    for copy in moves:
+        copy.start()
+    take = pltpu.make_async_copy(rows.at[0], kept, own_sem.at[0])
+    take.start()
+    take.wait()
+    put = pltpu.make_async_copy(kept, rows_out.at[0], own_sem.at[0])
+    put.start()
+    for c in (0, 2):
+        fold.hops[c].wait_recv()
+        fold.join(c)
+    for c in (1, 3):
+        fold.hops[c].wait_recv()
+    for c in (0, 2):
+        fold.joined[c].start()
+    for c in (1, 3):
+        fold.join(c)
+    for c in (0, 2):
+        fold.plain[c].wait_recv()
+    for c in (1, 3):
+        fold.joined[c].start()
+        fold.plain[c].wait_recv()
+    for c in range(4):
+        whole = fold.total(c)
+        scale = lax.rsqrt(jnp.mean(whole * whole, axis=-1, keepdims=True) + EPS)
+        out[fold.at[c], :] = (whole * scale * gain[...]).astype(jnp.bfloat16)
+    fold.close()
+    for copy in moves:
+        copy.wait()
+    put.wait()
+
+
+def finish(part, gain, rows):
+    groups, count, width = part.shape
+    peers = rows.shape[0]
+    return pl.pallas_call(
+        finish_kernel,
+        out_shape=[
+            jax.ShapeDtypeStruct((count, width), jnp.bfloat16),
+            jax.ShapeDtypeStruct(rows.shape, rows.dtype),
+        ],
+        in_specs=[VMEM, VMEM, ANY],
+        out_specs=[VMEM, ANY],
+        scratch_shapes=[pltpu.VMEM(rows.shape[1:], rows.dtype), DMA((1,))]
+        + fold_scratch(count, width)
+        + [DMA((peers - 1,)), DMA((peers - 1,))],
+        compiler_params=pltpu.CompilerParams(
+            collective_id=3, has_side_effects=True, vmem_limit_bytes=16 * 1024 * 1024
+        ),
+        cost_estimate=pl.CostEstimate(flops=10**10, bytes_accessed=10**6, transcendentals=0),
+    )(part, gain.reshape(1, width), rows)
+
+
+def attend_kernel(
+    heads, qn_ref, qt_ref, kv_ref, part, o_ref, sum_ref, rhs, s_buf, p_buf, peak, acc, *fold_refs
+):
     step = pl.program_id(0)
+    steps = pl.num_programs(0)
+    fold = Fold(part, *fold_refs)
+
+    @pl.when(step == 0)
+    def _():
+        fold.open()
+
+    @pl.when(step == steps * 5 // 16)
+    def _():
+        for c in range(4):
+            fold.hops[c].wait_recv()
+            fold.join(c)
+
+    @pl.when(step == steps * 5 // 16 + 1)
+    def _():
+        for c in (0, 2, 1, 3):
+            fold.joined[c].start()
+
     pair, size = kv_ref.shape[0], kv_ref.shape[2]
     subs = size // SUB
     wide = heads * NOPE
@@ -99,63 +452,60 @@
         finish(h, best)
         best = later
 
-    @pl.when(step == pl.num_programs(0) - 1)
+    @pl.when(step == steps - 1)
     def _():
+        for c in range(4):
+            fold.plain[c].wait_recv()
+            sum_ref[fold.at[c], :] = fold.total(c).astype(jnp.bfloat16)
+        fold.close()
         for h in range(heads):
             o_ref[h * VDIM : (h + 1) * VDIM, :] = (
                 acc[h, :VDIM, :] / acc[h, VDIM : VDIM + 1, :]
             ).astype(jnp.bfloat16)
 
 
-def attend(qn, qt, packed, pair=2):
+def attend(qn, qt, packed, part, pair=2):
     heads = qn.shape[0] // NOPE
     queries = qn.shape[1]
     blocks, height, size = packed.shape
     subs = size // SUB
     return pl.pallas_call(
         functools.partial(attend_kernel, heads),
-        out_shape=jax.ShapeDtypeStruct((heads * VDIM, queries), jnp.bfloat16),
+        out_shape=[
+            jax.ShapeDtypeStruct((heads * VDIM, queries), jnp.bfloat16),
+            jax.ShapeDtypeStruct(part.shape[1:], jnp.bfloat16),
+        ],
         grid=(blocks // pair,),
         in_specs=[
             pl.BlockSpec(qn.shape, lambda i: (0, 0)),
             pl.BlockSpec(qt.shape, lambda i: (0, 0)),
             pl.BlockSpec((pair, height, size), lambda i: (i, 0, 0)),
+            VMEM,
         ],
-        out_specs=pl.BlockSpec((heads * VDIM, queries), lambda i: (0, 0)),
+        out_specs=[
+            pl.BlockSpec((heads * VDIM, queries), lambda i: (0, 0)),
+            pl.BlockSpec(part.shape[1:], lambda i: (0, 0)),
+        ],
         scratch_shapes=[
             pltpu.VMEM((heads, subs, 256, queries), jnp.bfloat16),
             pltpu.VMEM((2, pair * size, queries), jnp.float32),
             pltpu.VMEM((2, pair * size, queries), jnp.bfloat16),
             pltpu.VMEM((8, queries), jnp.float32),
             pltpu.VMEM((heads, VDIM + 16, queries), jnp.float32),
-        ],
+        ]
+        + fold_scratch(part.shape[1], part.shape[2]),
         compiler_params=pltpu.CompilerParams(
-            dimension_semantics=("arbitrary",), vmem_limit_bytes=56 * 1024 * 1024
+            dimension_semantics=("arbitrary",),
+            vmem_limit_bytes=56 * 1024 * 1024,
+            collective_id=4,
+            has_side_effects=True,
         ),
         cost_estimate=pl.CostEstimate(
             flops=2 * heads * queries * blocks * size * (256 + VDIM),
             bytes_accessed=blocks * height * size * 2,
             transcendentals=heads * queries * blocks * size,
         ),
-    )(qn, qt, packed)
-
-
-def in_one_piece(arrays, axis, dim, along):
-    widths = [a.shape[along] for a in arrays]
-    both = jnp.concatenate(arrays, axis=along)
-    out = lax.all_gather(both, axis, axis=dim, tiled=True)
-    return tuple(jnp.split(out, [sum(widths[:k]) for k in range(1, len(widths))], axis=along))
-
-
-def split_up(shard, dim, peers):
-    before, after = (shard.shape[:dim], shard.shape[dim + 1 :])
-    return jnp.moveaxis(shard.reshape(*before, peers, -1, *after), dim, 0)
-
-
-def summed_on_arrival(shard, axis, dim):
-    blocks = split_up(shard, dim, lax.axis_size(axis))
-    arrived = lax.all_to_all(blocks, axis, split_axis=0, concat_axis=0, tiled=True)
-    return arrived.astype(jnp.float32).sum(axis=0)
+    )(qn, qt, packed, part)
 
 
 def norm_rows(values, gain):
@@ -219,10 +569,31 @@
     key_turn = rotate(
         jnp.dot(hidden, rotary_down, preferred_element_type=jnp.float32), cosine, sine
     ).astype(jnp.bfloat16)
-    collected = in_one_piece((query_lat, key_lat), "tp", 0, 1)
-    turned = lax.all_gather(key_turn, "tp", axis=1, tiled=True)
-    qlat, latents = collected
-    count = qlat.shape[0]
+    expert_hidden = norm_rows(expert_input, expert_norm).astype(jnp.bfloat16)
+    experts = lax.axis_size("ep")
+    topk = route_ids.shape[1]
+    capacity = 5 * tok_rows * topk // (4 * experts)
+    slots = experts * capacity
+    flat_ids = route_ids.reshape(-1)
+    onehot = (flat_ids[:, None] == jnp.arange(experts, dtype=jnp.int32)[None, :]).astype(jnp.int32)
+    order = jnp.sum((jnp.cumsum(onehot, axis=0) - onehot) * onehot, axis=1)
+    target = (flat_ids ^ lax.axis_index("ep")) * capacity + order
+    dispatch = jnp.any(
+        target.reshape(tok_rows, topk)[None, :, :]
+        == jnp.arange(slots, dtype=jnp.int32)[:, None, None],
+        axis=2,
+    ).astype(jnp.bfloat16)
+    outgoing = (
+        jnp.dot(dispatch, expert_hidden, preferred_element_type=jnp.float32)
+        .astype(jnp.bfloat16)
+        .reshape(experts, capacity, expert_hidden.shape[1] // 128, 128)
+    )
+    wide_turn = jnp.pad(key_turn, ((0, 0), (0, 128 - ROPE)))
+    latents, turned, qlat, received = exchange((key_lat, wide_turn, query_lat), outgoing)
+    count = groups * tok_rows
+    latents = latents.reshape(count, latents.shape[2])
+    qlat = qlat.reshape(count, qlat.shape[2])
+    turned = jnp.concatenate([turned[g, :, :ROPE] for g in range(groups)], axis=1)
     across = (((0,), (1,)), ((), ()))
     qn = lax.dot_general(query_plain, qlat, across, preferred_element_type=jnp.float32).astype(
         jnp.bfloat16
@@ -251,53 +622,27 @@
     )
     packed = jnp.concatenate([keys, values, turned], axis=0)
     packed = lax.all_gather(packed, "ep", axis=0, tiled=False)
-    attended = attend(qn, qt, packed)
-    mixed = summed_on_arrival(
-        lax.dot_general(
-            attended, output_proj, (((0,), (0,)), ((), ())), preferred_element_type=jnp.float32
-        ).astype(jnp.bfloat16),
-        "tp",
-        0,
-    )
-    mixer_out = norm_rows(mixed, mixed_gain).astype(jnp.bfloat16)
-    expert_hidden = norm_rows(expert_input, expert_norm).astype(jnp.bfloat16)
-    experts = lax.axis_size("ep")
-    topk = route_ids.shape[1]
-    capacity = 5 * tok_rows * topk // (4 * experts)
-    slots = experts * capacity
-    flat_ids = route_ids.reshape(-1)
-    onehot = (flat_ids[:, None] == jnp.arange(experts, dtype=jnp.int32)[None, :]).astype(jnp.int32)
-    order = jnp.sum((jnp.cumsum(onehot, axis=0) - onehot) * onehot, axis=1)
-    target = flat_ids * capacity + order
-    dispatch = jnp.any(
-        target.reshape(tok_rows, topk)[None, :, :]
-        == jnp.arange(slots, dtype=jnp.int32)[:, None, None],
-        axis=2,
-    ).astype(jnp.bfloat16)
-    outgoing = (
-        jnp.dot(dispatch, expert_hidden, preferred_element_type=jnp.float32)
-        .astype(jnp.bfloat16)
-        .reshape(experts, capacity, expert_hidden.shape[1])
-    )
     gate_w = gate_proj[0]
     up_w = up_proj[0]
     down_w = down_proj[0]
-    received = lax.all_to_all(outgoing, "ep", split_axis=0, concat_axis=0, tiled=True)
-    sources, count, width = received.shape
-    rows = received.reshape(sources * count, width)
-    piece = lax.all_gather(rows, "tp", axis=0, tiled=True)
+    width = expert_hidden.shape[1]
+    piece = gather_rows(received.reshape(slots, width)).reshape(groups * slots, width)
     gate = jnp.minimum(jnp.dot(piece, gate_w, preferred_element_type=jnp.float32), CLAMP)
     up = jnp.clip(jnp.dot(piece, up_w, preferred_element_type=jnp.float32), -CLAMP, CLAMP)
     acts = ((up + 1.0) * gate * jax.nn.sigmoid(ALPHA * gate)).astype(jnp.bfloat16)
-    sums = summed_on_arrival(
-        jnp.dot(acts, down_w, preferred_element_type=jnp.float32).astype(jnp.bfloat16), "tp", 0
-    )
-    returned = sums.astype(jnp.bfloat16).reshape(sources, count, width)
-    back_rows = lax.all_to_all(returned, "ep", split_axis=0, concat_axis=0, tiled=True).reshape(
-        slots, expert_hidden.shape[1]
-    )
-    picked = back_rows[target].astype(jnp.float32).reshape(tok_rows, topk, expert_hidden.shape[1])
-    combined = jnp.sum(picked * route_weight[:, :, None], axis=1)
+    part = jnp.dot(acts, down_w, preferred_element_type=jnp.float32).astype(jnp.bfloat16)
+    attended, sums = attend(qn, qt, packed, part.reshape(groups, slots, width))
+    mixed = lax.dot_general(
+        attended, output_proj, (((0,), (0,)), ((), ())), preferred_element_type=jnp.float32
+    ).astype(jnp.bfloat16)
+    mixer_out, back_rows = finish(
+        mixed.reshape(groups, tok_rows, width),
+        mixed_gain,
+        sums.reshape(experts, capacity, width // 128, 128),
+    )
+    back_rows = back_rows.reshape(slots, width // 128, 128)
+    picked = back_rows[target].astype(jnp.float32).reshape(tok_rows, topk, width // 128, 128)
+    combined = jnp.sum(picked * route_weight[:, :, None, None], axis=1).reshape(tok_rows, width)
     expert_out = norm_rows(combined, expert_gain).astype(jnp.bfloat16)
     return (mixer_out, expert_out)
 

time: 309 us -> 235 us (0.76)
  Pallas kernels: 50.8 us -> 161 us
  waiting for transfers between devices: 111 us -> 3.69 us
  blocking collectives: 47.4 us -> 0 us
  starting transfers between devices: 19 us -> 0.04 us
  other arithmetic: 17.4 us -> 9.74 us
  matrix products: 35.7 us -> 29.1 us
    pallas_call x1 -> x4, Pallas kernels: 50.8 us -> 161 us  [the longest x1 57.3 us: attend(): pl.pallas_call(functools.partial(attend_kernel, heads), out_shape=[jax.Sh...]
    all_to_all x3 -> x0, waiting for transfers between devices: 70.3 us -> none  [the longest x2 70.3 us: summed_on_arrival(): lax.all_to_all(blocks, axis, split_axis=0, concat_axis=0, tiled=True)]
    all_gather x2 -> x0, waiting for transfers between devices: 40.3 us -> none  [the longest x1 40.3 us: on_device(): piece = lax.all_gather(rows, 'tp', axis=0, tiled=True)]
    all_to_all x1 -> x0, blocking collectives: 38 us -> none  [on_device(): lax.all_to_all(outgoing, 'ep', split_axis=0, concat_axis=0, tiled=True)]
    all_to_all x3 -> x0, starting transfers between devices: 18.9 us -> none  [the longest x2 10.2 us: summed_on_arrival(): lax.all_to_all(blocks, axis, split_axis=0, concat_axis=0, tiled=True)]
    unnamed x42 -> x60, local copies, waits for them, and re-layouts: 0.33 us -> 10.8 us
    all_gather x1 -> x0, blocking collectives: 9.38 us -> none  [on_device(): turned = lax.all_gather(key_turn, 'tp', axis=1, tiled=True)]
    reduce_sum x3 -> x1, other arithmetic: 10.6 us -> 1.93 us  [on_device(): jnp.sum(picked * route_weight[:, :, None, None], axis=1)]
  transfers between devices with their start and end apart: 6 -> 1, of which waited for: 3 -> 1; matrix products, arithmetic and copies ran while one was open for 18% -> 9% of each run, Pallas kernels for 16% -> 20%
where the time goes in v2:
time: 235 us; the launch traced here: 234 us
  Pallas kernels  161 us (69%)
  matrix products  29.1 us (12%)
  local copies, waits for them, and re-layouts  15.8 us (7%)
  between operations  14.5 us (6%)
  other arithmetic  9.74 us (4%)
  waiting for transfers between devices  3.69 us (2%)
    pallas_call x1, Pallas kernels, attend(): pl.pallas_call(functools.partial(attend_kernel, heads), out_shape=[jax.Sh...  57.3 us
    pallas_call x1, Pallas kernels, gather_rows(): pl.pallas_call(gather_kernel, out_shape=jax.ShapeDtypeStruct((groups, *x....  45.8 us
    pallas_call x1, Pallas kernels, exchange(): pl.pallas_call(functools.partial(exchange_kernel, count), out_shape=[jax....  30.4 us
    pallas_call x1, Pallas kernels, finish(): pl.pallas_call(finish_kernel, out_shape=[jax.ShapeDtypeStruct((count, wid...  27.9 us
    unnamed x60, local copies, waits for them, and re-layouts  10.8 us
    dot_general x1, matrix products, on_device(): jnp.dot(acts, down_w, preferred_element_type=jnp.float32)  10.8 us
  transfers between devices with their start and end apart: 1, of which 1 were waited for; matrix products, arithmetic and copies ran while one was open for 9% of the time, Pallas kernels for 20%

profile of v2, /device:TPU:1, one launch (start us, length us, event | category | flops | bytes accessed | tf_op | source)
XLA Modules:
  0.0 234.4 jit_solution(6252097371677424185)
XLA Ops:
  7.3 0.9 copy.72
  8.2 0.1 eq.38
  8.4 0.1 eq.42
  8.5 1.2 fusion.11
  9.7 3.0 %multiply_reduce_fusion.2 = (f32[128]{0:T(128)S(1)}, f32[128,512]{1,0:T(8,128)}) fusion(bf16[2048,512]{1,0:T(8,128)(2,1)} %param.25, bf16[128,2048]{1,0:T(8,128)(2,1)} %param.21, f32[2048]{0:T(1024)} %param.23, f32[128]{0:T(128)S(1)} %add_rsqrt_fusion.4), kind=kOutput, calls=%fused_computation.44 | convolution fusion | flops 269614976 | bytes 2892800 | tf_op jit(solution)/shard_map/dot_general | solution.py:566
  12.8 0.3 fusion.43
  13.1 0.1 fusion.34
  13.3 0.1 copy.71
  13.4 3.9 %multiply_reduce_fusion.1 = (f32[128]{0:T(128)S(1)}, f32[128,1536]{1,0:T(8,128)S(1)}) fusion(bf16[2048,1536]{1,0:T(8,128)(2,1)} %param.24, bf16[128,2048]{1,0:T(8,128)(2,1)S(1)} %copy-done.11, f32[2048]{0:T(1024)S(1)} %copy-done.17, f32[128]{0:T(128)S(1)} %add_rsqrt_fusion.4), kind=kOutput, calls=%fused_computation.37 | convolution fusion | flops 806748032 | bytes 7611392 | tf_op jit(solution)/shard_map/dot_general | solution.py:563
  17.3 0.6 reduce-window.6
  17.9 0.2 slice_reduce_fusion
  18.3 0.1 reduce_sum.71
  18.5 1.2 fusion.14
  19.8 1.7 fusion.8
  21.5 0.3 copy.89
  21.9 0.1 multiply_convert_fusion.refs_2_
  22.1 30.4 %shard_map.212 = (bf16[4,128,512]{2,1,0:T(8,128)(2,1)S(1)}, bf16[4,128,128]{2,1,0:T(8,128)(2,1)S(1)}, bf16[4,128,1536]{2,1,0:T(8,128)(2,1)S(1)}, bf16[32,10,16,128]{3,2,1,0:T(8,128)(2,1)S(1)}) custom-call(bf16[128,512]{1,0:T(8,128)(2,1)S(1)} %multiply_convert_fusion.1.refs_0_, bf16[128,128]{1,0:T(8,128)(2,1)S(1)} %pad.4.refs_1_, ...), custom_call_target="tpu_custom_call" | custom-call | flops 10000000000 | bytes 1000000 | tf_op jit(solution)/shard_map/pallas_call | solution.py:139
  52.6 1.2 copy-done.2
  53.7 1.1 copy-done.4
  54.8 0.1 pad_maximum_fusion.2
  54.9 0.1 copy.80
  55.1 0.3 fusion.10
  55.4 0.3 convolution_convert_fusion.4
  55.8 0.9 pad_maximum_fusion
  56.7 2.1 copy.81
  58.8 1.4 copy.96
  60.2 0.1 copy.83
  60.3 0.1 copy.82
  60.4 0.1 mul.267
  60.6 0.2 multiply_cosine_fusion
  60.8 2.2 fusion.50
  63.1 0.7 pad_maximum_fusion.1
  63.8 1.3 fusion.9.qn_ref
  65.2 45.8 %shard_map.213 = bf16[4,320,2048]{2,1,0:T(8,128)(2,1)S(1)} custom-call(bf16[320,2048]{1,0:T(8,128)(2,1)S(1)} %bitcast.116), custom_call_target="tpu_custom_call" | custom-call | flops 10000000000 | bytes 1000000 | tf_op jit(solution)/shard_map/pallas_call | solution.py:209
  110.9 2.4 %copy-done.10 = bf16[4,320,2048]{2,1,0:T(8,128)(2,1)} copy-done((bf16[4,320,2048]{2,1,0:T(8,128)(2,1)}, bf16[4,320,2048]{2,1,0:T(8,128)(2,1)S(1)}, u32[]{:S(2)}) %copy-start.10) | copy-done | bytes 5242904
  113.3 4.5 %convolution_minimum_fusion = f32[1280,512]{1,0:T(8,128)} fusion(bf16[1280,2048]{1,0:T(8,128)(2,1)S(1)} %bitcast.121, bf16[1,2048,512]{2,1,0:T(8,128)(2,1)S(1)} %copy-done.24), kind=kOutput, calls=%fused_computation.3 | convolution fusion | flops 2685009920 | bytes 9961472 | tf_op jit(solution)/shard_map/dot_general | solution.py:630
  117.8 10.8 %convolution_convert_fusion = bf16[1280,2048]{1,0:T(8,128)(2,1)} fusion(bf16[1,512,2048]{2,1,0:T(8,128)(2,1)S(1)} %copy-done, f32[1280,512]{1,0:T(8,128)} %convolution_minimum_fusion, bf16[1280,2048]{1,0:T(8,128)(2,1)} %bitcast.122, bf16[1,2048,512]{2,1,0:T(8,128)(2,1)} %param.39), kind=kOutput, calls=%fused_computation.1 | convolution fusion | flops 5377228800 | bytes 17301504 | tf_op jit(solution)/shard_map/dot_general | solution.py:633
  128.6 3.7 %all-gather.3.cloned.1.call-done = bf16[17408,512]{1,0:T(8,128)(2,1)} async-done(((bf16[544,512]{1,0:T(8,128)(2,1)}), bf16[17408,512]{1,0:T(8,128)(2,1)}) %all-gather.3.cloned.1.call-update) | async-done | bytes 17825808 | tf_op jit(solution)/shard_map/all_gather | solution.py:624
  132.2 57.3 %shard_map.214 = (bf16[256,512]{1,0:T(8,128)(2,1)}, bf16[320,2048]{1,0:T(8,128)(2,1)}) custom-call(bf16[256,512]{1,0:T(8,128)(2,1)} %fusion.9.qn_ref, bf16[128,512]{1,0:T(8,128)(2,1)} %bitcast.126, bf16[32,544,512]{2,1,0:T(8,128)(2,1)} %bitcast.129, bf16[4,320,2048]{2,1,0:T(8,128)(2,1)} %bitcast.130), custom_call_target="tpu_custom_call" | custom-call | flops 21474836480 | bytes 17825792 | tf_op jit(solution)/shard_map/pallas_call | solution.py:472
  189.6 1.7 copy.91
  191.3 0.7 convolution_convert_fusion.1
  192.1 27.9 %shard_map.215 = (bf16[128,2048]{1,0:T(8,128)(2,1)S(1)}, bf16[32,10,16,128]{3,2,1,0:T(8,128)(2,1)S(1)}) custom-call(bf16[4,128,2048]{2,1,0:T(8,128)(2,1)S(1)} %bitcast.110, f32[1,2048]{1,0:T(1,128)S(1)} %bitcast.120, bf16[32,10,16,128]{3,2,1,0:T(8,128)(2,1)S(1)} %bitcast.118), custom_call_target="tpu_custom_call" | custom-call | flops 10000000000 | bytes 1000000 | tf_op jit(solution)/shard_map/pallas_call | solution.py:339
  220.0 0.8 copy-done.7
  220.8 1.7 gather_fusion
  222.6 1.9 fusion.4
  224.5 1.0 multiply_reduce_fusion
  225.5 1.2 fusion.18
  226.7 0.8 copy.98
  (77 shorter events, 0.7 us)
Async XLA Ops:
  7.2 110.7 %copy-start = (bf16[1,512,2048]{2,1,0:T(8,128)(2,1)S(1)}, bf16[1,512,2048]{2,1,0:T(8,128)(2,1)}, u32[]{:S(2)}) copy-start(bf16[1,512,2048]{2,1,0:T(8,128)(2,1)} %param.40) | copy-start | bytes 6291460
  7.2 5.6 %copy-start.11 = (bf16[128,2048]{1,0:T(8,128)(2,1)S(1)}, bf16[128,2048]{1,0:T(8,128)(2,1)}, u32[]{:S(2)}) copy-start(bf16[128,2048]{1,0:T(8,128)(2,1)} %param.21) | copy-start | bytes 1572868
  7.2 5.5 %copy-start.17 = (f32[2048]{0:T(1024)S(1)}, f32[2048]{0:T(1024)}, u32[]{:S(2)}) copy-start(f32[2048]{0:T(1024)} %param.23) | copy-start | bytes 24580
  7.2 5.5 %copy-start.26 = (bf16[2048,32]{0,1:T(8,128)(2,1)S(1)}, bf16[2048,32]{0,1:T(8,128)(2,1)}, u32[]{:S(2)}) copy-start(bf16[2048,32]{0,1:T(8,128)(2,1)} %param.26) | copy-start | bytes 393220
  7.2 125.0 %all-gather.3.cloned.1.call-start = ((), (), s32[]{:S(2)}) async-start(), calls=%async_computation | async-start | bytes 18382848 | tf_op jit(solution)/shard_map/all_gather | solution.py:624
  13.4 5.1 %copy-start.21 = (s32[128,2]{0,1:T(2,128)S(1)}, s32[128,2]{0,1:T(2,128)}, u32[]{:S(2)}) copy-start(s32[128,2]{0,1:T(2,128)} %param.36) | copy-start | bytes 3076
  13.4 6.4 %copy-start.18 = (f32[2048]{0:T(1024)S(1)}, f32[2048]{0:T(1024)}, u32[]{:S(2)}) copy-start(f32[2048]{0:T(1024)} %param.35) | copy-start | bytes 24580
  19.8 2.0 copy-start.14
  19.8 2.0 copy-start.22
  19.8 2.1 copy-start.19
  22.1 33.0 %copy-start.15 = (bf16[512,256]{1,0:T(8,128)(2,1)S(1)}, bf16[512,256]{1,0:T(8,128)(2,1)}, u32[]{:S(2)}) copy-start(bf16[512,256]{1,0:T(8,128)(2,1)} %param.32) | copy-start | bytes 786436
  22.1 33.3 %copy-start.16 = (bf16[512,256]{1,0:T(8,128)(2,1)S(1)}, bf16[512,256]{1,0:T(8,128)(2,1)}, u32[]{:S(2)}) copy-start(bf16[512,256]{1,0:T(8,128)(2,1)} %param.31) | copy-start | bytes 786436
  52.5 1.2 copy-start.2
  53.7 1.1 copy-start.4
  55.7 3.1 %copy-start.5 = (bf16[32,10,16,128]{3,2,1,0:T(8,128)(2,1)S(1)}, bf16[32,10,16,128]{3,2,1,0:T(8,128)(2,1)}, u32[]{:S(2)}) copy-start(bf16[32,10,16,128]{3,2,1,0:T(8,128)(2,1)} %copy-done.4) | copy-start | bytes 3932164
  56.7 3.6 %copy-start.23 = (f32[128,2]{0,1:T(2,128)S(1)}, f32[128,2]{0,1:T(2,128)}, u32[]{:S(2)}) copy-start(f32[128,2]{0,1:T(2,128)} %param.37) | copy-start | bytes 3076
  60.2 3.6 %copy-start.25 = (bf16[1536,256]{1,0:T(8,128)(2,1)S(1)}, bf16[1536,256]{1,0:T(8,128)(2,1)}, u32[]{:S(2)}) copy-start(bf16[1536,256]{1,0:T(8,128)(2,1)} %param.29) | copy-start | bytes 2359300
  60.6 3.2 %copy-start.3 = (bf16[4,128,1536]{2,1,0:T(8,128)(2,1)S(1)}, bf16[4,128,1536]{2,1,0:T(8,128)(2,1)}, u32[]{:S(2)}) copy-start(bf16[4,128,1536]{2,1,0:T(8,128)(2,1)} %copy-done.2) | copy-start | bytes 4718596
  63.1 2.1 copy-start.6
  65.2 48.2 %copy-start.24 = (bf16[1,2048,512]{2,1,0:T(8,128)(2,1)S(1)}, bf16[1,2048,512]{2,1,0:T(8,128)(2,1)}, u32[]{:S(2)}) copy-start(bf16[1,2048,512]{2,1,0:T(8,128)(2,1)} %param.38) | copy-start | bytes 6291460
  110.9 2.4 %copy-start.10 = (bf16[4,320,2048]{2,1,0:T(8,128)(2,1)}, bf16[4,320,2048]{2,1,0:T(8,128)(2,1)S(1)}, u32[]{:S(2)}) copy-start(bf16[4,320,2048]{2,1,0:T(8,128)(2,1)S(1)} %shard_map.213) | copy-start | bytes 15728644
  189.5 1.7 copy-start.12
  189.5 1.7 copy-start.13
  191.3 0.8 copy-start.9
  220.0 0.8 copy-start.7
  222.6 3.0 %copy-start.20 = (f32[2048]{0:T(1024)S(1)}, f32[2048]{0:T(1024)}, u32[]{:S(2)}) copy-start(f32[2048]{0:T(1024)} %param.41) | copy-start | bytes 24580
  222.6 4.2 %copy-start.8 = (bf16[128,2048]{1,0:T(8,128)(2,1)S(1)}, bf16[128,2048]{1,0:T(8,128)(2,1)}, u32[]{:S(2)}) copy-start(bf16[128,2048]{1,0:T(8,128)(2,1)} %copy-done.7) | copy-start | bytes 1572868
  222.6 5.0 %copy-start.1 = (bf16[1,512,2048]{2,1,0:T(8,128)(2,1)S(1)}, bf16[1,512,2048]{2,1,0:T(8,128)(2,1)}, u32[]{:S(2)}) copy-start(bf16[1,512,2048]{2,1,0:T(8,128)(2,1)} %param.40) | copy-start | bytes 6291460
Sparse Core Ops, SparseCore 0:
  58.9 73.2 all-gather.2

commit v3 on v2

--- a/solution.py
+++ b/solution.py
@@ -19,7 +19,7 @@
 FLOOR = -1e30
 LOG2E = 1.4426950408889634
 C = (NOPE + ROPE) ** (-0.5) * LOG2E
-SUB = 128
+SUB = 64
 
 MESH = pl.DeviceIdType.MESH
 ANY = pl.BlockSpec(memory_space=pl.ANY)
@@ -158,11 +158,160 @@
     )(*lats, rows)
 
 
-def gather_kernel(x, out, kept, own_sem, sends, recvs):
+class Spread:
+    def __init__(self, own, held, sends, recvs):
+        ep, tp = lax.axis_index("ep"), lax.axis_index("tp")
+        side = 4
+        core = lax.rem(ep, 2)
+        y = lax.rem(ep // 2, side)
+        z = ep // (2 * side)
+        self.own, self.held, self.sends, self.recvs = own, held, sends, recvs
+        self.ep, self.tp = ep, tp
+        self.mate = ep + 1 - 2 * core
+        cut = held.shape[2] // 32 * 16
+        self.parts = (pl.ds(0, cut), pl.ds(cut, held.shape[2] - cut))
+
+        def index(dz, dy):
+            return (lax.rem(z + dz, side) * side + lax.rem(y + dy, side)) * 2 + core
+
+        self.block = lambda f, a, b: index(b, a) if f == 0 else index(a, b)
+        self.neighbours = [index(1, 0), index(3, 0), index(0, 1), index(0, 3)]
+
+    def place(self, f, ring, way):
+        step = (1, 3)[way]
+        return (self.block(f, step, 0) if ring == 0 else self.block(f, 0, step), self.tp)
+
+    def copy(self, f, a, b, place, k, part=None):
+        mine = a == 0 and b == 0
+        where = self.block(f, a, b)
+        if part is None:
+            src = self.own.at[f] if mine else self.held.at[where, f]
+            dst = self.held.at[where, f]
+        else:
+            src = self.held.at[where, f, self.parts[part]]
+            dst = src
+        return remote(src, dst, self.sends, self.recvs, 36 * f + k, place)
+
+    def first(self, f, way):
+        return self.copy(f, 0, 0, self.place(f, 0, way), way)
+
+    def first_on(self, f, way):
+        return self.copy(f, (3, 1)[way], 0, self.place(f, 0, way), 2 + way, part=way)
+
+    def second(self, f, a, way):
+        return self.copy(f, a, 0, self.place(f, 1, way), 4 + 4 * a + way)
+
+    def second_on(self, f, a, way):
+        return self.copy(f, a, (3, 1)[way], self.place(f, 1, way), 6 + 4 * a + way, part=way)
+
+    def share(self, f, a, b):
+        return self.copy(f, a, b, (self.mate, self.tp), 20 + 4 * a + b)
+
+    def everyone(self):
+        return [(place, self.tp) for place in self.neighbours] + [(self.mate, self.tp)]
+
+    def start(self):
+        for f in range(2):
+            for way in range(2):
+                self.first(f, way).start()
+        for f in range(2):
+            self.share(f, 0, 0).start()
+            for way in range(2):
+                self.second(f, 0, way).start()
+
+    def got_first(self):
+        for f in range(2):
+            for way in range(2):
+                self.first(f, way).wait_recv()
+                self.first_on(f, way).start()
+                a = (3, 1)[way]
+                for there in range(2):
+                    self.second(f, a, there).start()
+                self.share(f, a, 0).start()
+
+    def got_second(self, a):
+        for f in range(2):
+            for way in range(2):
+                self.second(f, a, way).wait_recv()
+                self.second_on(f, a, way).start()
+                self.share(f, a, (3, 1)[way]).start()
+
+    def got_far_first(self):
+        for f in range(2):
+            for way in range(2):
+                self.first_on(f, way).wait_recv()
+            for there in range(2):
+                self.second(f, 2, there).start()
+            self.share(f, 2, 0).start()
+
+    def got_far_second(self, a):
+        for f in range(2):
+            for way in range(2):
+                self.second_on(f, a, way).wait_recv()
+            self.share(f, a, 2).start()
+
+    def close(self):
+        for f in range(2):
+            for a in range(4):
+                for b in range(4):
+                    self.share(f, a, b).wait()
+            for way in range(2):
+                self.first(f, way).wait_send()
+                self.first_on(f, way).wait_send()
+                for a in range(4):
+                    self.second(f, a, way).wait_send()
+                    self.second_on(f, a, way).wait_send()
+
+
+def gather_kernel(
+    x,
+    latents,
+    key_plain,
+    value_up,
+    turned,
+    qlat,
+    query_plain,
+    query_rotary,
+    cosine,
+    sine,
+    out,
+    held,
+    qn,
+    qt,
+    kept,
+    block,
+    own_sem,
+    sends,
+    recvs,
+    kv_sends,
+    kv_recvs,
+):
     ep, tp, right, left, across = ring_places()
     to_right, to_left = (ep, right), (ep, left)
-    greet([to_right, to_left])
     size = x.shape[0] // 4
+    spread = Spread(block, held, kv_sends, kv_recvs)
+    barrier = pltpu.get_barrier_semaphore()
+    places = [to_right, to_left] + spread.everyone()
+    for place in places:
+        pl.semaphore_signal(barrier, inc=1, device_id=place, device_id_type=MESH)
+    take = pltpu.make_async_copy(x, kept, own_sem.at[0])
+    take.start()
+
+    keys = jnp.dot(latents[...], key_plain[...], preferred_element_type=jnp.float32)
+    values = jnp.dot(latents[...], value_up[...], preferred_element_type=jnp.float32).T
+    keys, values = keys.astype(jnp.bfloat16), values.astype(jnp.bfloat16)
+    low = keys.shape[1]
+    half = low // 2
+    for f in range(2):
+        block[f, :half, :low] = keys[low * f : low * f + half]
+        block[f, :half, low:] = keys[low * f + half : low * f + low]
+        block[f, half:low, :low] = values[:half, low * f : low * f + low]
+        block[f, half:low, low:] = values[half:, low * f : low * f + low]
+        block[f, low:, :] = turned[f]
+    take.wait()
+    put = pltpu.make_async_copy(kept, out.at[tp], own_sem.at[0])
+    put.start()
+    pl.semaphore_wait(barrier, len(places))
 
     def chunk(c):
         return pl.ds(c * size, size)
@@ -182,18 +331,44 @@
     passed = [onward(c) for c in range(4)]
     for key in ((0, 0), (2, 1), (1, 0), (3, 1)):
         news[key].start()
-    take = pltpu.make_async_copy(x, kept, own_sem.at[0])
-    take.start()
-    take.wait()
-    put = pltpu.make_async_copy(kept, out.at[tp], own_sem.at[0])
-    put.start()
-    for c in range(2):
+    spread.start()
+    keep = pltpu.make_async_copy(block, held.at[ep], own_sem.at[1])
+    keep.start()
+
+    plain = jnp.dot(qlat[...], query_plain[...], preferred_element_type=jnp.float32)
+    qn[...] = plain.T.astype(jnp.bfloat16)
+    rotated = jnp.dot(qlat[...], query_rotary[...], preferred_element_type=jnp.float32).T
+    quarter = ROPE // 2
+    for h in range(rotated.shape[0] // ROPE):
+        a = rotated[h * ROPE : h * ROPE + quarter]
+        b = rotated[h * ROPE + quarter : h * ROPE + ROPE]
+        qt[h * ROPE : h * ROPE + quarter, :] = (a * cosine[...] - b * sine[...]).astype(
+            jnp.bfloat16
+        )
+        qt[h * ROPE + quarter : h * ROPE + ROPE, :] = (b * cosine[...] + a * sine[...]).astype(
+            jnp.bfloat16
+        )
+
+    def pass_rows(c):
         news[c, 0].wait_recv()
         passed[c].start()
         news[2 + c, 0].start()
         news[2 + c, 1].wait_recv()
         passed[2 + c].start()
         news[c, 1].start()
+
+    spread.got_first()
+    pass_rows(0)
+    spread.got_second(0)
+    pass_rows(1)
+    spread.got_far_first()
+    spread.got_second(3)
+    spread.got_second(1)
+    spread.got_far_second(0)
+    spread.got_second(2)
+    for a in (3, 1, 2):
+        spread.got_far_second(a)
+    spread.close()
     for c in range(2):
         news[2 + c, 0].wait_recv()
         news[c, 1].wait_recv()
@@ -202,21 +377,39 @@
     for copy in passed + list(news.values()):
         copy.wait_send()
     put.wait()
-
-
-def gather_rows(x):
-    groups = lax.axis_size("tp")
+    keep.wait()
+
+
+def gather(x, latents, key_plain, value_up, turned, qlat, query_plain, query_rotary, cosine, sine):
+    groups, peers = lax.axis_size("tp"), lax.axis_size("ep")
+    count = latents.shape[0]
+    low = key_plain.shape[1]
+    height = low + turned.shape[1]
+    wide = turned.shape[2]
     return pl.pallas_call(
         gather_kernel,
-        out_shape=jax.ShapeDtypeStruct((groups, *x.shape), x.dtype),
-        in_specs=[ANY],
-        out_specs=ANY,
-        scratch_shapes=[pltpu.VMEM(x.shape, x.dtype), DMA((1,)), DMA((12,)), DMA((12,))],
+        out_shape=[
+            jax.ShapeDtypeStruct((groups, *x.shape), x.dtype),
+            jax.ShapeDtypeStruct((peers, 2, height, wide), x.dtype),
+            jax.ShapeDtypeStruct((query_plain.shape[1], count), x.dtype),
+            jax.ShapeDtypeStruct((query_rotary.shape[1], count), x.dtype),
+        ],
+        in_specs=[ANY] + [VMEM] * 9,
+        out_specs=[ANY, ANY, VMEM, VMEM],
+        scratch_shapes=[
+            pltpu.VMEM(x.shape, x.dtype),
+            pltpu.VMEM((2, height, wide), x.dtype),
+            DMA((2,)),
+            DMA((12,)),
+            DMA((12,)),
+            DMA((72,)),
+            DMA((72,)),
+        ],
         compiler_params=pltpu.CompilerParams(
-            collective_id=2, has_side_effects=True, vmem_limit_bytes=8 * 1024 * 1024
+            collective_id=2, has_side_effects=True, vmem_limit_bytes=32 * 1024 * 1024
         ),
         cost_estimate=pl.CostEstimate(flops=10**10, bytes_accessed=10**6, transcendentals=0),
-    )(x)
+    )(x, latents, key_plain, value_up, turned, qlat, query_plain, query_rotary, cosine, sine)
 
 
 class Fold:
@@ -376,9 +569,9 @@
         for c in (0, 2, 1, 3):
             fold.joined[c].start()
 
-    pair, size = kv_ref.shape[0], kv_ref.shape[2]
+    pair, wide = kv_ref.shape[0], kv_ref.shape[2]
+    size = wide // 2
     subs = size // SUB
-    wide = heads * NOPE
     rows = pair * SUB
     queries = qn_ref.shape[1]
 
@@ -395,32 +588,25 @@
         acc[...] = jnp.zeros_like(acc)
 
     turned = jnp.concatenate(
-        [
-            kv_ref[b, 2 * wide :, g * 128 : (g + 1) * 128]
-            for b in range(pair)
-            for g in range(size // 128)
-        ],
+        [kv_ref[b, size:, g * 128 : (g + 1) * 128] for b in range(pair) for g in range(wide // 128)],
         axis=0,
     )
 
     def scores(h):
-        half = wide // SUB
+        half = size // 2
         best = None
         for j in range(subs):
+            at = j * SUB % half
+            lanes = j * SUB // half * size + h // 2 * 128
             left = jnp.concatenate(
-                [
-                    kv_ref[
-                        b,
-                        j % half * SUB : (j % half + 1) * SUB,
-                        j // half * wide + h // 2 * 128 : j // half * wide + h // 2 * 128 + 128,
-                    ]
-                    for b in range(pair)
-                ],
-                axis=0,
+                [kv_ref[b, at : at + SUB, lanes : lanes + 128] for b in range(pair)], axis=0
             )
             left = jnp.concatenate([left, turned], axis=1)
             part = jnp.dot(left, rhs[h, j], preferred_element_type=jnp.float32)
-            s_buf[h % 2, j * rows : (j + 1) * rows, :] = part
+            for b in range(pair):
+                s_buf[h % 2, b * size + j * SUB : b * size + (j + 1) * SUB, :] = part[
+                    b * SUB : (b + 1) * SUB
+                ]
             top = jnp.max(part.reshape(rows // 8, 8, queries), axis=0)
             best = top if best is None else jnp.maximum(best, top)
         return jnp.max(best, axis=0, keepdims=True)
@@ -431,13 +617,15 @@
         peak[h : h + 1, :] = new
         shrink = jnp.exp2((old - new) * C)
         base = new * C
-        for j in range(subs):
-            at = slice(j * rows, (j + 1) * rows)
+        for b in range(pair):
+            at = slice(b * size, (b + 1) * size)
             p_buf[h % 2, at, :] = jnp.exp2(s_buf[h % 2, at, :] * C - base).astype(jnp.bfloat16)
+        half = size // 2
+        at = h * VDIM % half
+        lanes = h * VDIM // half * size
         left = jnp.concatenate(
             [
-                kv_ref[b, wide + h * VDIM : wide + (h + 1) * VDIM, j * SUB : (j + 1) * SUB]
-                for j in range(subs)
+                kv_ref[b, half + at : half + at + VDIM, lanes : lanes + size]
                 for b in range(pair)
             ],
             axis=1,
@@ -464,10 +652,11 @@
             ).astype(jnp.bfloat16)
 
 
-def attend(qn, qt, packed, part, pair=2):
+def attend(qn, qt, packed, part, pair=4):
     heads = qn.shape[0] // NOPE
     queries = qn.shape[1]
-    blocks, height, size = packed.shape
+    blocks, height, wide = packed.shape
+    size = wide // 2
     subs = size // SUB
     return pl.pallas_call(
         functools.partial(attend_kernel, heads),
@@ -479,7 +668,7 @@
         in_specs=[
             pl.BlockSpec(qn.shape, lambda i: (0, 0)),
             pl.BlockSpec(qt.shape, lambda i: (0, 0)),
-            pl.BlockSpec((pair, height, size), lambda i: (i, 0, 0)),
+            pl.BlockSpec((pair, height, wide), lambda i: (i, 0, 0)),
             VMEM,
         ],
         out_specs=[
@@ -502,7 +691,7 @@
         ),
         cost_estimate=pl.CostEstimate(
             flops=2 * heads * queries * blocks * size * (256 + VDIM),
-            bytes_accessed=blocks * height * size * 2,
+            bytes_accessed=blocks * height * wide * 2,
             transcendentals=heads * queries * blocks * size,
         ),
     )(qn, qt, packed, part)
@@ -557,7 +746,6 @@
     groups = lax.axis_size("tp")
     group_base = lax.axis_index("ep") * groups * tok_rows
     offset = group_base + lax.axis_index("tp") * tok_rows
-    heads_here = query_plain.shape[1] // NOPE
     hidden = norm_rows(mixer_input, mixer_gain).astype(jnp.bfloat16)
     query_lat = norm_rows(
         jnp.dot(hidden, query_down, preferred_element_type=jnp.float32), query_gain
@@ -593,40 +781,27 @@
     count = groups * tok_rows
     latents = latents.reshape(count, latents.shape[2])
     qlat = qlat.reshape(count, qlat.shape[2])
-    turned = jnp.concatenate([turned[g, :, :ROPE] for g in range(groups)], axis=1)
-    across = (((0,), (1,)), ((), ()))
-    qn = lax.dot_general(query_plain, qlat, across, preferred_element_type=jnp.float32).astype(
-        jnp.bfloat16
+    turned = turned[:, :, :ROPE].reshape(2, 4, 4, 16, ROPE).transpose(0, 3, 2, 1, 4)
+    turned = turned.reshape(2, 16, 4 * 4 * ROPE)
+    all_cos, all_sin = turn_tables(group_base + jnp.arange(count, dtype=jnp.int32), ROPE)
+    width = expert_hidden.shape[1]
+    piece, packed, qn, qt = gather(
+        received.reshape(slots, width),
+        latents,
+        key_plain,
+        value_up,
+        turned,
+        qlat,
+        query_plain,
+        query_rotary,
+        all_cos.T,
+        all_sin.T,
     )
-    rotated = lax.dot_general(query_rotary, qlat, across, preferred_element_type=jnp.float32)
-    rotated = rotated.reshape(heads_here, 2, ROPE // 2, count)
-    all_cos, all_sin = turn_tables(group_base + jnp.arange(count, dtype=jnp.int32), ROPE)
-    all_cos, all_sin = all_cos.T[None], all_sin.T[None]
-    first, second = rotated[:, 0], rotated[:, 1]
-    qt = (
-        jnp.concatenate(
-            [first * all_cos - second * all_sin, second * all_cos + first * all_sin], axis=1
-        )
-        .astype(jnp.bfloat16)
-        .reshape(heads_here * ROPE, count)
-    )
-    keys = jnp.dot(latents, key_plain, preferred_element_type=jnp.float32).astype(jnp.bfloat16)
-    values = lax.dot_general(value_up, latents, across, preferred_element_type=jnp.float32).astype(
-        jnp.bfloat16
-    )
-    half = heads_here * NOPE
-    keys = jnp.concatenate([keys[g * half : (g + 1) * half] for g in range(count // half)], axis=1)
-    strips = tok_rows * turned.shape[1] // count
-    turned = jnp.concatenate(
-        [turned[g * strips : (g + 1) * strips] for g in range(tok_rows // strips)], axis=1
-    )
-    packed = jnp.concatenate([keys, values, turned], axis=0)
-    packed = lax.all_gather(packed, "ep", axis=0, tiled=False)
+    piece = piece.reshape(groups * slots, width)
+    packed = packed.reshape(-1, *packed.shape[2:])
     gate_w = gate_proj[0]
     up_w = up_proj[0]
     down_w = down_proj[0]
-    width = expert_hidden.shape[1]
-    piece = gather_rows(received.reshape(slots, width)).reshape(groups * slots, width)
     gate = jnp.minimum(jnp.dot(piece, gate_w, preferred_element_type=jnp.float32), CLAMP)
     up = jnp.clip(jnp.dot(piece, up_w, preferred_element_type=jnp.float32), -CLAMP, CLAMP)
     acts = ((up + 1.0) * gate * jax.nn.sigmoid(ALPHA * gate)).astype(jnp.bfloat16)

time: 235 us -> 220 us (0.936)
  between operations: 14.5 us -> 1.08 us
  Pallas kernels: 161 us -> 168 us
  matrix products: 29.1 us -> 23.9 us
  local copies, waits for them, and re-layouts: 15.8 us -> 19.6 us
  waiting for transfers between devices: 3.69 us -> 0 us
  other arithmetic: 9.74 us -> 7.03 us
    pallas_call x1, Pallas kernels: 45.8 us -> 53.5 us  [gather(): pl.pallas_call(gather_kernel, out_shape=[jax.ShapeDtypeStruct((groups, *x...]
    unnamed x60 -> x64, local copies, waits for them, and re-layouts: 10.8 us -> 15 us
    dot_general x4 -> x0, matrix products: 4.21 us -> none  [the longest x1 2.25 us: on_device(): lax.dot_general(query_rotary, qlat, across, preferred_element_type=jnp.fl...]
    all_gather x1 -> x0, waiting for transfers between devices: 3.68 us -> none  [on_device(): packed = lax.all_gather(packed, 'ep', axis=0, tiled=False)]
  transfers between devices with their start and end apart: 1 -> 0, of which waited for: 1 -> 0; matrix products, arithmetic and copies ran while one was open for 9% -> 0% of each run, Pallas kernels for 20% -> 0%
where the time goes in v3:
time: 220 us
  Pallas kernels  168 us (76%)
  matrix products  23.9 us (11%)
  local copies, waits for them, and re-layouts  19.6 us (9%)
  other arithmetic  7.03 us (3%)
    pallas_call x1, Pallas kernels, attend(): pl.pallas_call(functools.partial(attend_kernel, heads), out_shape=[jax.Sh...  56.5 us
    pallas_call x1, Pallas kernels, gather(): pl.pallas_call(gather_kernel, out_shape=[jax.ShapeDtypeStruct((groups, *x...  53.5 us
    pallas_call x1, Pallas kernels, exchange(): pl.pallas_call(functools.partial(exchange_kernel, count), out_shape=[jax....  30.4 us
    pallas_call x1, Pallas kernels, finish(): pl.pallas_call(finish_kernel, out_shape=[jax.ShapeDtypeStruct((count, wid...  27.7 us
    unnamed x64, local copies, waits for them, and re-layouts  15 us
    dot_general x1, matrix products, on_device(): jnp.dot(acts, down_w, preferred_element_type=jnp.float32)  10.4 us
    dot_general x1, matrix products, on_device(): jnp.dot(piece, gate_w, preferred_element_type=jnp.float32)  4.48 us

profile of v3, /device:TPU:1, one launch (start us, length us, event | category | flops | bytes accessed | tf_op | source)
XLA Modules:
  0.0 219.8 jit_solution(12651996078123161628)
XLA Ops:
  0.7 1.4 fusion.9
  2.1 2.4 %multiply_reduce_fusion.2 = (f32[128]{0:T(128)S(1)}, f32[128,512]{1,0:T(8,128)S(1)}) fusion(bf16[2048,512]{1,0:T(8,128)(2,1)} %param.25, bf16[128,2048]{1,0:T(8,128)(2,1)} %param.21, f32[2048]{0:T(1024)} %param.23, f32[128]{0:T(128)S(1)} %add_rsqrt_fusion.4), kind=kOutput, calls=%fused_computation.38 | convolution fusion | flops 269614976 | bytes 2892800 | tf_op jit(solution)/shard_map/dot_general | solution.py:754
  4.6 0.3 fusion.41
  5.0 0.1 fusion.32
  5.1 0.1 copy.51
  5.3 4.0 %multiply_reduce_fusion.1 = (f32[128]{0:T(128)S(1)}, f32[128,1536]{1,0:T(8,128)S(1)}) fusion(bf16[2048,1536]{1,0:T(8,128)(2,1)} %param.24, bf16[128,2048]{1,0:T(8,128)(2,1)S(1)} %copy-done.16, f32[2048]{0:T(1024)S(1)} %copy-done.20, f32[128]{0:T(128)S(1)} %add_rsqrt_fusion.4), kind=kOutput, calls=%fused_computation.32 | convolution fusion | flops 806748032 | bytes 7611392 | tf_op jit(solution)/shard_map/dot_general | solution.py:751
  9.3 0.1 multiply_convert_fusion.refs_2_
  9.4 0.1 copy.52
  9.5 0.1 eq.38
  9.7 0.1 eq.42
  9.8 0.6 reduce-window.6
  10.4 0.2 slice_reduce_fusion
  10.8 0.1 reduce_sum.71
  11.1 0.2 fusion.12
  11.3 0.6 fusion.8
  11.8 0.3 copy.60
  12.1 30.4 %shard_map.212 = (bf16[4,128,512]{2,1,0:T(8,128)(2,1)S(1)}, bf16[4,128,128]{2,1,0:T(8,128)(2,1)S(1)}, bf16[4,128,1536]{2,1,0:T(8,128)(2,1)S(1)}, bf16[32,10,16,128]{3,2,1,0:T(8,128)(2,1)S(1)}) custom-call(bf16[128,512]{1,0:T(8,128)(2,1)S(1)} %multiply_convert_fusion.1.refs_0_, bf16[128,128]{1,0:T(8,128)(2,1)S(1)} %pad.4.refs_1_, ...), custom_call_target="tpu_custom_call" | custom-call | flops 10000000000 | bytes 1000000 | tf_op jit(solution)/shard_map/pallas_call | solution.py:139
  42.6 1.1 copy-done.10
  43.8 0.8 copy-done.12
  44.5 0.3 copy.68
  44.9 0.8 copy.69
  45.7 1.1 reshape.174.turned
  46.7 0.2 multiply_sine_fusion
  46.9 1.1 copy-done.4
  48.1 1.0 copy-done.5
  49.1 0.9 copy-done.6
  50.0 0.9 copy-done.7
  51.0 1.4 copy-done.11
  52.4 1.0 copy-done.13
  53.4 53.5 %shard_map.213 = (bf16[4,320,2048]{2,1,0:T(8,128)(2,1)S(1)}, bf16[32,2,272,512]{3,2,1,0:T(8,128)(2,1)}, bf16[256,512]{1,0:T(8,128)(2,1)S(1)}, bf16[128,512]{1,0:T(8,128)(2,1)S(1)}) custom-call(bf16[320,2048]{1,0:T(8,128)(2,1)S(1)} %bitcast.76, bf16[512,512]{1,0:T(8,128)(2,1)S(1)} %bitcast.86, bf16[512,256]{1,0:T(8,128)(2,1)S(1)} %copy-done.6, ...), custom_call_target="tpu_custom_call" | custom-call | flops 10000000000 | bytes 1000000 | tf_op jit(solution)/shard_map/pallas_call | solution.py:389
  107.0 0.7 copy-done.14
  107.7 0.7 copy-done.15
  108.3 2.4 %copy-done.9 = bf16[4,320,2048]{2,1,0:T(8,128)(2,1)} copy-done((bf16[4,320,2048]{2,1,0:T(8,128)(2,1)}, bf16[4,320,2048]{2,1,0:T(8,128)(2,1)S(1)}, u32[]{:S(2)}) %copy-start.9) | copy-done | bytes 5242904
  110.7 4.5 %convolution_minimum_fusion = f32[1280,512]{1,0:T(8,128)} fusion(bf16[1280,2048]{1,0:T(8,128)(2,1)S(1)} %bitcast.83, bf16[1,2048,512]{2,1,0:T(8,128)(2,1)S(1)} %copy-done.27), kind=kOutput, calls=%fused_computation.3 | convolution fusion | flops 2685009920 | bytes 9961472 | tf_op jit(solution)/shard_map/dot_general | solution.py:805
  115.2 10.4 %convolution_convert_fusion = bf16[1280,2048]{1,0:T(8,128)(2,1)} fusion(bf16[1,512,2048]{2,1,0:T(8,128)(2,1)S(1)} %copy-done, f32[1280,512]{1,0:T(8,128)} %convolution_minimum_fusion, bf16[1280,2048]{1,0:T(8,128)(2,1)} %bitcast.84, bf16[1,2048,512]{2,1,0:T(8,128)(2,1)} %param.39), kind=kOutput, calls=%fused_computation.1 | convolution fusion | flops 5377228800 | bytes 17301504 | tf_op jit(solution)/shard_map/dot_general | solution.py:808
  125.6 56.5 %shard_map.214 = (bf16[256,512]{1,0:T(8,128)(2,1)}, bf16[320,2048]{1,0:T(8,128)(2,1)}) custom-call(bf16[256,512]{1,0:T(8,128)(2,1)} %copy-done.14, bf16[128,512]{1,0:T(8,128)(2,1)} %copy-done.15, bf16[64,272,512]{2,1,0:T(8,128)(2,1)} %bitcast.92, bf16[4,320,2048]{2,1,0:T(8,128)(2,1)} %bitcast.93), custom_call_target="tpu_custom_call" | custom-call | flops 21474836480 | bytes 17825792 | tf_op jit(solution)/shard_map/pallas_call | solution.py:661
  182.1 1.8 convolution_convert_fusion.1
  183.9 0.3 copy.62
  184.2 27.7 %shard_map.215 = (bf16[128,2048]{1,0:T(8,128)(2,1)S(1)}, bf16[32,10,16,128]{3,2,1,0:T(8,128)(2,1)S(1)}) custom-call(bf16[4,128,2048]{2,1,0:T(8,128)(2,1)S(1)} %bitcast.75, f32[1,2048]{1,0:T(1,128)S(1)} %bitcast.82, bf16[32,10,16,128]{3,2,1,0:T(8,128)(2,1)S(1)} %bitcast.79), custom_call_target="tpu_custom_call" | custom-call | flops 10000000000 | bytes 1000000 | tf_op jit(solution)/shard_map/pallas_call | solution.py:532
  211.9 0.8 copy-done.2
  212.7 0.1 copy.58
  212.8 0.1 copy.57
  213.0 0.1 mul.226
  213.1 1.8 gather_fusion
  214.9 1.8 fusion.4
  216.7 1.0 multiply_reduce_fusion
  217.8 1.2 fusion.16
  219.0 0.8 copy.71
  (66 shorter events, 0.6 us)
Async XLA Ops:
  0.6 114.6 %copy-start = (bf16[1,512,2048]{2,1,0:T(8,128)(2,1)S(1)}, bf16[1,512,2048]{2,1,0:T(8,128)(2,1)}, u32[]{:S(2)}) copy-start(bf16[1,512,2048]{2,1,0:T(8,128)(2,1)} %param.40) | copy-start | bytes 6291460
  0.6 3.9 %copy-start.16 = (bf16[128,2048]{1,0:T(8,128)(2,1)S(1)}, bf16[128,2048]{1,0:T(8,128)(2,1)}, u32[]{:S(2)}) copy-start(bf16[128,2048]{1,0:T(8,128)(2,1)} %param.21) | copy-start | bytes 1572868
  0.7 3.9 %copy-start.20 = (f32[2048]{0:T(1024)S(1)}, f32[2048]{0:T(1024)}, u32[]{:S(2)}) copy-start(f32[2048]{0:T(1024)} %param.23) | copy-start | bytes 24580
  0.7 3.8 %copy-start.25 = (f32[512]{0:T(512)S(1)}, f32[512]{0:T(512)}, u32[]{:S(2)}) copy-start(f32[512]{0:T(512)} %param.28) | copy-start | bytes 6148
  0.7 3.9 %copy-start.28 = (bf16[2048,32]{0,1:T(8,128)(2,1)S(1)}, bf16[2048,32]{0,1:T(8,128)(2,1)}, u32[]{:S(2)}) copy-start(bf16[2048,32]{0,1:T(8,128)(2,1)} %param.26) | copy-start | bytes 393220
  5.3 4.0 %copy-start.21 = (f32[1536]{0:T(1024)S(1)}, f32[1536]{0:T(1024)}, u32[]{:S(2)}) copy-start(f32[1536]{0:T(1024)} %param.27) | copy-start | bytes 18436
  5.3 4.2 %copy-start.24 = (s32[128,2]{0,1:T(2,128)S(1)}, s32[128,2]{0,1:T(2,128)}, u32[]{:S(2)}) copy-start(s32[128,2]{0,1:T(2,128)} %param.36) | copy-start | bytes 3076
  5.3 5.8 %copy-start.17 = (bf16[128,2048]{1,0:T(8,128)(2,1)S(1)}, bf16[128,2048]{1,0:T(8,128)(2,1)}, u32[]{:S(2)}) copy-start(bf16[128,2048]{1,0:T(8,128)(2,1)} %param.22) | copy-start | bytes 1572868
  5.3 6.0 %copy-start.22 = (f32[2048]{0:T(1024)S(1)}, f32[2048]{0:T(1024)}, u32[]{:S(2)}) copy-start(f32[2048]{0:T(1024)} %param.35) | copy-start | bytes 24580
  42.6 1.2 copy-start.10
  43.8 0.8 copy-start.12
  46.9 1.1 copy-start.4
  48.1 1.0 copy-start.5
  49.1 0.9 copy-start.6
  50.0 0.9 copy-start.7
  51.0 1.4 copy-start.11
  52.4 1.0 copy-start.13
  53.4 57.3 %copy-start.27 = (bf16[1,2048,512]{2,1,0:T(8,128)(2,1)S(1)}, bf16[1,2048,512]{2,1,0:T(8,128)(2,1)}, u32[]{:S(2)}) copy-start(bf16[1,2048,512]{2,1,0:T(8,128)(2,1)} %param.38) | copy-start | bytes 6291460
  107.0 0.7 copy-start.14
  107.7 0.7 copy-start.15
  108.3 2.4 %copy-start.9 = (bf16[4,320,2048]{2,1,0:T(8,128)(2,1)}, bf16[4,320,2048]{2,1,0:T(8,128)(2,1)S(1)}, u32[]{:S(2)}) copy-start(bf16[4,320,2048]{2,1,0:T(8,128)(2,1)S(1)} %get-tuple-element.21) | copy-start | bytes 15728644
  125.6 56.5 %copy-start.19 = (bf16[256,2048]{1,0:T(8,128)(2,1)S(1)}, bf16[256,2048]{1,0:T(8,128)(2,1)}, u32[]{:S(2)}) copy-start(bf16[256,2048]{1,0:T(8,128)(2,1)} %param.33) | copy-start | bytes 3145732
  182.1 1.8 copy-start.18
  182.1 2.1 copy-start.8
  184.2 28.5 %copy-start.26 = (f32[128,2]{0,1:T(2,128)S(1)}, f32[128,2]{0,1:T(2,128)}, u32[]{:S(2)}) copy-start(f32[128,2]{0,1:T(2,128)} %param.37) | copy-start | bytes 3076
  211.9 0.8 copy-start.2
  213.1 4.7 %copy-start.23 = (f32[2048]{0:T(1024)S(1)}, f32[2048]{0:T(1024)}, u32[]{:S(2)}) copy-start(f32[2048]{0:T(1024)} %param.41) | copy-start | bytes 24580
  213.1 6.6 %copy-start.1 = (bf16[1,512,2048]{2,1,0:T(8,128)(2,1)S(1)}, bf16[1,512,2048]{2,1,0:T(8,128)(2,1)}, u32[]{:S(2)}) copy-start(bf16[1,512,2048]{2,1,0:T(8,128)(2,1)} %param.40) | copy-start | bytes 6291460
  214.9 4.1 %copy-start.3 = (bf16[128,2048]{1,0:T(8,128)(2,1)S(1)}, bf16[128,2048]{1,0:T(8,128)(2,1)}, u32[]{:S(2)}) copy-start(bf16[128,2048]{1,0:T(8,128)(2,1)} %copy-done.2) | copy-start | bytes 1572868

commit v4 on v3

--- a/solution.py
+++ b/solution.py
@@ -23,6 +23,7 @@
 
 MESH = pl.DeviceIdType.MESH
 ANY = pl.BlockSpec(memory_space=pl.ANY)
+HBM = pl.BlockSpec(memory_space=pltpu.HBM)
 VMEM = pl.BlockSpec(memory_space=pltpu.VMEM)
 DMA = pltpu.SemaphoreType.DMA
 
@@ -141,7 +142,7 @@
         out_shape=[jax.ShapeDtypeStruct((groups, *a.shape), a.dtype) for a in lats]
         + [jax.ShapeDtypeStruct(rows.shape, rows.dtype)],
         in_specs=[ANY] * (count + 1),
-        out_specs=[ANY] * (count + 1),
+        out_specs=[HBM] * (count + 1),
         scratch_shapes=[pltpu.VMEM(a.shape, a.dtype) for a in lats]
         + [
             pltpu.VMEM(rows.shape[1:], rows.dtype),
@@ -158,57 +159,72 @@
     )(*lats, rows)
 
 
+KV_ORDER = (
+    [(f, 0, 0, p) for p in range(2) for f in range(2)]
+    + [(f, a, 0, p) for p in range(2) for f in range(2) for a in (3, 1)]
+    + [(f, 0, b, p) for p in range(2) for f in range(2) for b in (3, 1)]
+    + [(f, 2, 0, p) for p in range(2) for f in range(2)]
+    + [(f, 3, b, p) for p in range(2) for f in range(2) for b in (3, 1)]
+    + [(f, 1, b, p) for p in range(2) for f in range(2) for b in (3, 1)]
+    + [(f, 0, 2, p) for p in range(2) for f in range(2)]
+    + [(f, 2, b, p) for p in range(2) for f in range(2) for b in (3, 1)]
+    + [(f, a, 2, p) for a in (3, 1, 2) for p in range(2) for f in range(2)]
+)
+KV_SLOT = {key: k for k, key in enumerate(KV_ORDER)}
+
+OWN, LEFT, RIGHT, FAR = range(4)
+ROW_ORDER = (
+    [(OWN, 0), (OWN, 1), (LEFT, 0), (RIGHT, 2), (LEFT, 1), (RIGHT, 3), (OWN, 2), (FAR, 0)]
+    + [(FAR, 2), (FAR, 1), (FAR, 3), (RIGHT, 0), (LEFT, 2), (RIGHT, 1), (LEFT, 3), (OWN, 3)]
+)
+ROW_SLOT = {key: k for k, key in enumerate(ROW_ORDER)}
+BACK = (3, 1)
+
+
 class Spread:
-    def __init__(self, own, held, sends, recvs):
+    def __init__(self, held, sends, recvs):
         ep, tp = lax.axis_index("ep"), lax.axis_index("tp")
         side = 4
         core = lax.rem(ep, 2)
         y = lax.rem(ep // 2, side)
         z = ep // (2 * side)
-        self.own, self.held, self.sends, self.recvs = own, held, sends, recvs
-        self.ep, self.tp = ep, tp
-        self.mate = ep + 1 - 2 * core
-        cut = held.shape[2] // 32 * 16
-        self.parts = (pl.ds(0, cut), pl.ds(cut, held.shape[2] - cut))
+        self.held, self.sends, self.recvs = held, sends, recvs
+        self.mate = (ep + 1 - 2 * core, tp)
+        cut = held.shape[1] // 32 * 16
+        self.parts = (pl.ds(0, cut), pl.ds(cut, held.shape[1] - cut))
 
         def index(dz, dy):
-            return (lax.rem(z + dz, side) * side + lax.rem(y + dy, side)) * 2 + core
-
-        self.block = lambda f, a, b: index(b, a) if f == 0 else index(a, b)
-        self.neighbours = [index(1, 0), index(3, 0), index(0, 1), index(0, 3)]
-
-    def place(self, f, ring, way):
-        step = (1, 3)[way]
-        return (self.block(f, step, 0) if ring == 0 else self.block(f, 0, step), self.tp)
-
-    def copy(self, f, a, b, place, k, part=None):
-        mine = a == 0 and b == 0
-        where = self.block(f, a, b)
-        if part is None:
-            src = self.own.at[f] if mine else self.held.at[where, f]
-            dst = self.held.at[where, f]
-        else:
-            src = self.held.at[where, f, self.parts[part]]
-            dst = src
+            return ((lax.rem(z + dz, side) * side + lax.rem(y + dy, side)) * 2 + core, tp)
+
+        around = [(index(0, 1), index(0, 3)), (index(1, 0), index(3, 0))]
+        self.places = [around, around[::-1]]
+        self.neighbours = [place for pair in around for place in pair] + [self.mate]
+
+    def copy(self, f, here, there, place, k, part=None):
+        src = self.held.at[KV_SLOT[(f, *here)]]
+        dst = self.held.at[KV_SLOT[(f, *there)]]
+        if part is not None:
+            src, dst = src.at[self.parts[part]], dst.at[self.parts[part]]
         return remote(src, dst, self.sends, self.recvs, 36 * f + k, place)
 
     def first(self, f, way):
-        return self.copy(f, 0, 0, self.place(f, 0, way), way)
+        return self.copy(f, (0, 0, 0), (BACK[way], 0, 0), self.places[f][0][way], way)
 
     def first_on(self, f, way):
-        return self.copy(f, (3, 1)[way], 0, self.place(f, 0, way), 2 + way, part=way)
+        return self.copy(
+            f, (BACK[way], 0, 0), (2, 0, 0), self.places[f][0][way], 2 + way, part=way
+        )
 
     def second(self, f, a, way):
-        return self.copy(f, a, 0, self.place(f, 1, way), 4 + 4 * a + way)
+        return self.copy(f, (a, 0, 0), (a, BACK[way], 0), self.places[f][1][way], 4 + 4 * a + way)
 
     def second_on(self, f, a, way):
-        return self.copy(f, a, (3, 1)[way], self.place(f, 1, way), 6 + 4 * a + way, part=way)
+        return self.copy(
+            f, (a, BACK[way], 0), (a, 2, 0), self.places[f][1][way], 6 + 4 * a + way, part=way
+        )
 
     def share(self, f, a, b):
-        return self.copy(f, a, b, (self.mate, self.tp), 20 + 4 * a + b)
-
-    def everyone(self):
-        return [(place, self.tp) for place in self.neighbours] + [(self.mate, self.tp)]
+        return self.copy(f, (a, b, 0), (a, b, 1), self.mate, 20 + 4 * a + b)
 
     def start(self):
         for f in range(2):
@@ -224,7 +240,7 @@
             for way in range(2):
                 self.first(f, way).wait_recv()
                 self.first_on(f, way).start()
-                a = (3, 1)[way]
+                a = BACK[way]
                 for there in range(2):
                     self.second(f, a, there).start()
                 self.share(f, a, 0).start()
@@ -234,7 +250,7 @@
             for way in range(2):
                 self.second(f, a, way).wait_recv()
                 self.second_on(f, a, way).start()
-                self.share(f, a, (3, 1)[way]).start()
+                self.share(f, a, BACK[way]).start()
 
     def got_far_first(self):
         for f in range(2):
@@ -250,11 +266,16 @@
                 self.second_on(f, a, way).wait_recv()
             self.share(f, a, 2).start()
 
+    def got_shares(self, *spots):
+        for f in range(2):
+            for a, b in spots:
+                self.share(f, a, b).wait_recv()
+
     def close(self):
         for f in range(2):
             for a in range(4):
                 for b in range(4):
-                    self.share(f, a, b).wait()
+                    self.share(f, a, b).wait_send()
             for way in range(2):
                 self.first(f, way).wait_send()
                 self.first_on(f, way).wait_send()
@@ -263,202 +284,83 @@
                     self.second_on(f, a, way).wait_send()
 
 
-def gather_kernel(
-    x,
-    latents,
-    key_plain,
-    value_up,
-    turned,
-    qlat,
-    query_plain,
-    query_rotary,
-    cosine,
-    sine,
-    out,
-    held,
-    qn,
-    qt,
-    kept,
-    block,
-    own_sem,
-    sends,
-    recvs,
-    kv_sends,
-    kv_recvs,
-):
-    ep, tp, right, left, across = ring_places()
-    to_right, to_left = (ep, right), (ep, left)
-    size = x.shape[0] // 4
-    spread = Spread(block, held, kv_sends, kv_recvs)
-    barrier = pltpu.get_barrier_semaphore()
-    places = [to_right, to_left] + spread.everyone()
-    for place in places:
-        pl.semaphore_signal(barrier, inc=1, device_id=place, device_id_type=MESH)
-    take = pltpu.make_async_copy(x, kept, own_sem.at[0])
-    take.start()
-
-    keys = jnp.dot(latents[...], key_plain[...], preferred_element_type=jnp.float32)
-    values = jnp.dot(latents[...], value_up[...], preferred_element_type=jnp.float32).T
-    keys, values = keys.astype(jnp.bfloat16), values.astype(jnp.bfloat16)
-    low = keys.shape[1]
-    half = low // 2
-    for f in range(2):
-        block[f, :half, :low] = keys[low * f : low * f + half]
-        block[f, :half, low:] = keys[low * f + half : low * f + low]
-        block[f, half:low, :low] = values[:half, low * f : low * f + low]
-        block[f, half:low, low:] = values[half:, low * f : low * f + low]
-        block[f, low:, :] = turned[f]
-    take.wait()
-    put = pltpu.make_async_copy(kept, out.at[tp], own_sem.at[0])
-    put.start()
-    pl.semaphore_wait(barrier, len(places))
-
-    def chunk(c):
-        return pl.ds(c * size, size)
-
-    def fresh(c, way):
-        return remote(
-            x.at[chunk(c)], out.at[tp, chunk(c)], sends, recvs, 4 * way + c, (to_right, to_left)[way]
-        )
-
-    def onward(c):
-        way = c // 2
-        origin = (left, right)[way]
-        part = out.at[origin, chunk(c)]
-        return remote(part, part, sends, recvs, 8 + c, (to_right, to_left)[way])
-
-    news = {(c, way): fresh(c, way) for c in range(4) for way in range(2)}
-    passed = [onward(c) for c in range(4)]
-    for key in ((0, 0), (2, 1), (1, 0), (3, 1)):
-        news[key].start()
-    spread.start()
-    keep = pltpu.make_async_copy(block, held.at[ep], own_sem.at[1])
-    keep.start()
-
-    plain = jnp.dot(qlat[...], query_plain[...], preferred_element_type=jnp.float32)
-    qn[...] = plain.T.astype(jnp.bfloat16)
-    rotated = jnp.dot(qlat[...], query_rotary[...], preferred_element_type=jnp.float32).T
-    quarter = ROPE // 2
-    for h in range(rotated.shape[0] // ROPE):
-        a = rotated[h * ROPE : h * ROPE + quarter]
-        b = rotated[h * ROPE + quarter : h * ROPE + ROPE]
-        qt[h * ROPE : h * ROPE + quarter, :] = (a * cosine[...] - b * sine[...]).astype(
-            jnp.bfloat16
-        )
-        qt[h * ROPE + quarter : h * ROPE + ROPE, :] = (b * cosine[...] + a * sine[...]).astype(
-            jnp.bfloat16
-        )
-
-    def pass_rows(c):
-        news[c, 0].wait_recv()
-        passed[c].start()
-        news[2 + c, 0].start()
-        news[2 + c, 1].wait_recv()
-        passed[2 + c].start()
-        news[c, 1].start()
-
-    spread.got_first()
-    pass_rows(0)
-    spread.got_second(0)
-    pass_rows(1)
-    spread.got_far_first()
-    spread.got_second(3)
-    spread.got_second(1)
-    spread.got_far_second(0)
-    spread.got_second(2)
-    for a in (3, 1, 2):
-        spread.got_far_second(a)
-    spread.close()
-    for c in range(2):
-        news[2 + c, 0].wait_recv()
-        news[c, 1].wait_recv()
-    for copy in passed:
-        copy.wait_recv()
-    for copy in passed + list(news.values()):
-        copy.wait_send()
-    put.wait()
-    keep.wait()
-
-
-def gather(x, latents, key_plain, value_up, turned, qlat, query_plain, query_rotary, cosine, sine):
-    groups, peers = lax.axis_size("tp"), lax.axis_size("ep")
-    count = latents.shape[0]
-    low = key_plain.shape[1]
-    height = low + turned.shape[1]
-    wide = turned.shape[2]
-    return pl.pallas_call(
-        gather_kernel,
-        out_shape=[
-            jax.ShapeDtypeStruct((groups, *x.shape), x.dtype),
-            jax.ShapeDtypeStruct((peers, 2, height, wide), x.dtype),
-            jax.ShapeDtypeStruct((query_plain.shape[1], count), x.dtype),
-            jax.ShapeDtypeStruct((query_rotary.shape[1], count), x.dtype),
-        ],
-        in_specs=[ANY] + [VMEM] * 9,
-        out_specs=[ANY, ANY, VMEM, VMEM],
-        scratch_shapes=[
-            pltpu.VMEM(x.shape, x.dtype),
-            pltpu.VMEM((2, height, wide), x.dtype),
-            DMA((2,)),
-            DMA((12,)),
-            DMA((12,)),
-            DMA((72,)),
-            DMA((72,)),
-        ],
-        compiler_params=pltpu.CompilerParams(
-            collective_id=2, has_side_effects=True, vmem_limit_bytes=32 * 1024 * 1024
-        ),
-        cost_estimate=pl.CostEstimate(flops=10**10, bytes_accessed=10**6, transcendentals=0),
-    )(x, latents, key_plain, value_up, turned, qlat, query_plain, query_rotary, cosine, sine)
+class Ring:
+    def __init__(self, x, rows, sends, recvs):
+        ep, tp, right, left, across = ring_places()
+        self.places = ((ep, right), (ep, left))
+        size = rows.shape[1]
+        self.news, self.passed, self.own = {}, [], []
+        for c in range(4):
+            chunk = x.at[pl.ds(c * size, size)]
+            for way in range(2):
+                origin = (LEFT, RIGHT)[way]
+                self.news[c, way] = remote(
+                    chunk, rows.at[ROW_SLOT[origin, c]], sends, recvs, 4 * way + c, self.places[way]
+                )
+            way = c // 2
+            origin = (LEFT, RIGHT)[way]
+            self.passed.append(
+                remote(
+                    rows.at[ROW_SLOT[origin, c]],
+                    rows.at[ROW_SLOT[FAR, c]],
+                    sends,
+                    recvs,
+                    8 + c,
+                    self.places[way],
+                )
+            )
+
+    def start(self):
+        for key in ((0, 0), (2, 1), (1, 0), (3, 1)):
+            self.news[key].start()
+
+    def relay(self, c):
+        self.news[c, 0].wait_recv()
+        self.passed[c].start()
+        self.news[2 + c, 0].start()
+        self.news[2 + c, 1].wait_recv()
+        self.passed[2 + c].start()
+        self.news[c, 1].start()
+
+    def arrived(self, whose, c):
+        if whose == FAR:
+            self.passed[c].wait_recv()
+        elif whose in (LEFT, RIGHT) and c // 2 != whose - LEFT:
+            self.news[c, whose - LEFT].wait_recv()
+
+    def close(self):
+        for copy in self.passed + list(self.news.values()):
+            copy.wait_send()
 
 
 class Fold:
     def __init__(self, part, far, near, mixed, sends, recvs):
         self.part, self.far, self.near, self.mixed = part, far, near, mixed
         ep, tp, right, left, across = ring_places()
-        self.tp, self.sides = tp, (right, left)
         self.places = ((ep, right), (ep, left))
-        self.size = size = part.shape[1] // 4
-        self.at = [pl.ds(c * size, size) for c in range(4)]
-        self.hops = []
-        self.plain = []
-        self.joined = []
+        self.hops, self.plain, self.joined = [], [], []
         for c in range(4):
             way = c // 2
             other = 1 - way
-            self.hops.append(
-                remote(part.at[across, self.at[c]], far.at[c], sends, recvs, c, self.places[way])
-            )
+            self.hops.append(remote(part(FAR, c), far.at[c], sends, recvs, c, self.places[way]))
             self.plain.append(
                 remote(
-                    part.at[self.sides[other], self.at[c]],
-                    near.at[c],
-                    sends,
-                    recvs,
-                    4 + c,
-                    self.places[other],
+                    part((RIGHT, LEFT)[other], c), near.at[c], sends, recvs, 4 + c, self.places[other]
                 )
             )
             self.joined.append(
                 remote(mixed.at[c], far.at[4 + c], sends, recvs, 8 + c, self.places[way])
             )
 
-    def open(self):
-        greet(list(self.places))
-        for c in (0, 2, 1, 3):
-            self.hops[c].start()
-        for c in (2, 0, 3, 1):
-            self.plain[c].start()
-
     def join(self, c):
-        own = self.part[self.sides[c // 2], self.at[c], :]
+        own = self.part((RIGHT, LEFT)[c // 2], c)[...]
         self.mixed[c] = (own.astype(jnp.float32) + self.far[c].astype(jnp.float32)).astype(
             jnp.bfloat16
         )
 
     def total(self, c):
         self.joined[c].wait_recv()
-        own = self.part[self.tp, self.at[c], :].astype(jnp.float32)
+        own = self.part(OWN, c)[...].astype(jnp.float32)
         return own + self.near[c].astype(jnp.float32) + self.far[4 + c].astype(jnp.float32)
 
     def close(self):
@@ -483,7 +385,12 @@
     barrier = pltpu.get_barrier_semaphore()
     for place in swaps:
         pl.semaphore_signal(barrier, inc=1, device_id=place, device_id_type=MESH)
-    fold = Fold(part, far, near, mixed, sends, recvs)
+    size = part.shape[1] // 4
+
+    def piece(whose, c):
+        return part.at[(tp, left, right, across)[whose], pl.ds(c * size, size)]
+
+    fold = Fold(piece, far, near, mixed, sends, recvs)
     for place in fold.places:
         pl.semaphore_signal(barrier, inc=1, device_id=place, device_id_type=MESH)
     pl.semaphore_wait(barrier, len(swaps) + 2)
@@ -519,7 +426,7 @@
     for c in range(4):
         whole = fold.total(c)
         scale = lax.rsqrt(jnp.mean(whole * whole, axis=-1, keepdims=True) + EPS)
-        out[fold.at[c], :] = (whole * scale * gain[...]).astype(jnp.bfloat16)
+        out[c * size : (c + 1) * size, :] = (whole * scale * gain[...]).astype(jnp.bfloat16)
     fold.close()
     for copy in moves:
         copy.wait()
@@ -547,47 +454,198 @@
     )(part, gain.reshape(1, width), rows)
 
 
-def attend_kernel(
-    heads, qn_ref, qt_ref, kv_ref, part, o_ref, sum_ref, rhs, s_buf, p_buf, peak, acc, *fold_refs
+def core_kernel(
+    x,
+    latents_in,
+    qlat_in,
+    turned,
+    key_plain_in,
+    value_up_in,
+    query_plain_in,
+    query_rotary_in,
+    gate_in,
+    up_in,
+    down_in,
+    cosine,
+    sine,
+    o_ref,
+    sum_ref,
+    rhs,
+    s_buf,
+    p_buf,
+    peak,
+    acc,
+    held,
+    rows,
+    part,
+    latents,
+    qlat,
+    key_plain,
+    value_up,
+    query_plain,
+    query_rotary,
+    gate_w,
+    up_w,
+    down_w,
+    load_sem,
+    row_sends,
+    row_recvs,
+    kv_sends,
+    kv_recvs,
+    *fold_refs,
 ):
     step = pl.program_id(0)
-    steps = pl.num_programs(0)
-    fold = Fold(part, *fold_refs)
+    heads = acc.shape[0]
+    pair = 4
+    wide = held.shape[2]
+    size = wide // 2
+    subs = size // SUB
+    count = pair * SUB
+    queries = o_ref.shape[1]
+    chunk_rows = rows.shape[1]
+    spread = Spread(held, kv_sends, kv_recvs)
+    ring = Ring(x, rows, row_sends, row_recvs)
+    fold = Fold(lambda whose, c: part.at[ROW_SLOT[whose, c]], *fold_refs)
+    loads = [
+        pltpu.make_async_copy(src, dst, load_sem.at[k])
+        for k, (src, dst) in enumerate(
+            [
+                (latents_in, latents),
+                (key_plain_in, key_plain),
+                (value_up_in, value_up),
+                (qlat_in, qlat),
+                (query_plain_in, query_plain),
+                (query_rotary_in, query_rotary),
+                (gate_in, gate_w),
+                (up_in, up_w),
+                (down_in, down_w),
+            ]
+        )
+    ]
+    takes = [
+        pltpu.make_async_copy(
+            x.at[pl.ds(c * chunk_rows, chunk_rows)], rows.at[ROW_SLOT[OWN, c]], load_sem.at[9 + c]
+        )
+        for c in range(4)
+    ]
 
     @pl.when(step == 0)
     def _():
-        fold.open()
-
-    @pl.when(step == steps * 5 // 16)
-    def _():
-        for c in range(4):
-            fold.hops[c].wait_recv()
-            fold.join(c)
-
-    @pl.when(step == steps * 5 // 16 + 1)
-    def _():
-        for c in (0, 2, 1, 3):
-            fold.joined[c].start()
-
-    pair, wide = kv_ref.shape[0], kv_ref.shape[2]
-    size = wide // 2
-    subs = size // SUB
-    rows = pair * SUB
-    queries = qn_ref.shape[1]
-
-    @pl.when(step == 0)
-    def _():
+        barrier = pltpu.get_barrier_semaphore()
+        places = list(ring.places) + spread.neighbours
+        for place in places:
+            pl.semaphore_signal(barrier, inc=1, device_id=place, device_id_type=MESH)
+        for copy in loads[:3] + takes + loads[3:]:
+            copy.start()
+        pl.semaphore_wait(barrier, len(places))
+        ring.start()
+        for copy in loads[:3]:
+            copy.wait()
+        keys = jnp.dot(latents[...], key_plain[...], preferred_element_type=jnp.float32)
+        values = jnp.dot(latents[...], value_up[...], preferred_element_type=jnp.float32).T
+        keys, values = keys.astype(jnp.bfloat16), values.astype(jnp.bfloat16)
+        half = size // 2
+        for f in range(2):
+            own = KV_SLOT[f, 0, 0, 0]
+            held[own, :half, :size] = keys[size * f : size * f + half]
+            held[own, :half, size:] = keys[size * f + half : size * f + size]
+            held[own, half:size, :size] = values[:half, size * f : size * f + size]
+            held[own, half:size, size:] = values[half:, size * f : size * f + size]
+            held[own, size:, :] = turned[f]
         rhs[...] = jnp.zeros_like(rhs)
+        peak[...] = jnp.full_like(peak, FLOOR)
+        acc[...] = jnp.zeros_like(acc)
+        spread.start()
+        for copy in loads[3:6]:
+            copy.wait()
+        plain = jnp.dot(qlat[...], query_plain[...], preferred_element_type=jnp.float32)
+        plain = plain.T.astype(jnp.bfloat16)
+        rotated = jnp.dot(qlat[...], query_rotary[...], preferred_element_type=jnp.float32).T
+        quarter = ROPE // 2
         for h in range(heads):
+            a = rotated[h * ROPE : h * ROPE + quarter]
+            b = rotated[h * ROPE + quarter : h * ROPE + ROPE]
+            first = (a * cosine[...] - b * sine[...]).astype(jnp.bfloat16)
+            second = (b * cosine[...] + a * sine[...]).astype(jnp.bfloat16)
+            at = h % 2 * NOPE
             for j in range(subs):
-                at = h % 2 * NOPE
-                rhs[h, j, at : at + NOPE, :] = qn_ref[h * NOPE : (h + 1) * NOPE, :]
+                rhs[h, j, at : at + NOPE, :] = plain[h * NOPE : (h + 1) * NOPE]
                 low = 128 + j * ROPE
-                rhs[h, j, low : low + ROPE, :] = qt_ref[h * ROPE : (h + 1) * ROPE, :]
-        peak[...] = jnp.full_like(peak, -1e30)
-        acc[...] = jnp.zeros_like(acc)
-
-    turned = jnp.concatenate(
+                rhs[h, j, low : low + quarter, :] = first
+                rhs[h, j, low + quarter : low + ROPE, :] = second
+        for copy in takes + loads[6:]:
+            copy.wait()
+        spread.got_shares((0, 0))
+
+    plan = {
+        1: [lambda: spread.got_first()],
+        2: [lambda: ring.relay(0), lambda: spread.got_shares((3, 0), (1, 0))],
+        3: [lambda: spread.got_second(0)],
+        4: [
+            lambda: ring.relay(1),
+            lambda: spread.got_shares((0, 3), (0, 1)),
+            lambda: spread.got_far_first(),
+        ],
+        5: [lambda: spread.got_shares((2, 0))],
+        6: [lambda: spread.got_second(3)],
+        7: [lambda: spread.got_shares((3, 3), (3, 1)), lambda: spread.got_second(1)],
+        8: [lambda: fold.hops[0].start()],
+        9: [
+            lambda: fold.hops[2].start(),
+            lambda: spread.got_shares((1, 3), (1, 1)),
+            lambda: spread.got_far_second(0),
+            lambda: spread.got_second(2),
+        ],
+        10: [lambda: fold.hops[1].start(), lambda: spread.got_shares((0, 2))]
+        + [fold.plain[c].start for c in (2, 0, 3, 1)],
+        11: [lambda: fold.hops[3].start(), lambda: spread.got_far_second(3)],
+        12: [
+            lambda: spread.got_shares((2, 3), (2, 1)),
+            lambda: spread.got_far_second(1),
+            lambda: fold.hops[0].wait_recv(),
+            lambda: fold.join(0),
+        ],
+        13: [
+            lambda: spread.got_shares((3, 2)),
+            lambda: fold.joined[0].start(),
+            lambda: spread.got_far_second(2),
+            lambda: fold.hops[2].wait_recv(),
+            lambda: fold.join(2),
+        ],
+        14: [
+            lambda: spread.got_shares((1, 2)),
+            lambda: fold.joined[2].start(),
+            lambda: fold.hops[1].wait_recv(),
+            lambda: fold.join(1),
+        ],
+        15: [
+            lambda: spread.got_shares((2, 2)),
+            lambda: fold.joined[1].start(),
+            lambda: fold.hops[3].wait_recv(),
+            lambda: fold.join(3),
+        ],
+    }
+    for k, actions in plan.items():
+
+        @pl.when(step == k)
+        def _(k=k, actions=actions):
+            for action in actions:
+                action()
+            ring.arrived(*ROW_ORDER[k])
+
+    gate = jnp.minimum(
+        jnp.dot(rows[step], gate_w[...], preferred_element_type=jnp.float32), CLAMP
+    )
+    up = jnp.clip(
+        jnp.dot(rows[step], up_w[...], preferred_element_type=jnp.float32), -CLAMP, CLAMP
+    )
+    acts = ((up + 1.0) * gate * jax.nn.sigmoid(ALPHA * gate)).astype(jnp.bfloat16)
+    part[step] = jnp.dot(acts, down_w[...], preferred_element_type=jnp.float32).astype(
+        jnp.bfloat16
+    )
+
+    kv_ref = held.at[pl.ds(pair * step, pair)]
+    turns = jnp.concatenate(
         [kv_ref[b, size:, g * 128 : (g + 1) * 128] for b in range(pair) for g in range(wide // 128)],
         axis=0,
     )
@@ -601,13 +659,13 @@
             left = jnp.concatenate(
                 [kv_ref[b, at : at + SUB, lanes : lanes + 128] for b in range(pair)], axis=0
             )
-            left = jnp.concatenate([left, turned], axis=1)
-            part = jnp.dot(left, rhs[h, j], preferred_element_type=jnp.float32)
+            left = jnp.concatenate([left, turns], axis=1)
+            block = jnp.dot(left, rhs[h, j], preferred_element_type=jnp.float32)
             for b in range(pair):
-                s_buf[h % 2, b * size + j * SUB : b * size + (j + 1) * SUB, :] = part[
+                s_buf[h % 2, b * size + j * SUB : b * size + (j + 1) * SUB, :] = block[
                     b * SUB : (b + 1) * SUB
                 ]
-            top = jnp.max(part.reshape(rows // 8, 8, queries), axis=0)
+            top = jnp.max(block.reshape(count // 8, 8, queries), axis=0)
             best = top if best is None else jnp.maximum(best, top)
         return jnp.max(best, axis=0, keepdims=True)
 
@@ -640,61 +698,63 @@
         finish(h, best)
         best = later
 
-    @pl.when(step == steps - 1)
+    @pl.when(step == pl.num_programs(0) - 1)
     def _():
-        for c in range(4):
-            fold.plain[c].wait_recv()
-            sum_ref[fold.at[c], :] = fold.total(c).astype(jnp.bfloat16)
-        fold.close()
+        fold.joined[3].start()
         for h in range(heads):
             o_ref[h * VDIM : (h + 1) * VDIM, :] = (
                 acc[h, :VDIM, :] / acc[h, VDIM : VDIM + 1, :]
             ).astype(jnp.bfloat16)
-
-
-def attend(qn, qt, packed, part, pair=4):
-    heads = qn.shape[0] // NOPE
-    queries = qn.shape[1]
-    blocks, height, wide = packed.shape
-    size = wide // 2
+        for c in range(4):
+            fold.plain[c].wait_recv()
+            sum_ref[c * chunk_rows : (c + 1) * chunk_rows, :] = fold.total(c).astype(jnp.bfloat16)
+        fold.close()
+        ring.close()
+        spread.close()
+
+
+def core(x, latents, qlat, turned, mats, cosine, sine):
+    key_plain, value_up, query_plain, query_rotary, gate_w, up_w, down_w = mats
+    heads = query_plain.shape[1] // NOPE
+    queries = latents.shape[0]
+    size = key_plain.shape[1]
+    wide = turned.shape[2]
+    height = size + turned.shape[1]
+    slots, width = x.shape
     subs = size // SUB
+    bf16 = jnp.bfloat16
     return pl.pallas_call(
-        functools.partial(attend_kernel, heads),
+        core_kernel,
         out_shape=[
-            jax.ShapeDtypeStruct((heads * VDIM, queries), jnp.bfloat16),
-            jax.ShapeDtypeStruct(part.shape[1:], jnp.bfloat16),
+            jax.ShapeDtypeStruct((heads * VDIM, queries), bf16),
+            jax.ShapeDtypeStruct((slots, width), bf16),
         ],
-        grid=(blocks // pair,),
-        in_specs=[
-            pl.BlockSpec(qn.shape, lambda i: (0, 0)),
-            pl.BlockSpec(qt.shape, lambda i: (0, 0)),
-            pl.BlockSpec((pair, height, wide), lambda i: (i, 0, 0)),
-            VMEM,
-        ],
-        out_specs=[
-            pl.BlockSpec((heads * VDIM, queries), lambda i: (0, 0)),
-            pl.BlockSpec(part.shape[1:], lambda i: (0, 0)),
-        ],
+        grid=(16,),
+        in_specs=[HBM] * 3 + [VMEM] + [HBM] * 7 + [VMEM] * 2,
+        out_specs=[VMEM, VMEM],
         scratch_shapes=[
-            pltpu.VMEM((heads, subs, 256, queries), jnp.bfloat16),
-            pltpu.VMEM((2, pair * size, queries), jnp.float32),
-            pltpu.VMEM((2, pair * size, queries), jnp.bfloat16),
+            pltpu.VMEM((heads, subs, 256, queries), bf16),
+            pltpu.VMEM((2, 4 * size, queries), jnp.float32),
+            pltpu.VMEM((2, 4 * size, queries), bf16),
             pltpu.VMEM((8, queries), jnp.float32),
             pltpu.VMEM((heads, VDIM + 16, queries), jnp.float32),
+            pltpu.VMEM((64, height, wide), bf16),
+            pltpu.VMEM((16, slots // 4, width), bf16),
+            pltpu.VMEM((16, slots // 4, width), bf16),
+            pltpu.VMEM(latents.shape, bf16),
+            pltpu.VMEM(qlat.shape, bf16),
         ]
-        + fold_scratch(part.shape[1], part.shape[2]),
+        + [pltpu.VMEM(a.shape, bf16) for a in mats]
+        + [DMA((13,)), DMA((12,)), DMA((12,)), DMA((72,)), DMA((72,))]
+        + fold_scratch(slots, width),
         compiler_params=pltpu.CompilerParams(
             dimension_semantics=("arbitrary",),
-            vmem_limit_bytes=56 * 1024 * 1024,
+            vmem_limit_bytes=63 * 1024 * 1024,
             collective_id=4,
             has_side_effects=True,
         ),
-        cost_estimate=pl.CostEstimate(
-            flops=2 * heads * queries * blocks * size * (256 + VDIM),
-            bytes_accessed=blocks * height * wide * 2,
-            transcendentals=heads * queries * blocks * size,
-        ),
-    )(qn, qt, packed, part)
+        cost_estimate=pl.CostEstimate(flops=10**11, bytes_accessed=10**7, transcendentals=10**7),
+    )(x, latents, qlat, turned, *mats, cosine, sine)
 
 
 def norm_rows(values, gain):
@@ -785,28 +845,18 @@
     turned = turned.reshape(2, 16, 4 * 4 * ROPE)
     all_cos, all_sin = turn_tables(group_base + jnp.arange(count, dtype=jnp.int32), ROPE)
     width = expert_hidden.shape[1]
-    piece, packed, qn, qt = gather(
-        received.reshape(slots, width),
-        latents,
+    mats = (
         key_plain,
         value_up,
-        turned,
-        qlat,
         query_plain,
         query_rotary,
-        all_cos.T,
-        all_sin.T,
-    )
-    piece = piece.reshape(groups * slots, width)
-    packed = packed.reshape(-1, *packed.shape[2:])
-    gate_w = gate_proj[0]
-    up_w = up_proj[0]
-    down_w = down_proj[0]
-    gate = jnp.minimum(jnp.dot(piece, gate_w, preferred_element_type=jnp.float32), CLAMP)
-    up = jnp.clip(jnp.dot(piece, up_w, preferred_element_type=jnp.float32), -CLAMP, CLAMP)
-    acts = ((up + 1.0) * gate * jax.nn.sigmoid(ALPHA * gate)).astype(jnp.bfloat16)
-    part = jnp.dot(acts, down_w, preferred_element_type=jnp.float32).astype(jnp.bfloat16)
-    attended, sums = attend(qn, qt, packed, part.reshape(groups, slots, width))
+        gate_proj[0],
+        up_proj[0],
+        down_proj[0],
+    )
+    attended, sums = core(
+        received.reshape(slots, width), latents, qlat, turned, mats, all_cos.T, all_sin.T
+    )
     mixed = lax.dot_general(
         attended, output_proj, (((0,), (0,)), ((), ())), preferred_element_type=jnp.float32
     ).astype(jnp.bfloat16)

time: 220 us -> 182 us (0.83)
  matrix products: 23.9 us -> 8.71 us
  local copies, waits for them, and re-layouts: 19.6 us -> 8.2 us
  Pallas kernels: 168 us -> 158 us
    dot_general x2 -> x0, matrix products: 14.9 us -> none  [the longest x1 10.4 us: on_device(): jnp.dot(acts, down_w, preferred_element_type=jnp.float32)]
    pallas_call x2 -> x1, Pallas kernels: 110 us -> 100 us  [core(): pl.pallas_call(core_kernel, out_shape=[jax.ShapeDtypeStruct((heads * VDIM...]
    unnamed x64 -> x36, local copies, waits for them, and re-layouts: 15 us -> 5.42 us
where the time goes in v4:
time: 182 us
  Pallas kernels  158 us (87%)
  matrix products  8.71 us (5%)
  local copies, waits for them, and re-layouts  8.2 us (5%)
  other arithmetic  6.08 us (3%)
    pallas_call x1, Pallas kernels, core(): pl.pallas_call(core_kernel, out_shape=[jax.ShapeDtypeStruct((heads * VDIM...  100 us
    pallas_call x1, Pallas kernels, exchange(): pl.pallas_call(functools.partial(exchange_kernel, count), out_shape=[jax....  30.4 us
    pallas_call x1, Pallas kernels, finish(): pl.pallas_call(finish_kernel, out_shape=[jax.ShapeDtypeStruct((count, wid...  27.4 us
    unnamed x36, local copies, waits for them, and re-layouts  5.42 us
    dot_general x1, matrix products, on_device(): jnp.dot(hidden, query_down, preferred_element_type=jnp.float32)  4.04 us

profile of v4, /device:TPU:1, one launch (start us, length us, event | category | flops | bytes accessed | tf_op | source)
XLA Modules:
  0.0 181.9 jit_solution(1034002345234101988)
XLA Ops:
  0.6 0.0 copy-start
  0.6 0.0 copy-start.11
  0.7 1.3 fusion.2
  2.0 1.4 fusion.28
  3.4 0.1 fusion.23
  3.6 0.1 copy.51
  3.7 0.8 copy.52
  4.5 0.1 eq.42
  4.7 0.6 reduce-window.6
  5.2 0.2 slice_reduce_fusion
  5.5 0.1 eq.38
  5.6 0.1 fusion.16
  5.7 0.1 reduce_sum.71
  5.9 0.1 copy.55
  5.9 0.1 fusion.13
  6.0 0.2 fusion.5
  6.2 0.0 copy-start.4
  6.2 0.0 copy-start.9
  6.2 0.6 fusion.1
  6.8 0.3 copy.60
  7.1 0.1 copy-done.4
  7.3 4.0 %multiply_reduce_fusion.1 = (f32[128]{0:T(128)S(1)}, f32[128,1536]{1,0:T(8,128)S(1)}) fusion(bf16[2048,1536]{1,0:T(8,128)(2,1)} %param.24, bf16[128,2048]{1,0:T(8,128)(2,1)S(1)} %copy-done.4, f32[2048]{0:T(1024)S(1)} %copy-done.9, f32[128]{0:T(128)S(1)} %add_rsqrt_fusion.4), kind=kOutput, calls=%fused_computation.22 | convolution fusion | flops 806748032 | bytes 7611392 | tf_op jit(solution)/shard_map/dot_general | solution.py:811
  11.3 0.0 copy-start.12
  11.3 0.1 multiply_convert_fusion.refs_2_
  11.5 0.6 multiply_reduce_fusion.2
  12.1 0.1 multiply_convert_fusion.1.refs_0_
  12.2 30.4 %shard_map.212 = (bf16[4,128,512]{2,1,0:T(8,128)(2,1)S(1)}, bf16[4,128,128]{2,1,0:T(8,128)(2,1)S(1)}, bf16[4,128,1536]{2,1,0:T(8,128)(2,1)S(1)}, bf16[32,10,16,128]{3,2,1,0:T(8,128)(2,1)S(1)}) custom-call(bf16[128,512]{1,0:T(8,128)(2,1)S(1)} %multiply_convert_fusion.1.refs_0_, bf16[128,128]{1,0:T(8,128)(2,1)S(1)} %pad.4.refs_1_, ...), custom_call_target="tpu_custom_call" | custom-call | flops 10000000000 | bytes 1000000 | tf_op jit(solution)/shard_map/pallas_call | solution.py:140
  42.7 1.1 copy-done.2
  43.8 1.4 copy.68
  45.2 0.1 copy.69
  45.3 0.8 reshape.166.turned
  46.1 0.8 multiply_sine_fusion
  46.9 100.1 %shard_map.213 = (bf16[256,512]{1,0:T(8,128)(2,1)}, bf16[320,2048]{1,0:T(8,128)(2,1)}) custom-call(bf16[320,2048]{1,0:T(8,128)(2,1)} %bitcast.72, bf16[512,512]{1,0:T(8,128)(2,1)} %bitcast.70, bf16[512,1536]{1,0:T(8,128)(2,1)} %bitcast.69, bf16[2,16,512]{2,1,0:T(8,128)(2,1)} %reshape.166.turned, bf16[512,256]{1,0:T(8,128)(2,1)} %key_plain_in.1, ...), custom_call_target="tpu_custom_call" | custom-call | flops 99999997952 | bytes 10000000 | tf_op jit(solution)/shard_map/pallas_call | solution.py:726
  147.1 2.1 %convolution_convert_fusion = bf16[512,2048]{1,0:T(8,128)(2,1)S(1)} fusion(bf16[256,512]{1,0:T(8,128)(2,1)} %get-tuple-element.14, bf16[256,2048]{1,0:T(8,128)(2,1)} %param.33), kind=kOutput, calls=%fused_computation.1 | convolution fusion | flops 537919488 | bytes 3407872 | tf_op jit(solution)/shard_map/dot_general | solution.py:860
  149.2 0.0 copy-start.1
  149.2 0.3 copy.62
  149.5 0.4 copy-done.1
  149.9 27.4 %shard_map.214 = (bf16[128,2048]{1,0:T(8,128)(2,1)S(1)}, bf16[32,10,16,128]{3,2,1,0:T(8,128)(2,1)S(1)}) custom-call(bf16[4,128,2048]{2,1,0:T(8,128)(2,1)S(1)} %bitcast.62, f32[1,2048]{1,0:T(1,128)S(1)} %bitcast.68, bf16[32,10,16,128]{3,2,1,0:T(8,128)(2,1)S(1)} %bitcast.65), custom_call_target="tpu_custom_call" | custom-call | flops 10000000000 | bytes 1000000 | tf_op jit(solution)/shard_map/pallas_call | solution.py:439
  177.3 0.0 copy-start.13
  177.3 0.1 copy.57
  177.4 0.1 mul.210
  177.6 0.8 gather_fusion
  178.4 0.0 copy-start.10
  178.5 0.1 copy.58
  178.6 0.3 fusion
  178.9 1.0 multiply_reduce_fusion
  180.0 1.2 fusion.9
  181.1 0.8 copy.71
  (35 shorter events, 0.2 us)
Async XLA Ops:
  0.6 1.4 copy-start
  0.6 5.3 %copy-start.11 = (s32[128,2]{0,1:T(2,128)S(1)}, s32[128,2]{0,1:T(2,128)}, u32[]{:S(2)}) copy-start(s32[128,2]{0,1:T(2,128)} %param.36) | copy-start | bytes 3076
  0.7 5.4 %copy-start.5 = (bf16[128,2048]{1,0:T(8,128)(2,1)S(1)}, bf16[128,2048]{1,0:T(8,128)(2,1)}, u32[]{:S(2)}) copy-start(bf16[128,2048]{1,0:T(8,128)(2,1)} %param.22) | copy-start | bytes 1572868
  0.7 5.5 %copy-start.7 = (f32[2048]{0:T(1024)S(1)}, f32[2048]{0:T(1024)}, u32[]{:S(2)}) copy-start(f32[2048]{0:T(1024)} %param.35) | copy-start | bytes 24580
  6.2 1.0 copy-start.4
  6.2 1.0 copy-start.9
  7.3 4.1 %copy-start.8 = (f32[1536]{0:T(1024)S(1)}, f32[1536]{0:T(1024)}, u32[]{:S(2)}) copy-start(f32[1536]{0:T(1024)} %param.27) | copy-start | bytes 18436
  7.3 4.2 %copy-start.14 = (bf16[2048,512]{1,0:T(8,128)(2,1)S(1)}, bf16[2048,512]{1,0:T(8,128)(2,1)}, u32[]{:S(2)}) copy-start(bf16[2048,512]{1,0:T(8,128)(2,1)} %param.25) | copy-start | bytes 6291460
  11.3 0.8 copy-start.12
  42.6 1.2 copy-start.2
  43.8 1.5 copy-start.3
  147.0 2.2 %copy-start.6 = (bf16[320,2048]{1,0:T(8,128)(2,1)S(1)}, bf16[320,2048]{1,0:T(8,128)(2,1)}, u32[]{:S(2)}) copy-start(bf16[320,2048]{1,0:T(8,128)(2,1)} %get-tuple-element.15) | copy-start | bytes 3932164
  149.2 0.7 copy-start.1
  177.3 1.1 copy-start.13
  178.4 1.5 copy-start.10

commit v5 on v4

--- a/solution.py
+++ b/solution.py
@@ -61,102 +61,66 @@
     )
 
 
-def exchange_kernel(latent_count, *refs):
-    lats, rows = refs[:latent_count], refs[latent_count]
-    outs, rows_out = refs[latent_count + 1 : 2 * latent_count + 1], refs[2 * latent_count + 1]
-    kept, kept_rows = refs[2 * latent_count + 2 : 3 * latent_count + 2], refs[3 * latent_count + 2]
-    own_sem, sends, recvs, row_sends, row_recvs = refs[3 * latent_count + 3 :]
-    ep, tp, right, left, across = ring_places()
-    peers = rows.shape[0]
-    swaps = [(partner(ep, r), tp) for r in range(1, peers)]
-    to_right, to_left = (ep, right), (ep, left)
-    greet(swaps + [to_right, to_left])
-    own = [
-        pltpu.make_async_copy(src, dst, own_sem.at[k])
-        for k, (src, dst) in enumerate(
-            [(a, b) for a, b in zip(lats, kept)] + [(rows.at[0], kept_rows)]
-        )
-    ]
-    first, second, waits = [], [], []
-    for k, (lat, out) in enumerate(zip(lats, outs)):
-        half = lat.shape[0] // 2
-        for part, place in ((0, to_right), (1, to_left), (1, to_right), (0, to_left)):
-            way = 0 if place is to_right else 1
-            at = pl.ds(part * half, half)
-            first.append(
-                remote(
-                    lat.at[at], out.at[tp, at], sends, recvs, 6 * k + 2 * way + part, place
-                )
+class Latents:
+    def __init__(self, mine, outs, sends, recvs):
+        ep, tp, right, left, across = ring_places()
+        places = ((ep, right), (ep, left))
+        self.mine, self.outs, self.tp = mine, outs, tp
+        self.news, self.passed = [], []
+        for k, (src, out) in enumerate(zip(mine, outs)):
+            half = src.shape[0] // 2
+            at = [pl.ds(part * half, half) for part in range(2)]
+            self.news.append(
+                {
+                    (part, way): remote(
+                        src.at[at[part]],
+                        out.at[tp, at[part]],
+                        sends,
+                        recvs,
+                        6 * k + 2 * way + part,
+                        places[way],
+                    )
+                    for part in range(2)
+                    for way in range(2)
+                }
             )
-        for way, place, origin in ((0, to_right, left), (1, to_left, right)):
-            at = pl.ds(way * half, half)
-            second.append(
-                remote(
-                    out.at[origin, at], out.at[origin, at], sends, recvs, 6 * k + 4 + way, place
-                )
+            self.passed.append(
+                [
+                    remote(
+                        out.at[(left, right)[way], at[way]],
+                        out.at[(left, right)[way], at[way]],
+                        sends,
+                        recvs,
+                        6 * k + 4 + way,
+                        places[way],
+                    )
+                    for way in range(2)
+                ]
             )
-    moves = [
-        remote(rows.at[r], rows_out.at[r], row_sends, row_recvs, r - 1, swaps[r - 1])
-        for r in range(1, peers)
-    ]
-    for copy in first:
-        copy.start()
-    for copy in moves:
-        copy.start()
-    for copy in own:
-        copy.start()
-    for copy in own:
-        copy.wait()
-    back = [
-        pltpu.make_async_copy(src, dst, own_sem.at[k])
-        for k, (src, dst) in enumerate(
-            [(a, b.at[tp]) for a, b in zip(kept, outs)] + [(kept_rows, rows_out.at[0])]
-        )
-    ]
-    for copy in back:
-        copy.start()
-    for k in range(latent_count):
-        first[4 * k].wait_recv()
-        second[2 * k].start()
-        first[4 * k + 1].wait_recv()
-        second[2 * k + 1].start()
-    for k in range(latent_count):
-        first[4 * k + 2].wait_recv()
-        first[4 * k + 3].wait_recv()
-    for copy in second:
-        copy.wait_recv()
-    for copy in moves:
-        copy.wait_recv()
-    for copy in first + second + moves:
-        copy.wait_send()
-    for copy in back:
-        copy.wait()
-
-
-def exchange(lats, rows):
-    groups = lax.axis_size("tp")
-    count = len(lats)
-    peers = rows.shape[0]
-    return pl.pallas_call(
-        functools.partial(exchange_kernel, count),
-        out_shape=[jax.ShapeDtypeStruct((groups, *a.shape), a.dtype) for a in lats]
-        + [jax.ShapeDtypeStruct(rows.shape, rows.dtype)],
-        in_specs=[ANY] * (count + 1),
-        out_specs=[HBM] * (count + 1),
-        scratch_shapes=[pltpu.VMEM(a.shape, a.dtype) for a in lats]
-        + [
-            pltpu.VMEM(rows.shape[1:], rows.dtype),
-            DMA((count + 1,)),
-            DMA((6 * count,)),
-            DMA((6 * count,)),
-            DMA((peers - 1,)),
-            DMA((peers - 1,)),
-        ],
-        compiler_params=pltpu.CompilerParams(
-            collective_id=1, has_side_effects=True, vmem_limit_bytes=8 * 1024 * 1024
-        ),
-        cost_estimate=pl.CostEstimate(flops=10**10, bytes_accessed=10**6, transcendentals=0),
-    )(*lats, rows)
+
+    def early(self, k):
+        self.news[k][0, 0].start()
+        self.news[k][1, 1].start()
+
+    def late(self, k):
+        self.news[k][1, 0].start()
+        self.news[k][0, 1].start()
+
+    def relay(self, k):
+        for way in range(2):
+            self.news[k][way, way].wait_recv()
+            self.passed[k][way].start()
+
+    def arrived(self, k):
+        self.news[k][1, 0].wait_recv()
+        self.news[k][0, 1].wait_recv()
+        for copy in self.passed[k]:
+            copy.wait_recv()
+
+    def close(self):
+        for news, passed in zip(self.news, self.passed):
+            for copy in list(news.values()) + passed:
+                copy.wait_send()
 
 
 KV_ORDER = (
@@ -174,9 +138,11 @@
 
 OWN, LEFT, RIGHT, FAR = range(4)
 ROW_ORDER = (
-    [(OWN, 0), (OWN, 1), (LEFT, 0), (RIGHT, 2), (LEFT, 1), (RIGHT, 3), (OWN, 2), (FAR, 0)]
-    + [(FAR, 2), (FAR, 1), (FAR, 3), (RIGHT, 0), (LEFT, 2), (RIGHT, 1), (LEFT, 3), (OWN, 3)]
+    [(OWN, 0), (OWN, 1), (LEFT, 0), (RIGHT, 2), (LEFT, 1), (RIGHT, 3), (FAR, 0), (FAR, 2)]
+    + [(RIGHT, 0), (LEFT, 2), (FAR, 1), (FAR, 3), (RIGHT, 1), (LEFT, 3), (OWN, 2), (OWN, 3)]
 )
+GROUP_OF = (0, 3, 1, 2)
+CHUNK_OF = (0, 2, 3, 1)
 ROW_SLOT = {key: k for k, key in enumerate(ROW_ORDER)}
 BACK = (3, 1)
 
@@ -285,13 +251,12 @@
 
 
 class Ring:
-    def __init__(self, x, rows, sends, recvs):
+    def __init__(self, rows, sends, recvs):
         ep, tp, right, left, across = ring_places()
         self.places = ((ep, right), (ep, left))
-        size = rows.shape[1]
         self.news, self.passed, self.own = {}, [], []
         for c in range(4):
-            chunk = x.at[pl.ds(c * size, size)]
+            chunk = rows.at[ROW_SLOT[OWN, c]]
             for way in range(2):
                 origin = (LEFT, RIGHT)[way]
                 self.news[c, way] = remote(
@@ -310,9 +275,8 @@
                 )
             )
 
-    def start(self):
-        for key in ((0, 0), (2, 1), (1, 0), (3, 1)):
-            self.news[key].start()
+    def start(self, c):
+        self.news[c, c // 2].start()
 
     def relay(self, c):
         self.news[c, 0].wait_recv()
@@ -455,10 +419,12 @@
 
 
 def core_kernel(
-    x,
-    latents_in,
-    qlat_in,
-    turned,
+    key_lat,
+    wide_turn,
+    hidden_in,
+    query_down,
+    query_gain,
+    outgoing,
     key_plain_in,
     value_up_in,
     query_plain_in,
@@ -479,6 +445,7 @@
     rows,
     part,
     latents,
+    turned,
     qlat,
     key_plain,
     value_up,
@@ -487,7 +454,12 @@
     gate_w,
     up_w,
     down_w,
+    hidden,
     load_sem,
+    lat_sends,
+    lat_recvs,
+    swap_sends,
+    swap_recvs,
     row_sends,
     row_recvs,
     kv_sends,
@@ -502,18 +474,34 @@
     subs = size // SUB
     count = pair * SUB
     queries = o_ref.shape[1]
-    chunk_rows = rows.shape[1]
+    chunk_rows, pieces = rows.shape[1], rows.shape[2]
+    peers, slots_each = outgoing.shape[0], outgoing.shape[1]
+    ep, tp = lax.axis_index("ep"), lax.axis_index("tp")
     spread = Spread(held, kv_sends, kv_recvs)
-    ring = Ring(x, rows, row_sends, row_recvs)
+    ring = Ring(rows, row_sends, row_recvs)
     fold = Fold(lambda whose, c: part.at[ROW_SLOT[whose, c]], *fold_refs)
+    lat = Latents(
+        (key_lat, wide_turn, qlat.at[tp]), (latents, turned, qlat), lat_sends, lat_recvs
+    )
+    swaps = [(partner(ep, r), tp) for r in range(1, peers)]
+    group = peers // 4
+
+    def spot(r):
+        return rows.at[ROW_SLOT[OWN, CHUNK_OF[r // group]], pl.ds(r % group * slots_each, slots_each)]
+
+    moves = [
+        remote(outgoing.at[r], spot(r), swap_sends, swap_recvs, r - 1, swaps[r - 1])
+        for r in range(1, peers)
+    ]
     loads = [
         pltpu.make_async_copy(src, dst, load_sem.at[k])
         for k, (src, dst) in enumerate(
             [
-                (latents_in, latents),
+                (key_lat, latents.at[tp]),
+                (wide_turn, turned.at[tp]),
                 (key_plain_in, key_plain),
                 (value_up_in, value_up),
-                (qlat_in, qlat),
+                (outgoing.at[0], spot(0)),
                 (query_plain_in, query_plain),
                 (query_rotary_in, query_rotary),
                 (gate_in, gate_w),
@@ -522,27 +510,42 @@
             ]
         )
     ]
-    takes = [
+
+    deep, broad = query_down.shape[0] // 256, query_down.shape[1] // queries
+    tiles = [rhs.at[k // 4, k % 4] for k in range(16)]
+    tiles += [p_buf.at[k // 4, pl.ds(k % 4 * 256, 256)] for k in range(8)]
+    tiles = tiles[: deep * broad]
+    weights = [pltpu.make_async_copy(hidden_in, hidden, load_sem.at[10])] + [
         pltpu.make_async_copy(
-            x.at[pl.ds(c * chunk_rows, chunk_rows)], rows.at[ROW_SLOT[OWN, c]], load_sem.at[9 + c]
+            query_down.at[pl.ds(256 * (k % deep), 256), pl.ds(queries * (k // deep), queries)],
+            tile,
+            load_sem.at[11 + k],
         )
-        for c in range(4)
+        for k, tile in enumerate(tiles)
     ]
 
-    @pl.when(step == 0)
-    def _():
-        barrier = pltpu.get_barrier_semaphore()
-        places = list(ring.places) + spread.neighbours
-        for place in places:
-            pl.semaphore_signal(barrier, inc=1, device_id=place, device_id_type=MESH)
-        for copy in loads[:3] + takes + loads[3:]:
-            copy.start()
-        pl.semaphore_wait(barrier, len(places))
-        ring.start()
-        for copy in loads[:3]:
+    def make_query_latents():
+        for copy in weights:
             copy.wait()
-        keys = jnp.dot(latents[...], key_plain[...], preferred_element_type=jnp.float32)
-        values = jnp.dot(latents[...], value_up[...], preferred_element_type=jnp.float32).T
+        blocks = []
+        for n in range(broad):
+            total = None
+            for k in range(deep):
+                term = jnp.dot(
+                    hidden[:, 256 * k : 256 * (k + 1)],
+                    tiles[n * deep + k][...],
+                    preferred_element_type=jnp.float32,
+                )
+                total = term if total is None else total + term
+            blocks.append(total)
+        whole = jnp.concatenate(blocks, axis=1)
+        scale = lax.rsqrt(jnp.mean(whole * whole, axis=-1, keepdims=True) + EPS)
+        qlat[tp] = (whole * scale * query_gain[...]).astype(jnp.bfloat16)
+
+    def make_keys():
+        both = latents[...].reshape(queries, latents.shape[2])
+        keys = jnp.dot(both, key_plain[...], preferred_element_type=jnp.float32)
+        values = jnp.dot(both, value_up[...], preferred_element_type=jnp.float32).T
         keys, values = keys.astype(jnp.bfloat16), values.astype(jnp.bfloat16)
         half = size // 2
         for f in range(2):
@@ -551,16 +554,21 @@
             held[own, :half, size:] = keys[size * f + half : size * f + size]
             held[own, half:size, :size] = values[:half, size * f : size * f + size]
             held[own, half:size, size:] = values[half:, size * f : size * f + size]
-            held[own, size:, :] = turned[f]
-        rhs[...] = jnp.zeros_like(rhs)
-        peak[...] = jnp.full_like(peak, FLOOR)
-        acc[...] = jnp.zeros_like(acc)
-        spread.start()
-        for copy in loads[3:6]:
-            copy.wait()
-        plain = jnp.dot(qlat[...], query_plain[...], preferred_element_type=jnp.float32)
+            turns = (
+                turned[2 * f, :SUB]
+                + turned[2 * f, SUB:]
+                + turned[2 * f + 1, :SUB]
+                + turned[2 * f + 1, SUB:]
+            )
+            tall = held.shape[1] - size
+            for g in range(SUB // tall):
+                held[own, size:, g * 128 : (g + 1) * 128] = turns[g * tall : (g + 1) * tall]
+
+    def make_queries():
+        both = qlat[...].reshape(queries, qlat.shape[2])
+        plain = jnp.dot(both, query_plain[...], preferred_element_type=jnp.float32)
         plain = plain.T.astype(jnp.bfloat16)
-        rotated = jnp.dot(qlat[...], query_rotary[...], preferred_element_type=jnp.float32).T
+        rotated = jnp.dot(both, query_rotary[...], preferred_element_type=jnp.float32).T
         quarter = ROPE // 2
         for h in range(heads):
             a = rotated[h * ROPE : h * ROPE + quarter]
@@ -573,76 +581,112 @@
                 low = 128 + j * ROPE
                 rhs[h, j, low : low + quarter, :] = first
                 rhs[h, j, low + quarter : low + ROPE, :] = second
-        for copy in takes + loads[6:]:
+
+    def collect(c):
+        g = GROUP_OF[c]
+        for r in range(max(1, g * group), (g + 1) * group):
+            moves[r - 1].wait_recv()
+        ring.start(c)
+
+    @pl.when(step == 0)
+    def _():
+        barrier = pltpu.get_barrier_semaphore()
+        places = list(ring.places) + swaps
+        for place in places:
+            pl.semaphore_signal(barrier, inc=1, device_id=place, device_id_type=MESH)
+        for copy in weights + loads:
+            copy.start()
+        peak[...] = jnp.full_like(peak, FLOOR)
+        acc[...] = jnp.zeros_like(acc)
+        pl.semaphore_wait(barrier, len(places))
+        for k in range(2):
+            lat.early(k)
+            lat.late(k)
+        for g in (0, 1, 3, 2):
+            for r in range(max(1, g * group), (g + 1) * group):
+                moves[r - 1].start()
+        make_query_latents()
+        rhs[...] = jnp.zeros_like(rhs)
+        for k in range(2):
+            lat.relay(k)
+        lat.early(2)
+        lat.late(2)
+        for copy in loads[:5]:
             copy.wait()
+        for k in range(2):
+            lat.arrived(k)
+        make_keys()
+        lat.relay(2)
+        spread.start()
+        collect(0)
+        collect(2)
+        for copy in loads[5:7]:
+            copy.wait()
+        lat.arrived(2)
+        make_queries()
+        collect(1)
+        collect(3)
+        for copy in loads[7:]:
+            copy.wait()
+        spread.got_first()
         spread.got_shares((0, 0))
 
+    def expert(k):
+        both = 2 * chunk_rows
+        piece = rows[pl.ds(2 * k, 2)].reshape(both, pieces * 128)
+        gate = jnp.minimum(jnp.dot(piece, gate_w[...], preferred_element_type=jnp.float32), CLAMP)
+        up = jnp.clip(jnp.dot(piece, up_w[...], preferred_element_type=jnp.float32), -CLAMP, CLAMP)
+        acts = ((up + 1.0) * gate * jax.nn.sigmoid(ALPHA * gate)).astype(jnp.bfloat16)
+        result = jnp.dot(acts, down_w[...], preferred_element_type=jnp.float32)
+        part[pl.ds(2 * k, 2)] = result.astype(jnp.bfloat16).reshape(2, chunk_rows, -1)
+
+    def shares(*spots):
+        return lambda: spread.got_shares(*spots)
+
+    def second(a):
+        return lambda: spread.got_second(a)
+
+    def far_second(a):
+        return lambda: spread.got_far_second(a)
+
+    def join(c):
+        def run():
+            fold.hops[c].wait_recv()
+            fold.join(c)
+
+        return run
+
     plan = {
-        1: [lambda: spread.got_first()],
-        2: [lambda: ring.relay(0), lambda: spread.got_shares((3, 0), (1, 0))],
-        3: [lambda: spread.got_second(0)],
-        4: [
-            lambda: ring.relay(1),
-            lambda: spread.got_shares((0, 3), (0, 1)),
-            lambda: spread.got_far_first(),
-        ],
-        5: [lambda: spread.got_shares((2, 0))],
-        6: [lambda: spread.got_second(3)],
-        7: [lambda: spread.got_shares((3, 3), (3, 1)), lambda: spread.got_second(1)],
-        8: [lambda: fold.hops[0].start()],
-        9: [
-            lambda: fold.hops[2].start(),
-            lambda: spread.got_shares((1, 3), (1, 1)),
-            lambda: spread.got_far_second(0),
-            lambda: spread.got_second(2),
-        ],
-        10: [lambda: fold.hops[1].start(), lambda: spread.got_shares((0, 2))]
-        + [fold.plain[c].start for c in (2, 0, 3, 1)],
-        11: [lambda: fold.hops[3].start(), lambda: spread.got_far_second(3)],
-        12: [
-            lambda: spread.got_shares((2, 3), (2, 1)),
-            lambda: spread.got_far_second(1),
-            lambda: fold.hops[0].wait_recv(),
-            lambda: fold.join(0),
-        ],
-        13: [
-            lambda: spread.got_shares((3, 2)),
-            lambda: fold.joined[0].start(),
-            lambda: spread.got_far_second(2),
-            lambda: fold.hops[2].wait_recv(),
-            lambda: fold.join(2),
-        ],
-        14: [
-            lambda: spread.got_shares((1, 2)),
-            lambda: fold.joined[2].start(),
-            lambda: fold.hops[1].wait_recv(),
-            lambda: fold.join(1),
-        ],
-        15: [
-            lambda: spread.got_shares((2, 2)),
-            lambda: fold.joined[1].start(),
-            lambda: fold.hops[3].wait_recv(),
-            lambda: fold.join(3),
-        ],
+        1: [lambda: ring.relay(0)],
+        2: [shares((3, 0), (1, 0)), lambda: ring.relay(1)],
+        3: [second(0)],
+        4: [shares((0, 3), (0, 1)), lambda: spread.got_far_first()],
+        5: [fold.hops[0].start, fold.hops[2].start, shares((2, 0)), second(3)],
+        6: [fold.plain[2].start, fold.plain[0].start, second(1)],
+        7: [shares((3, 3), (3, 1)), second(2)],
+        8: [far_second(0)],
+        9: [fold.hops[1].start, fold.hops[3].start, shares((1, 3), (1, 1)), far_second(3)],
+        10: [fold.plain[3].start, fold.plain[1].start, shares((0, 2)), far_second(1)],
+        11: [join(0), join(2), far_second(2)],
+        12: [fold.joined[0].start, fold.joined[2].start, shares((2, 3), (2, 1))],
+        13: [shares((3, 2))],
+        14: [shares((1, 2)), join(1), join(3)],
+        15: [fold.joined[1].start, fold.joined[3].start, shares((2, 2))],
     }
-    for k, actions in plan.items():
+    work = {0: 0, 1: 1, 2: 2, 4: 3, 6: 4, 8: 5, 10: 6, 12: 7}
+    for k in range(16):
 
         @pl.when(step == k)
-        def _(k=k, actions=actions):
-            for action in actions:
+        def _(k=k):
+            for action in plan.get(k, ()):
                 action()
-            ring.arrived(*ROW_ORDER[k])
-
-    gate = jnp.minimum(
-        jnp.dot(rows[step], gate_w[...], preferred_element_type=jnp.float32), CLAMP
-    )
-    up = jnp.clip(
-        jnp.dot(rows[step], up_w[...], preferred_element_type=jnp.float32), -CLAMP, CLAMP
-    )
-    acts = ((up + 1.0) * gate * jax.nn.sigmoid(ALPHA * gate)).astype(jnp.bfloat16)
-    part[step] = jnp.dot(acts, down_w[...], preferred_element_type=jnp.float32).astype(
-        jnp.bfloat16
-    )
+            if k in work:
+                for key in ROW_ORDER[2 * work[k] : 2 * work[k] + 2]:
+                    ring.arrived(*key)
+
+    @pl.when((step <= 2) | ((step <= 12) & (lax.rem(step, 2) == 0)))
+    def _():
+        expert(jnp.where(step <= 2, step, 1 + step // 2))
 
     kv_ref = held.at[pl.ds(pair * step, pair)]
     turns = jnp.concatenate(
@@ -700,27 +744,32 @@
 
     @pl.when(step == pl.num_programs(0) - 1)
     def _():
-        fold.joined[3].start()
         for h in range(heads):
             o_ref[h * VDIM : (h + 1) * VDIM, :] = (
                 acc[h, :VDIM, :] / acc[h, VDIM : VDIM + 1, :]
             ).astype(jnp.bfloat16)
         for c in range(4):
             fold.plain[c].wait_recv()
-            sum_ref[c * chunk_rows : (c + 1) * chunk_rows, :] = fold.total(c).astype(jnp.bfloat16)
+            at = GROUP_OF[c] * chunk_rows
+            sum_ref[at : at + chunk_rows, :] = fold.total(c).astype(jnp.bfloat16)
         fold.close()
         ring.close()
         spread.close()
-
-
-def core(x, latents, qlat, turned, mats, cosine, sine):
+        lat.close()
+        for copy in moves:
+            copy.wait_send()
+
+
+def core(key_lat, wide_turn, hidden, query_down, query_gain, outgoing, mats, cosine, sine):
     key_plain, value_up, query_plain, query_rotary, gate_w, up_w, down_w = mats
     heads = query_plain.shape[1] // NOPE
-    queries = latents.shape[0]
+    groups = lax.axis_size("tp")
+    queries = groups * key_lat.shape[0]
     size = key_plain.shape[1]
-    wide = turned.shape[2]
-    height = size + turned.shape[1]
-    slots, width = x.shape
+    wide = 2 * size
+    height = size + SUB // 4
+    peers, capacity, pieces, _ = outgoing.shape
+    slots, width = peers * capacity, pieces * 128
     subs = size // SUB
     bf16 = jnp.bfloat16
     return pl.pallas_call(
@@ -730,7 +779,7 @@
             jax.ShapeDtypeStruct((slots, width), bf16),
         ],
         grid=(16,),
-        in_specs=[HBM] * 3 + [VMEM] + [HBM] * 7 + [VMEM] * 2,
+        in_specs=[HBM] * 4 + [VMEM] + [HBM] * 8 + [VMEM] * 2,
         out_specs=[VMEM, VMEM],
         scratch_shapes=[
             pltpu.VMEM((heads, subs, 256, queries), bf16),
@@ -739,13 +788,14 @@
             pltpu.VMEM((8, queries), jnp.float32),
             pltpu.VMEM((heads, VDIM + 16, queries), jnp.float32),
             pltpu.VMEM((64, height, wide), bf16),
+            pltpu.VMEM((16, slots // 4, pieces, 128), bf16),
             pltpu.VMEM((16, slots // 4, width), bf16),
-            pltpu.VMEM((16, slots // 4, width), bf16),
-            pltpu.VMEM(latents.shape, bf16),
-            pltpu.VMEM(qlat.shape, bf16),
         ]
+        + [pltpu.VMEM((groups, *a.shape), bf16) for a in (key_lat, wide_turn)]
+        + [pltpu.VMEM((groups, key_lat.shape[0], query_down.shape[1]), bf16)]
         + [pltpu.VMEM(a.shape, bf16) for a in mats]
-        + [DMA((13,)), DMA((12,)), DMA((12,)), DMA((72,)), DMA((72,))]
+        + [pltpu.VMEM(hidden.shape, bf16)]
+        + [DMA((n,)) for n in (35, 18, 18, peers - 1, peers - 1, 12, 12, 72, 72)]
         + fold_scratch(slots, width),
         compiler_params=pltpu.CompilerParams(
             dimension_semantics=("arbitrary",),
@@ -754,7 +804,17 @@
             has_side_effects=True,
         ),
         cost_estimate=pl.CostEstimate(flops=10**11, bytes_accessed=10**7, transcendentals=10**7),
-    )(x, latents, qlat, turned, *mats, cosine, sine)
+    )(
+        key_lat,
+        wide_turn,
+        hidden,
+        query_down,
+        query_gain.reshape(1, -1),
+        outgoing,
+        *mats,
+        cosine,
+        sine,
+    )
 
 
 def norm_rows(values, gain):
@@ -807,9 +867,6 @@
     group_base = lax.axis_index("ep") * groups * tok_rows
     offset = group_base + lax.axis_index("tp") * tok_rows
     hidden = norm_rows(mixer_input, mixer_gain).astype(jnp.bfloat16)
-    query_lat = norm_rows(
-        jnp.dot(hidden, query_down, preferred_element_type=jnp.float32), query_gain
-    ).astype(jnp.bfloat16)
     key_lat = norm_rows(
         jnp.dot(hidden, latent_down, preferred_element_type=jnp.float32), latent_gain
     ).astype(jnp.bfloat16)
@@ -836,13 +893,11 @@
         .astype(jnp.bfloat16)
         .reshape(experts, capacity, expert_hidden.shape[1] // 128, 128)
     )
-    wide_turn = jnp.pad(key_turn, ((0, 0), (0, 128 - ROPE)))
-    latents, turned, qlat, received = exchange((key_lat, wide_turn, query_lat), outgoing)
+    strip = lax.axis_index("tp") % 2 * 2 + jnp.arange(tok_rows, dtype=jnp.int32)[:, None] // SUB
+    lane = jnp.arange(128, dtype=jnp.int32)[None, :] // ROPE
+    wide_turn = jnp.where(lane == strip, jnp.tile(key_turn, (1, 128 // ROPE)), 0)
+    wide_turn = wide_turn.astype(jnp.bfloat16)
     count = groups * tok_rows
-    latents = latents.reshape(count, latents.shape[2])
-    qlat = qlat.reshape(count, qlat.shape[2])
-    turned = turned[:, :, :ROPE].reshape(2, 4, 4, 16, ROPE).transpose(0, 3, 2, 1, 4)
-    turned = turned.reshape(2, 16, 4 * 4 * ROPE)
     all_cos, all_sin = turn_tables(group_base + jnp.arange(count, dtype=jnp.int32), ROPE)
     width = expert_hidden.shape[1]
     mats = (
@@ -855,7 +910,7 @@
         down_proj[0],
     )
     attended, sums = core(
-        received.reshape(slots, width), latents, qlat, turned, mats, all_cos.T, all_sin.T
+        key_lat, wide_turn, hidden, query_down, query_gain, outgoing, mats, all_cos.T, all_sin.T
     )
     mixed = lax.dot_general(
         attended, output_proj, (((0,), (0,)), ((), ())), preferred_element_type=jnp.float32

time: 182 us -> 164 us (0.901)
  Pallas kernels: 158 us -> 145 us
  matrix products: 8.71 us -> 3.53 us
  local copies, waits for them, and re-layouts: 8.2 us -> 5.71 us
  other arithmetic: 6.08 us -> 8.55 us
    pallas_call x1 -> x0, Pallas kernels: 30.4 us -> none  [exchange(): pl.pallas_call(functools.partial(exchange_kernel, count), out_shape=[jax....]
    pallas_call x1, Pallas kernels: 100 us -> 119 us  [core(): pl.pallas_call(core_kernel, out_shape=[jax.ShapeDtypeStruct((heads * VDIM...]
    dot_general x1 -> x0, matrix products: 4.04 us -> none  [on_device(): jnp.dot(hidden, query_down, preferred_element_type=jnp.float32)]
    unnamed x36 -> x29, local copies, waits for them, and re-layouts: 5.42 us -> 3.22 us
where the time goes in v5:
time: 164 us; the launch traced here: 163 us
  Pallas kernels  145 us (88%)
  other arithmetic  8.55 us (5%)
  local copies, waits for them, and re-layouts  5.71 us (3%)
  matrix products  3.53 us (2%)
    pallas_call x1, Pallas kernels, core(): pl.pallas_call(core_kernel, out_shape=[jax.ShapeDtypeStruct((heads * VDIM...  119 us
    pallas_call x1, Pallas kernels, finish(): pl.pallas_call(finish_kernel, out_shape=[jax.ShapeDtypeStruct((count, wid...  25.7 us

profile of v5, /device:TPU:1, one launch (start us, length us, event | category | flops | bytes accessed | tf_op | source)
XLA Modules:
  0.0 163.2 jit_solution(4262487481273560835)
XLA Ops:
  0.6 0.0 copy-start
  0.7 1.3 fusion.2
  2.0 1.2 fusion.4.hidden_in
  3.3 0.0 copy-done
  3.3 0.0 copy-start.2
  3.3 0.3 fusion.28
  3.6 0.1 fusion.23
  3.8 0.1 copy.39
  3.9 0.7 compare_select_fusion.wide_turn
  4.6 0.0 copy-done.9
  4.6 0.1 copy.40
  4.7 0.1 eq.60
  4.8 0.6 reduce-window.6
  5.4 0.2 slice_reduce_fusion
  5.7 0.1 eq.56
  5.8 0.1 fusion.16
  5.9 0.1 reduce_sum.61
  6.1 0.1 copy.43
  6.1 0.1 fusion.13
  6.2 0.0 copy-done.4
  6.2 0.2 fusion.5
  6.4 0.0 copy-done.6
  6.4 0.0 copy-start.3
  6.4 0.6 fusion.1
  7.0 1.4 copy.47
  8.4 0.0 copy-done.2
  8.4 0.6 multiply_reduce_fusion.1
  8.9 0.1 copy-done.10
  9.0 0.7 multiply_convert_fusion.key_lat
  9.8 0.8 multiply_sine_fusion
  10.6 0.0 copy-done.8
  10.6 0.6 reshape.233.query_gain
  11.2 118.8 %shard_map.212 = (bf16[256,512]{1,0:T(8,128)(2,1)}, bf16[320,2048]{1,0:T(8,128)(2,1)}) custom-call(bf16[128,512]{1,0:T(8,128)(2,1)} %multiply_convert_fusion.key_lat, bf16[128,128]{1,0:T(8,128)(2,1)} %compare_select_fusion.wide_turn, bf16[128,2048]{1,0:T(8,128)(2,1)} %copy-done.2, bf16[2048,1536]{1,0:T(8,128)(2,1)} %query_down.1, ...), custom_call_target="tpu_custom_call" | custom-call | flops 99999997952 | bytes 10000000 | tf_op jit(solution)/shard_map/pallas_call | solution.py:775
  130.1 2.1 %convolution_convert_fusion = bf16[512,2048]{1,0:T(8,128)(2,1)S(1)} fusion(bf16[256,512]{1,0:T(8,128)(2,1)} %get-tuple-element.6, bf16[256,2048]{1,0:T(8,128)(2,1)} %param.33), kind=kOutput, calls=%fused_computation.1 | convolution fusion | flops 537919488 | bytes 3407872 | tf_op jit(solution)/shard_map/dot_general | solution.py:915
  132.2 0.0 copy-start.1
  132.2 0.3 copy.48
  132.5 0.4 copy-done.1
  132.9 25.7 %shard_map.213 = (bf16[128,2048]{1,0:T(8,128)(2,1)S(1)}, bf16[32,10,16,128]{3,2,1,0:T(8,128)(2,1)S(1)}) custom-call(bf16[4,128,2048]{2,1,0:T(8,128)(2,1)S(1)} %bitcast.52, f32[1,2048]{1,0:T(1,128)S(1)} %bitcast.55, bf16[32,10,16,128]{3,2,1,0:T(8,128)(2,1)S(1)} %bitcast.53), custom_call_target="tpu_custom_call" | custom-call | flops 10000000000 | bytes 1000000 | tf_op jit(solution)/shard_map/pallas_call | solution.py:403
  158.6 0.0 copy-start.11
  158.6 0.1 copy.44
  158.7 0.1 mul.190
  158.9 0.8 gather_fusion
  159.8 0.0 copy-start.7
  159.8 0.1 copy.45
  159.9 0.3 fusion
  160.2 1.0 multiply_reduce_fusion
  161.3 1.2 fusion.9
  162.5 0.8 copy.53
  (26 shorter events, 0.2 us)
Async XLA Ops:
  0.6 2.6 %copy-start = (bf16[2048,32]{0,1:T(8,128)(2,1)S(1)}, bf16[2048,32]{0,1:T(8,128)(2,1)}, u32[]{:S(2)}) copy-start(bf16[2048,32]{0,1:T(8,128)(2,1)} %param.26) | copy-start | bytes 393220
  0.6 3.9 %copy-start.9 = (s32[128,2]{0,1:T(2,128)S(1)}, s32[128,2]{0,1:T(2,128)}, u32[]{:S(2)}) copy-start(s32[128,2]{0,1:T(2,128)} %param.36) | copy-start | bytes 3076
  0.7 5.5 %copy-start.4 = (bf16[128,2048]{1,0:T(8,128)(2,1)S(1)}, bf16[128,2048]{1,0:T(8,128)(2,1)}, u32[]{:S(2)}) copy-start(bf16[128,2048]{1,0:T(8,128)(2,1)} %param.22) | copy-start | bytes 1572868
  0.7 5.7 %copy-start.6 = (f32[2048]{0:T(1024)S(1)}, f32[2048]{0:T(1024)}, u32[]{:S(2)}) copy-start(f32[2048]{0:T(1024)} %param.35) | copy-start | bytes 24580
  3.3 5.1 %copy-start.2 = (bf16[128,2048]{1,0:T(8,128)(2,1)}, bf16[128,2048]{1,0:T(8,128)(2,1)S(1)}, u32[]{:S(2)}) copy-start(bf16[128,2048]{1,0:T(8,128)(2,1)S(1)} %fusion.4.hidden_in) | copy-start | bytes 1572868
  6.4 2.0 %copy-start.3 = (bf16[2048,512]{1,0:T(8,128)(2,1)S(1)}, bf16[2048,512]{1,0:T(8,128)(2,1)}, u32[]{:S(2)}) copy-start(bf16[2048,512]{1,0:T(8,128)(2,1)} %param.25) | copy-start | bytes 6291460
  8.4 0.7 copy-start.10
  8.4 2.3 %copy-start.8 = (f32[1536]{0:T(1024)S(1)}, f32[1536]{0:T(1024)}, u32[]{:S(2)}) copy-start(f32[1536]{0:T(1024)} %param.27) | copy-start | bytes 18436
  130.1 2.2 %copy-start.5 = (bf16[320,2048]{1,0:T(8,128)(2,1)S(1)}, bf16[320,2048]{1,0:T(8,128)(2,1)}, u32[]{:S(2)}) copy-start(bf16[320,2048]{1,0:T(8,128)(2,1)} %get-tuple-element.7) | copy-start | bytes 3932164
  132.2 0.7 copy-start.1
  158.6 1.1 copy-start.11
  159.8 1.5 copy-start.7
